TPU v7x, 512 devices: a whole 4x8x8 slice. The times are simulated.
512 devices in a mesh: sp: 64 (over z, y), tp: 8 (over x, core).
Axes of the slice: x: 4, y: 8, z: 8, core: 2. Of those that a mesh axis runs over, the one named last changes fastest.
Arguments:
- tokens: bfloat16 [14336, 2048], P('sp', 'tp'), may hold values from -6 to 6
- norm_gain: float32 [2048], replicated, may hold values from 0.1 to 1.9
- query_weight: bfloat16 [2048, 2048], P('sp', 'tp'), may hold values from -0.125 to 0.125
- key_weight: bfloat16 [2048, 1024], P('sp', 'tp'), may hold values from -0.125 to 0.125
- value_weight: bfloat16 [2048, 1024], P('sp', 'tp'), may hold values from -0.125 to 0.125
- glu_value_weight: bfloat16 [2048, 1536], P('sp', 'tp'), may hold values from -0.125 to 0.125
- glu_gate_weight: bfloat16 [2048, 1536], P('sp', 'tp'), may hold values from -0.125 to 0.125
- query_gain: float32 [64], replicated, may hold values from 1.2 to 1.6
- key_gain: float32 [64], replicated, may hold values from 1.1 to 1.4
- lambdas: float32 [16], P('tp'), may hold values from 0.3 to 0.8
- head_gain: float32 [128], replicated, may hold values from 0.1 to 1.9
- conv_weight: float32 [31, 1536], P(None, 'tp'), may hold values from -11 to 11
- channel_gain: float32 [1536], P('tp'), may hold values from 0.1 to 1.9
- attn_out_weight: bfloat16 [2048, 2048], P('sp', 'tp'), may hold values from -0.09375 to 0.09375
- conv_out_weight: bfloat16 [2048, 1536], P('sp', 'tp'), may hold values from -0.09375 to 0.09375
Outputs:
- mixed: bfloat16 [14336, 2048], P(('sp', 'tp'))
All inputs are finite; a program needn't handle non-finite values.
Results may differ from a plain program's by a relative error of at most 0.014.
Values may be sent and summed in bfloat16 or wider, within the bound.
No kernel may reach another device: no remote copies, remote signals or barrier semaphores. Data moves between devices by JAX's collectives and lax.ppermute only.
A program may use at most 64 MiB of HBM per device.

v0:
```python
import jax
import jax.numpy as jnp
from jax import lax
from jax.sharding import Mesh
from jax.sharding import PartitionSpec as P

HEAD_DIM = 64
C_CH = 1536
CONV_W = 31
TP = ("tp_0", "tp_1")
SP_TP = ("sp", "tp_0", "tp_1")


EPS = 1e-06
LAMBDA_INIT = 0.2


def joined_along(parts, dim):
    parts = jnp.moveaxis(parts, 0, dim)
    lengths = parts.shape
    return parts.reshape(*lengths[:dim], lengths[dim] * lengths[dim + 1], *lengths[dim + 2 :])


def all_blocks(array, axes, sequence):
    parts = array[None]
    for k in sequence:
        parts = lax.all_gather(parts, axes[k], axis=0, tiled=True)
    carried = [lax.axis_size(axes[k]) for k in reversed(sequence)]
    parts = parts.reshape(*carried, *array.shape)
    turned = sorted(range(len(sequence)), key=lambda place: sequence[len(sequence) - 1 - place])
    return parts.transpose(*turned, *range(len(sequence), parts.ndim)).reshape(-1, *array.shape)


def gather_axes(array, axes, sequence, dim):
    return joined_along(all_blocks(array, axes, sequence), dim)


def side_by_side(arrays, axis, dim, along):
    widths = [a.shape[along] for a in arrays]
    both = jnp.concatenate(arrays, axis=along)
    whole = lax.all_gather(both, axis, axis=dim, tiled=True)
    return tuple(jnp.split(whole, [sum(widths[:k]) for k in range(1, len(widths))], axis=along))


def with_halo(cells, sides, width):
    for axis, dim in sides:
        count = lax.axis_size(axis)
        ends = count - 1
        head = lax.slice_in_dim(cells, 0, width, axis=dim)
        tail = lax.slice_in_dim(cells, cells.shape[dim] - width, cells.shape[dim], axis=dim)
        cells = jnp.concatenate(
            [
                lax.ppermute(tail, axis, [(i, (i + 1) % count) for i in range(ends)]),
                cells,
                lax.ppermute(head, axis, [((i + 1) % count, i) for i in range(ends)]),
            ],
            axis=dim,
        )
    return cells


def copy_for_each(array, axis):
    copies = jnp.broadcast_to(array, (lax.axis_size(axis), *array.shape))
    return lax.all_to_all(copies, axis, split_axis=0, concat_axis=0, tiled=True)


def taken_together(array, axis):
    everything = copy_for_each(array, axis)
    return jnp.sum(everything, axis=0)


def split_up(array, dim, count):
    lengths = array.shape
    parts = array.reshape(*lengths[:dim], count, lengths[dim] // count, *lengths[dim + 1 :])
    return jnp.moveaxis(parts, dim, 0)


def sent_and_summed(array, axis, dim):
    parts = split_up(array, dim, lax.axis_size(axis))
    arrived = lax.all_to_all(parts, axis, split_axis=0, concat_axis=0, tiled=True)
    return arrived.astype(jnp.float32).sum(axis=0)


def rms_scale(values, gain):
    return values * lax.rsqrt(jnp.mean(values * values, axis=-1, keepdims=True) + EPS) * gain


def contract_last(left, right):
    return lax.dot_general(
        left, right, (((1,), (1,)), ((), ())), preferred_element_type=jnp.float32
    )


def local(
    tokens,
    norm_gain,
    query_weight,
    key_weight,
    value_weight,
    glu_value_weight,
    glu_gate_weight,
    query_gain,
    key_gain,
    lambdas,
    head_gain,
    conv_weight,
    channel_gain,
    attn_out_weight,
    conv_out_weight,
):
    gathered = gather_axes(tokens, TP, (0, 1), 1).astype(jnp.float32)
    normed = rms_scale(gathered, norm_gain).astype(jnp.bfloat16)
    tok_rows, model_width = normed.shape
    pieces = side_by_side(
        (query_weight, key_weight, value_weight, glu_value_weight, glu_gate_weight), "sp", 0, 1
    )
    projected = tuple(
        (jnp.dot(normed, w_piece, preferred_element_type=jnp.float32) for w_piece in pieces)
    )
    q_heads = query_weight.shape[1] // (2 * HEAD_DIM)
    kv_heads = key_weight.shape[1] // (2 * HEAD_DIM)
    group = q_heads // kv_heads
    queries = projected[0].reshape(tok_rows, q_heads, 2, HEAD_DIM)
    query_normed = rms_scale(queries, query_gain).astype(jnp.bfloat16)
    query_blocks = query_normed.reshape(tok_rows, kv_heads, group, 2, HEAD_DIM).transpose(
        1, 2, 3, 0, 4
    )
    keys = projected[1].reshape(tok_rows, kv_heads, 2, HEAD_DIM)
    key_rows = (
        rms_scale(keys, key_gain).astype(jnp.bfloat16).reshape(tok_rows, kv_heads * 2 * HEAD_DIM)
    )
    value_rows = projected[2].astype(jnp.bfloat16)

    def attend_block(carry, key_block, value_block):
        run_max, run_sum, numer = carry
        key_count = key_block.shape[0]
        key_heads = key_block.reshape(key_count, kv_heads, 2, HEAD_DIM).transpose(1, 2, 0, 3)
        value_heads = value_block.reshape(key_count, kv_heads, 2 * HEAD_DIM).transpose(1, 0, 2)
        scores = jnp.einsum(
            "kgprd,kpnd->kgprn", query_blocks, key_heads, preferred_element_type=jnp.float32
        ) * HEAD_DIM ** (-0.5)
        new_max = jnp.maximum(run_max, jnp.max(scores, axis=-1))
        expo = jnp.exp(scores - new_max[..., None])
        factor = jnp.exp(run_max - new_max)
        run_sum = run_sum * factor + jnp.sum(expo, axis=-1)
        numer = numer * factor[..., None] + jnp.einsum(
            "kgprn,knd->kgprd",
            expo.astype(jnp.bfloat16),
            value_heads,
            preferred_element_type=jnp.float32,
        )
        return (new_max, run_sum, numer)

    start_carry = (
        jnp.full((kv_heads, group, 2, tok_rows), -jnp.inf, jnp.float32),
        jnp.zeros((kv_heads, group, 2, tok_rows), jnp.float32),
        jnp.zeros((kv_heads, group, 2, tok_rows, 2 * HEAD_DIM), jnp.float32),
    )
    carry = start_carry
    pieces = side_by_side((key_rows, value_rows), "sp", 0, 1)
    key_count = pieces[0].shape[0]
    step_rows = key_count
    while step_rows > 1024 and step_rows % 2 == 0:
        step_rows = step_rows // 2
    turn_count = key_count // step_rows
    key_steps = pieces[0].reshape(turn_count, step_rows, pieces[0].shape[1])
    value_steps = pieces[1].reshape(turn_count, step_rows, pieces[1].shape[1])

    def one_turn(inner, both):
        return (attend_block(inner, both[0], both[1]), None)

    carry, unused = lax.scan(one_turn, carry, (key_steps, value_steps))
    run_max, run_sum, numer = carry
    ratio = numer / run_sum[..., None]
    weight_two = lambdas.reshape(kv_heads, group, 1, 1)
    difference = ratio[:, :, 0] - weight_two * ratio[:, :, 1]
    att_rows = difference.transpose(2, 0, 1, 3).reshape(tok_rows, q_heads, 2 * HEAD_DIM)
    att_normed = (rms_scale(att_rows, head_gain) * (1.0 - LAMBDA_INIT)).astype(jnp.bfloat16)
    att_out = att_normed.reshape(tok_rows, q_heads * 2 * HEAD_DIM)
    glu_rows = (projected[3] * jax.nn.sigmoid(projected[4])).astype(jnp.bfloat16)
    padded = with_halo(glu_rows, (("sp", 0),), CONV_W // 2)
    conv_sum = jnp.zeros((tok_rows, glu_rows.shape[1]), jnp.float32)
    for offset in range(CONV_W):
        conv_sum = conv_sum + conv_weight[offset] * padded[offset : offset + tok_rows].astype(
            jnp.float32
        )
    squares = taken_together(jnp.sum(conv_sum * conv_sum, axis=1), TP)
    scaled = conv_sum * lax.rsqrt(squares / C_CH + EPS)[:, None] * channel_gain
    conv_out = jax.nn.silu(scaled).astype(jnp.bfloat16)
    pieces = side_by_side((attn_out_weight, conv_out_weight), "sp", 0, 1)
    partial_term = contract_last(att_out, pieces[0]) + contract_last(conv_out, pieces[1])
    return sent_and_summed(partial_term.astype(jnp.bfloat16), TP, 0).astype(jnp.bfloat16)


def solution(mesh):
    finer = Mesh(mesh.devices.reshape(mesh.shape["sp"], 4, 2), ("sp", "tp_0", "tp_1"))
    placed = (
        P("sp", TP),
        P(),
        P("sp", TP),
        P("sp", TP),
        P("sp", TP),
        P("sp", TP),
        P("sp", TP),
        P(),
        P(),
        P(TP),
        P(),
        P(None, TP),
        P(TP),
        P("sp", TP),
        P("sp", TP),
    )
    return jax.shard_map(
        local, mesh=finer, in_specs=placed, out_specs=P(SP_TP, None), check_vma=False
    )
```

profile of v0, /device:TPU:1, one launch (start us, length us, event | category | flops | bytes accessed | tf_op | source)
XLA Modules:
  0.0 311.4 jit_solution(12068846682396332455)
XLA Ops:
  8.9 11.1 %all-gather = bf16[896,256]{1,0:T(8,128)(2,1)S(1)} all-gather(bf16[224,256]{1,0:T(8,128)(2,1)} %param.17), channel_id=2, replica_groups=mesh['sp'=64,'tp_0'=4,'tp_1'=2] {'tp_0'}, dimensions={0}, use_global_device_ids=true | all-gather | bytes 573440 | tf_op jit(solution)/shard_map/all_gather | solution.py:27
  20.0 10.6 %all_gather.16 = bf16[8,224,256]{2,1,0:T(8,128)(2,1)S(1)} all-gather(bf16[4,224,256]{2,1,0:T(8,128)(2,1)S(1)} %bitcast.182), channel_id=1, replica_groups=mesh['sp'=64,'tp_0'=4,'tp_1'=2] {'tp_1'}, dimensions={0}, use_global_device_ids=true | all-gather | bytes 1376256 | tf_op jit(solution)/shard_map/all_gather | solution.py:27
  31.9 65.8 %all-gather.5.cloned.1.call-done = bf16[2048,896]{1,0:T(8,128)(2,1)} async-done(((bf16[32,896]{1,0:T(8,128)(2,1)}), bf16[2048,896]{1,0:T(8,128)(2,1)}) %all-gather.5.cloned.1.call-update) | async-done | bytes 3670032 | tf_op jit(solution)/shard_map/all_gather | solution.py:41
  107.3 2.4 fusion.21
  109.7 1.8 fusion.22
  111.6 2.7 collective-permute-start
  116.1 3.0 collective-permute-done.1
  119.1 2.5 multiply_reduce_fusion.3
  122.2 10.6 %all-to-all-start = ((f32[8,1,224]{2,1,0:T(1,128)}), f32[8,1,224]{2,1,0:T(1,128)S(1)}, u32[]{:S(2)}, u32[]{:S(2)}) async-start(f32[8,1,224]{2,1,0:T(1,128)} %broadcast_in_dim.16), calls=%async_computation | async-start | bytes 16384 | tf_op jit(solution)/shard_map/all_to_all | solution.py:64
  132.9 4.5 %all-to-all-done = f32[8,1,224]{2,1,0:T(1,128)S(1)} async-done(((f32[8,1,224]{2,1,0:T(1,128)}), f32[8,1,224]{2,1,0:T(1,128)S(1)}, u32[]{:S(2)}, u32[]{:S(2)}) %all-to-all-start) | async-done | bytes 7200 | tf_op jit(solution)/shard_map/all_to_all | solution.py:64
  137.4 59.4 %all-gather.7.cloned.1.call-done = bf16[14336,256]{1,0:T(8,128)(2,1)} async-done(((bf16[224,256]{1,0:T(8,128)(2,1)}), bf16[14336,256]{1,0:T(8,128)(2,1)}) %all-gather.7.cloned.1.call-update) | async-done | bytes 7340048 | tf_op jit(solution)/shard_map/all_gather | solution.py:41
  196.8 5.2 %fusion.78 = (bf16[14336,128]{1,0:T(8,128)(2,1)}, bf16[14336,128]{1,0:T(8,128)(2,1)}) fusion(bf16[14336,256]{1,0:T(8,128)(2,1)} %all-gather.7.cloned.1.call-done), kind=kLoop, calls=%fused_computation.156 | loop fusion | bytes 14680064 | tf_op jit(solution)/shard_map/split | solution.py:42
  202.0 70.1 %while.15 = (s32[]{:T(128)}, f32[1,2,2,224]{3,1,2,0:T(2,128)S(1)}, f32[1,2,2,224]{3,1,2,0:T(2,128)S(1)}, f32[1,2,2,224,128]{4,3,2,1,0:T(8,128)S(1)}, bf16[16,896...) while((s32[]{:T(128)}, f32[1,2,2,224]{3,1,2,0:T(2,128)S(1)}, ...), condition=%wide.region_6.7_spmd.clone, body=%wide.region_3.6_spmd.clone.sunk | while | flops 313447680 | bytes 12103289 | solution.py:172
  204.8 1.6 fusion.100
  209.2 1.6 fusion.100
  213.5 1.6 fusion.100
  217.9 1.6 fusion.100
  222.3 1.6 fusion.100
  226.7 1.6 fusion.100
  231.1 1.6 fusion.100
  235.5 1.6 fusion.100
  239.8 1.6 fusion.100
  244.2 1.6 fusion.100
  248.6 1.6 fusion.100
  253.0 1.6 fusion.100
  257.4 1.6 fusion.100
  261.8 1.6 fusion.100
  266.2 1.6 fusion.100
  270.5 1.6 fusion.100
  273.0 4.1 %all-gather.9.cloned.1.call-done = bf16[2048,448]{1,0:T(8,128)(2,1)} async-done(((bf16[32,448]{1,0:T(8,128)(2,1)}), bf16[2048,448]{1,0:T(8,128)(2,1)}) %all-gather.9.cloned.1.call-update) | async-done | bytes 1835024 | tf_op jit(solution)/shard_map/all_gather | solution.py:41
  277.3 1.9 fusion.26
  280.0 23.9 %all_to_all.11 = bf16[8,28,2048]{2,1,0:T(8,128)(2,1)S(1)} all-to-all(bf16[8,28,2048]{2,1,0:T(8,128)(2,1)S(1)} %reshape.184), channel_id=1, replica_groups=mesh['sp'=64,'tp_0'=4,'tp_1'=2] {'tp_0','tp_1'}, dimensions={0} | all-to-all | bytes 1835008 | tf_op jit(solution)/shard_map/all_to_all | solution.py:80
  (207 shorter events, 62.0 us)
Async XLA Ops:
  6.5 95.9 %copy-start = (f32[128]{0:T(128)S(1)}, f32[128]{0:T(128)}, u32[]{:S(2)}) copy-start(f32[128]{0:T(128)} %param.27) | copy-start | bytes 1540
  6.5 91.2 %all-gather.5.cloned.1.call-start = ((), (), s32[]{:S(2)}) async-start(), calls=%async_computation.2 | async-start | bytes 3727360 | tf_op jit(solution)/shard_map/all_gather | solution.py:41
  8.1 188.8 %all-gather.7.cloned.1.call-start = ((), (), s32[]{:S(2)}) async-start(), calls=%async_computation.3 | async-start | bytes 7454720 | tf_op jit(solution)/shard_map/all_gather | solution.py:41
  30.9 0.7 copy-start.4
  31.9 69.8 %copy-start.6 = (bf16[32,192]{1,0:T(8,128)(2,1)S(1)}, bf16[32,192]{1,0:T(8,128)(2,1)}, u32[]{:S(2)}) copy-start(bf16[32,192]{1,0:T(8,128)(2,1)} %param.31) | copy-start | bytes 36868
  31.9 69.8 %copy-start.7 = (bf16[32,256]{1,0:T(8,128)(2,1)S(1)}, bf16[32,256]{1,0:T(8,128)(2,1)}, u32[]{:S(2)}) copy-start(bf16[32,256]{1,0:T(8,128)(2,1)} %param.30) | copy-start | bytes 49156
  31.9 70.5 %copy-start.5 = (f32[31,192]{1,0:T(8,128)S(1)}, f32[31,192]{1,0:T(8,128)}, u32[]{:S(2)}) copy-start(f32[31,192]{1,0:T(8,128)} %param.28) | copy-start | bytes 71428
  101.6 175.4 %all-gather.9.cloned.1.call-start = ((), (), s32[]{:S(2)}) async-start(), calls=%async_computation.4 | async-start | bytes 2129920 | tf_op jit(solution)/shard_map/all_gather | solution.py:41
  107.3 8.3 %copy-start.2 = (bf16[256,2048]{1,0:T(8,128)(2,1)S(1)}, bf16[256,2048]{1,0:T(8,128)(2,1)}, u32[]{:S(2)}) copy-start(bf16[256,2048]{1,0:T(8,128)(2,1)} %copy.93) | copy-start | bytes 3145732
  107.3 8.3 %copy-start.3 = (bf16[224,2048,1,1]{1,0,2,3:T(8,128)(2,1)S(1)}, bf16[224,2048,1,1]{1,0,2,3:T(8,128)(2,1)}, u32[]{:S(2)}) copy-start(bf16[224,2048,1,1]{1,0,2,3:T(8,128)(2,1)} %reshape.198) | copy-start | bytes 2752516
  111.5 21.3 %copy-start.9 = (f32[64]{0:T(128)S(1)}, f32[64]{0:T(128)}, u32[]{:S(2)}) copy-start(f32[64]{0:T(128)} %param.24) | copy-start | bytes 772
  111.6 4.5 %collective-permute-start = (bf16[15,192]{0,1:T(8,128)(2,1)S(1)}, bf16[15,192]{0,1:T(8,128)(2,1)S(1)}, u32[]{:S(2)}, u32[]{:S(2)}) collective-permute-start(bf16[15,192]{0,1:T(8,128)(2,1)S(1)} %get-tuple-element.144), channel_id=1, source_target_pairs={{0,8},{8,16},{16,24},{24,32},{32,40},{40,48},{48,56},{56,64},{64,7... | collective-permute-start | bytes 17288 | tf_op jit(solution)/shard_map/ppermute | solution.py:53
  114.3 4.8 %collective-permute-start.1 = (bf16[15,192]{0,1:T(8,128)(2,1)S(1)}, bf16[15,192]{0,1:T(8,128)(2,1)S(1)}, u32[]{:S(2)}, u32[]{:S(2)}) collective-permute-start(bf16[15,192]{0,1:T(8,128)(2,1)S(1)} %get-tuple-element.145), channel_id=1, source_target_pairs={{8,0},{16,8},{24,16},{32,24},{40,32},{48,40},{56,48},{64,56},{72,6... | collective-permute-start | bytes 17288 | tf_op jit(solution)/shard_map/ppermute | solution.py:55
  122.2 15.2 %all-to-all-start = ((f32[8,1,224]{2,1,0:T(1,128)}), f32[8,1,224]{2,1,0:T(1,128)S(1)}, u32[]{:S(2)}, u32[]{:S(2)}) async-start(f32[8,1,224]{2,1,0:T(1,128)} %broadcast_in_dim.16), calls=%async_computation | async-start | bytes 16384 | tf_op jit(solution)/shard_map/all_to_all | solution.py:64
  202.0 70.4 %copy-start.10 = (f32[2]{0:T(128)S(1)}, f32[2]{0:T(128)}, u32[]{:S(2)}) copy-start(f32[2]{0:T(128)} %param.26) | copy-start | bytes 28
  272.8 6.4 %copy-start.8 = (f32[192]{0:T(256)S(1)}, f32[192]{0:T(256)}, u32[]{:S(2)}) copy-start(f32[192]{0:T(256)} %param.29) | copy-start | bytes 2308
  277.0 2.2 copy-start.1
Sparse Core Ops, SparseCore 0:
  10.3 87.3 all-gather.4
  101.7 95.0 all-gather.6
  199.9 77.0 all-gather.8
where the time goes:
time: 313 us; the launch traced here: 311 us
  waiting for transfers between devices  137 us (44%)
  matrix products  47.6 us (15%)
  blocking collectives  45.7 us (15%)
  local copies, waits for them, and re-layouts  32.5 us (10%)
  other arithmetic  19.6 us (6%)
  starting transfers between devices  14.7 us (5%)
  between operations  13.5 us (4%)
    all_gather x3, waiting for transfers between devices, side_by_side(): whole = lax.all_gather(both, axis, axis=dim, tiled=True)  129 us
    dot_general x16, matrix products, attend_block(): jnp.einsum('kgprn,knd->kgprd', expo.astype(jnp.bfloat16), value_heads, pr...  25.5 us
    all_to_all x1, blocking collectives, sent_and_summed(): lax.all_to_all(parts, axis, split_axis=0, concat_axis=0, tiled=True)  23.9 us
    all_gather x2, blocking collectives, all_blocks(): parts = lax.all_gather(parts, axes[k], axis=0, tiled=True)  21.8 us
    dynamic_slice x32, local copies, waits for them, and re-layouts, local(): carry, unused = lax.scan(one_turn, carry, (key_steps, value_steps))  18 us
    another operation x16, other arithmetic  13.1 us
    dot_general x16, matrix products, attend_block(): jnp.einsum('kgprd,kpnd->kgprn', query_blocks, key_heads, preferred_elemen...  12 us
    all_to_all x1, starting transfers between devices, copy_for_each(): return lax.all_to_all(copies, axis, split_axis=0, concat_axis=0, tiled=True)  10.6 us
  transfers between devices with their start and end apart: 6, of which 5 were waited for; matrix products, arithmetic and copies ran while one was open for 29% of the time, Pallas kernels for 0%

commit v1 on v0

v1 whole, which is shorter than its diff:
```python
import functools
import math

import jax
import jax.numpy as jnp
from jax import lax
from jax.experimental import pallas as pl
from jax.experimental.pallas import tpu as pltpu
from jax.sharding import Mesh
from jax.sharding import PartitionSpec as P

HEAD_DIM = 64
C_CH = 1536
CONV_W = 31
TP = ("x", "c")
SP_TP = ("sp", "x", "c")
EPS = 1e-06
LAMBDA_INIT = 0.2
BF = jnp.bfloat16
F32 = jnp.float32


def rms_scale(values, gain):
    return values * lax.rsqrt(jnp.mean(values * values, axis=-1, keepdims=True) + EPS) * gain


def contract_last(left, right):
    return lax.dot_general(left, right, (((1,), (1,)), ((), ())), preferred_element_type=F32)


def attend_kernel(q_ref, k_ref, v_ref, o_ref, *, rows, keys):
    @pl.when(pl.program_id(0) == 0)
    def _():
        o_ref[...] = jnp.zeros_like(o_ref)

    ones = jnp.ones((keys, 2 * HEAD_DIM), BF)
    for j in range(k_ref.shape[0] // keys):
        k = k_ref[j * keys : (j + 1) * keys, :]
        v = jnp.concatenate([v_ref[j * keys : (j + 1) * keys, :], ones], axis=1)
        for r in range(q_ref.shape[0] // rows):
            part = pl.ds(r * rows, rows)
            s = contract_last(q_ref[part, :], k)
            e = jnp.exp2(s).astype(BF)
            o_ref[part, :] += jnp.dot(e, v, preferred_element_type=F32)


def attend(q_rows, kv, block, rows, keys):
    count, total = q_rows.shape[0], kv.shape[0]
    width = 2 * HEAD_DIM
    return pl.pallas_call(
        functools.partial(attend_kernel, rows=rows, keys=keys),
        grid=(total // block,),
        in_specs=[
            pl.BlockSpec((count, width), lambda i: (0, 0)),
            pl.BlockSpec((block, width), lambda i: (i, 0)),
            pl.BlockSpec((block, width), lambda i: (i, 1)),
        ],
        out_specs=pl.BlockSpec((count, 2 * width), lambda i: (0, 0)),
        out_shape=jax.ShapeDtypeStruct((count, 2 * width), F32),
        cost_estimate=pl.CostEstimate(
            flops=6 * count * total * width,
            transcendentals=count * total,
            bytes_accessed=total * 4 * width + count * 10 * width,
        ),
        name="attend",
    )(q_rows, kv, kv)


def local(
    tokens,
    norm_gain,
    query_weight,
    key_weight,
    value_weight,
    glu_value_weight,
    glu_gate_weight,
    query_gain,
    key_gain,
    lambdas,
    head_gain,
    conv_weight,
    channel_gain,
    attn_out_weight,
    conv_out_weight,
):
    weights = (
        query_weight,
        key_weight,
        value_weight,
        glu_value_weight,
        glu_gate_weight,
        attn_out_weight,
        conv_out_weight,
    )
    ends = [0]
    for w in weights:
        ends.append(ends[-1] + w.shape[1])
    gathered_w = lax.all_gather(jnp.concatenate(weights, axis=1), "sp", axis=0, tiled=True)
    wq, wk, wv, wgv, wgg, wao, wco = (
        gathered_w[:, ends[i] : ends[i + 1]] for i in range(len(weights))
    )

    gathered = lax.all_gather(tokens, TP, axis=1, tiled=True).astype(F32)
    normed = rms_scale(gathered, norm_gain).astype(BF)
    tok_rows = normed.shape[0]

    def project(w):
        return jnp.dot(normed, w, preferred_element_type=F32)

    q_heads = query_weight.shape[1] // (2 * HEAD_DIM)
    kv_heads = key_weight.shape[1] // (2 * HEAD_DIM)
    width = 2 * HEAD_DIM
    key_rows = rms_scale(project(wk).reshape(tok_rows, 2 * kv_heads, HEAD_DIM), key_gain)
    kv_rows = jnp.concatenate(
        [key_rows.astype(BF).reshape(tok_rows, width * kv_heads), project(wv).astype(BF)], axis=1
    )
    kv = lax.all_gather(kv_rows, "sp", axis=0, tiled=True)

    fold = math.log2(math.e) * HEAD_DIM ** (-0.5)
    queries = project(wq).reshape(tok_rows, 2 * q_heads, HEAD_DIM)
    q_normed = rms_scale(queries, query_gain * fold).astype(BF).reshape(tok_rows, q_heads, width)
    lane_pair = lax.broadcasted_iota(jnp.int32, (1, width), 1) // HEAD_DIM
    q_rows = jnp.concatenate(
        [
            jnp.where(lane_pair == p, q_normed[:, h], jnp.zeros((), BF))
            for h in range(q_heads)
            for p in range(2)
        ],
        axis=0,
    )
    sums = attend(q_rows, kv, 2048, q_rows.shape[0] // 2, 256)
    sums = sums.reshape(q_heads, 2, tok_rows, 2 * width)
    ratio = sums[..., :width] / sums[..., width:]
    difference = ratio[:, 0] - lambdas.reshape(q_heads, 1, 1) * ratio[:, 1]
    att = (rms_scale(difference, head_gain) * (1.0 - LAMBDA_INIT)).astype(BF)

    glu_rows = (project(wgv) * jax.nn.sigmoid(project(wgg))).astype(BF)
    reach = CONV_W // 2
    count = lax.axis_size("sp")
    up = [(i, i + 1) for i in range(count - 1)]
    padded = jnp.concatenate(
        [
            lax.ppermute(glu_rows[tok_rows - reach :], "sp", up),
            glu_rows,
            lax.ppermute(glu_rows[:reach], "sp", [(b, a) for a, b in up]),
        ],
        axis=0,
    )
    conv_sum = jnp.zeros((tok_rows, glu_rows.shape[1]), F32)
    for offset in range(CONV_W):
        conv_sum = conv_sum + conv_weight[offset] * padded[offset : offset + tok_rows].astype(F32)
    partial_squares = jnp.sum(conv_sum * conv_sum, axis=1)
    eight = lax.axis_size("x") * lax.axis_size("c")
    squares = jnp.sum(
        lax.all_to_all(
            jnp.broadcast_to(partial_squares, (eight, tok_rows)), TP, 0, 0, tiled=True
        ),
        axis=0,
    )
    scaled = conv_sum * lax.rsqrt(squares / C_CH + EPS)[:, None] * channel_gain
    conv_out = jax.nn.silu(scaled).astype(BF)

    term = contract_last(conv_out, wco)
    for h in range(q_heads):
        term = term + contract_last(att[h], wao[:, h * width : (h + 1) * width])
    parts = term.astype(BF).reshape(eight, tok_rows // eight, term.shape[1])
    arrived = lax.all_to_all(parts, TP, 0, 0, tiled=True)
    return arrived.astype(F32).sum(axis=0).astype(BF)


def solution(mesh):
    finer = Mesh(mesh.devices.reshape(mesh.shape["sp"], 4, 2), SP_TP)
    both, rows = P("sp", TP), P()
    placed = (both, rows) + (both,) * 5 + (rows, rows, P(TP), rows, P(None, TP), P(TP), both, both)
    return jax.shard_map(
        local, mesh=finer, in_specs=placed, out_specs=P(SP_TP, None), check_vma=False
    )
```

time: 313 us -> 251 us (0.80)
  matrix products: 47.6 us -> 13.8 us
  local copies, waits for them, and re-layouts: 32.5 us -> 3.76 us
  Pallas kernels: 0 us -> 17.7 us
  other arithmetic: 19.6 us -> 6.71 us
  blocking collectives: 45.7 us -> 40.6 us
    dot_general x37 -> x5, matrix products: 45 us -> 9.05 us  [project(): return jnp.dot(normed, w, preferred_element_type=F32)]
    dynamic_slice x32 -> x0, local copies, waits for them, and re-layouts: 18 us -> none  [local(): carry, unused = lax.scan(one_turn, carry, (key_steps, value_steps))]
    pallas_call x0 -> x1, Pallas kernels: none -> 17.7 us  [attend(): pl.pallas_call(functools.partial(attend_kernel, rows=rows, keys=keys), gr...]
    another operation x16 -> x0, other arithmetic: 13.1 us -> none
    all_gather x3 -> x2, waiting for transfers between devices: 129 us -> 135 us  [the longest x1 72.6 us: local(): lax.all_gather(jnp.concatenate(weights, axis=1), 'sp', axis=0, tiled=True)]
    split x1 -> x0, local copies, waits for them, and re-layouts: 5.2 us -> none  [side_by_side(): jnp.split(whole, [sum(widths[:k]) for k in range(1, len(widths))], axis=a...]
    all_to_all x1, blocking collectives: 23.9 us -> 20.1 us  [local(): arrived = lax.all_to_all(parts, TP, 0, 0, tiled=True)]
    all_gather x2 -> x1, blocking collectives: 21.8 us -> 20.5 us  [local(): gathered = lax.all_gather(tokens, TP, axis=1, tiled=True).astype(F32)]
  transfers between devices with their start and end apart: 6 -> 5, of which waited for: 5 -> 4; matrix products, arithmetic and copies ran while one was open for 29% -> 5% of each run, Pallas kernels for 0% -> 0%
where the time goes in v1:
time: 251 us; the launch traced here: 250 us
  waiting for transfers between devices  140 us (56%)
  blocking collectives  40.6 us (16%)
  Pallas kernels  17.7 us (7%)
  starting transfers between devices  13.8 us (5%)
  matrix products  13.8 us (5%)
  between operations  13.7 us (5%)
  other arithmetic  6.71 us (3%)
  local copies, waits for them, and re-layouts  3.76 us (1%)
    all_gather x1, waiting for transfers between devices, local(): lax.all_gather(jnp.concatenate(weights, axis=1), 'sp', axis=0, tiled=True)  72.6 us
    all_gather x1, waiting for transfers between devices, local(): kv = lax.all_gather(kv_rows, 'sp', axis=0, tiled=True)  62.1 us
    all_gather x1, blocking collectives, local(): gathered = lax.all_gather(tokens, TP, axis=1, tiled=True).astype(F32)  20.5 us
    all_to_all x1, blocking collectives, local(): arrived = lax.all_to_all(parts, TP, 0, 0, tiled=True)  20.1 us
    pallas_call x1, Pallas kernels, attend(): pl.pallas_call(functools.partial(attend_kernel, rows=rows, keys=keys), gr...  17.7 us
    all_to_all x1, starting transfers between devices, local(): lax.all_to_all(jnp.broadcast_to(partial_squares, (eight, tok_rows)), TP,...  9.84 us
    dot_general x5, matrix products, project(): return jnp.dot(normed, w, preferred_element_type=F32)  9.05 us
  transfers between devices with their start and end apart: 5, of which 4 were waited for; matrix products, arithmetic and copies ran while one was open for 5% of the time, Pallas kernels for 0%

profile of v1, /device:TPU:1, one launch (start us, length us, event | category | flops | bytes accessed | tf_op | source)
XLA Modules:
  0.0 250.3 jit_solution(13422578200943392099)
XLA Ops:
  6.5 1.5 concatenate.44
  8.2 0.7 mul.575
  8.9 20.5 %all_gather.9 = bf16[224,2048]{1,0:T(8,128)(2,1)S(1)} all-gather(bf16[224,256]{1,0:T(8,128)(2,1)} %param.15), channel_id=1, replica_groups=mesh['sp'=64,'x'=4,'c'=2] {'x','c'}, dimensions={1}, use_global_device_ids=true | all-gather | bytes 1032192 | tf_op jit(solution)/shard_map/all_gather | solution.py:103
  29.4 0.3 fusion.1
  29.7 72.6 %all-gather.3.cloned.1.call-done = bf16[2048,1344]{1,0:T(8,128)(2,1)} async-done(((bf16[32,1344]{1,0:T(8,128)(2,1)}), bf16[2048,1344]{1,0:T(8,128)(2,1)}) %all-gather.3.cloned.1.call-update) | async-done | bytes 5505040 | tf_op jit(solution)/shard_map/all_gather | solution.py:98
  102.2 1.5 fusion.64
  104.0 1.5 convolution_convert_fusion
  105.5 0.7 pad_maximum_fusion.1
  106.4 2.5 %fusion.6 = f32[224,192]{0,1:T(8,128)S(1)} fusion(bf16[2048,1344]{1,0:T(8,128)(2,1)} %all-gather.3.cloned.1.call-done, bf16[224,2048]{1,0:T(8,128)(2,1)S(1)} %all_gather.9, f32[2048]{0:T(1024)S(1)} %copy-done.4, f32[224]{0:T(256)S(1)} %add_rsqrt_fusion.4), kind=kOutput, calls=%fused_computation.12 | convolution fusion | flops 178124800 | bytes 2147200 | tf_op jit(solution)/shard_map/dot_general | solution.py:108
  108.9 1.8 fusion.7
  110.9 2.7 %collective-permute-start = (bf16[15,192]{0,1:T(8,128)(2,1)S(1)}, bf16[15,192]{0,1:T(8,128)(2,1)S(1)}, u32[]{:S(2)}, u32[]{:S(2)}) collective-permute-start(bf16[15,192]{0,1:T(8,128)(2,1)S(1)} %get-tuple-element.13), channel_id=1, source_target_pairs={{0,8},{8,16},{16,24},{24,32},{32,40},{40,48},{48,56},{56,64},{64,7... | collective-permute-start | bytes 17288 | tf_op jit(solution)/shard_map/ppermute | solution.py:143
  113.5 1.3 collective-permute-start.1
  114.8 1.7 fusion.63
  116.5 0.1 copy.30
  116.8 0.1 copy.32
  117.0 1.5 collective-permute-done.1
  118.5 2.5 multiply_reduce_fusion.1
  121.0 0.6 broadcast_in_dim.43
  121.6 9.8 %all-to-all-start = ((f32[8,1,224]{2,1,0:T(1,128)}), f32[8,1,224]{2,1,0:T(1,128)S(1)}, u32[]{:S(2)}, u32[]{:S(2)}) async-start(f32[8,1,224]{2,1,0:T(1,128)} %broadcast_in_dim.43), calls=%async_computation | async-start | bytes 16384 | tf_op jit(solution)/shard_map/all_to_all | solution.py:155
  131.4 0.7 pad_maximum_fusion.q_ref
  132.1 4.0 %all-to-all-done = f32[8,1,224]{2,1,0:T(1,128)S(1)} async-done(((f32[8,1,224]{2,1,0:T(1,128)}), f32[8,1,224]{2,1,0:T(1,128)S(1)}, u32[]{:S(2)}, u32[]{:S(2)}) %all-to-all-start) | async-done | bytes 7200 | tf_op jit(solution)/shard_map/all_to_all | solution.py:155
  136.1 1.9 fusion.10
  138.0 62.1 %all-gather.5.cloned.1.call-done.k_ref.v_ref = bf16[14336,256]{1,0:T(8,128)(2,1)} async-done(((bf16[224,256]{1,0:T(8,128)(2,1)}), bf16[14336,256]{1,0:T(8,128)(2,1)}) %all-gather.5.cloned.1.call-update) | async-done | bytes 7340048 | tf_op jit(solution)/shard_map/all_gather | solution.py:117
  200.1 17.7 %attend.1 = f32[896,256]{1,0:T(8,128)} custom-call(bf16[896,128]{1,0:T(8,128)(2,1)} %pad_maximum_fusion.q_ref, bf16[14336,256]{1,0:T(8,128)(2,1)} %all-gather.5.cloned.1.call-done.k_ref.v_ref, bf16[14336,256]{1,0:T(8,128)(2,1)} %all-gather.5.cloned.1.call-done.k_ref.v_ref), custom_call_target="tpu_custom_call" | custom-call | flops 9865003008 | bytes 8486912 | tf_op jit(solution)/shard_map/attend/pallas_call | solution.py:50
  217.8 1.2 slice_divide_fusion
  219.1 0.2 multiply_reduce_fusion
  219.3 0.1 multiply_convert_fusion
  219.4 1.4 convolution_add_fusion.1
  220.9 1.4 fusion
  222.3 0.2 reshape.112
  222.5 20.1 %all_to_all.11 = bf16[8,28,2048]{2,1,0:T(8,128)(2,1)S(1)} all-to-all(bf16[8,28,2048]{2,1,0:T(8,128)(2,1)S(1)} %reshape.112), channel_id=1, replica_groups=mesh['sp'=64,'x'=4,'c'=2] {'x','c'}, dimensions={0} | all-to-all | bytes 1835008 | tf_op jit(solution)/shard_map/all_to_all | solution.py:167
  242.6 0.8 reduce_sum.72
  (40 shorter events, 0.8 us)
Async XLA Ops:
  6.5 95.7 %copy-start.4 = (f32[2048]{0:T(1024)S(1)}, f32[2048]{0:T(1024)}, u32[]{:S(2)}) copy-start(f32[2048]{0:T(1024)} %param.16) | copy-start | bytes 24580
  6.5 95.7 %all-gather.3.cloned.1.call-start = ((), (), s32[]{:S(2)}) async-start(), calls=%async_computation.2 | async-start | bytes 5857280 | tf_op jit(solution)/shard_map/all_gather | solution.py:98
  8.1 192.0 %all-gather.5.cloned.1.call-start = ((), (), s32[]{:S(2)}) async-start(), calls=%async_computation.3 | async-start | bytes 7454720 | tf_op jit(solution)/shard_map/all_gather | solution.py:117
  103.8 2.4 copy-start.5
  103.8 2.5 %copy-start = (f32[31,192]{1,0:T(8,128)S(1)}, f32[31,192]{1,0:T(8,128)}, u32[]{:S(2)}) copy-start(f32[31,192]{1,0:T(8,128)} %param.26) | copy-start | bytes 71428
  110.9 6.1 %collective-permute-start = (bf16[15,192]{0,1:T(8,128)(2,1)S(1)}, bf16[15,192]{0,1:T(8,128)(2,1)S(1)}, u32[]{:S(2)}, u32[]{:S(2)}) collective-permute-start(bf16[15,192]{0,1:T(8,128)(2,1)S(1)} %get-tuple-element.13), channel_id=1, source_target_pairs={{0,8},{8,16},{16,24},{24,32},{32,40},{40,48},{48,56},{56,64},{64,7... | collective-permute-start | bytes 17288 | tf_op jit(solution)/shard_map/ppermute | solution.py:143
  113.5 5.0 %collective-permute-start.1 = (bf16[15,192]{0,1:T(8,128)(2,1)S(1)}, bf16[15,192]{0,1:T(8,128)(2,1)S(1)}, u32[]{:S(2)}, u32[]{:S(2)}) collective-permute-start(bf16[15,192]{0,1:T(8,128)(2,1)S(1)} %get-tuple-element.14), channel_id=1, source_target_pairs={{8,0},{16,8},{24,16},{32,24},{40,32},{48,40},{56,48},{64,56},{72,6... | collective-permute-start | bytes 17288 | tf_op jit(solution)/shard_map/ppermute | solution.py:145
  116.5 19.6 %copy-start.2 = (f32[192]{0:T(256)S(1)}, f32[192]{0:T(256)}, u32[]{:S(2)}) copy-start(f32[192]{0:T(256)} %param.27) | copy-start | bytes 2308
  121.6 14.5 %all-to-all-start = ((f32[8,1,224]{2,1,0:T(1,128)}), f32[8,1,224]{2,1,0:T(1,128)S(1)}, u32[]{:S(2)}, u32[]{:S(2)}) async-start(f32[8,1,224]{2,1,0:T(1,128)} %broadcast_in_dim.43), calls=%async_computation | async-start | bytes 16384 | tf_op jit(solution)/shard_map/all_to_all | solution.py:155
  138.0 81.0 %copy-start.1 = (f32[2]{0:T(128)S(1)}, f32[2]{0:T(128)}, u32[]{:S(2)}) copy-start(f32[2]{0:T(128)} %param.24) | copy-start | bytes 28
  217.8 1.5 copy-start.3
Sparse Core Ops, SparseCore 0:
  10.3 91.8 all-gather.2
  106.4 93.7 all-gather.4

commit v2 on v1

v2 whole, which is shorter than its diff:
```python
import functools
import math

import jax
import jax.numpy as jnp
from jax import lax
from jax.experimental import pallas as pl
from jax.experimental.pallas import tpu as pltpu
from jax.sharding import Mesh
from jax.sharding import PartitionSpec as P

HEAD_DIM = 64
WIDTH = 2 * HEAD_DIM
C_CH = 1536
CONV_W = 31
REACH = CONV_W // 2
EPS = 1e-06
LAMBDA_INIT = 0.2
BF = jnp.bfloat16
F32 = jnp.float32
TP = ("x", "c")
PLANE = ("y", "x", "c")
TOK_RING = ("z", "x", "c")


def rms_scale(values, gain):
    return values * lax.rsqrt(jnp.mean(values * values, axis=-1, keepdims=True) + EPS) * gain


def contract_last(left, right):
    return lax.dot_general(left, right, (((1,), (1,)), ((), ())), preferred_element_type=F32)


def copies_to(array, axis):
    copies = jnp.broadcast_to(array, (lax.axis_size(axis), *array.shape))
    return lax.all_to_all(copies, axis, 0, 0, tiled=True)


def diagonal(size):
    rows = lax.broadcasted_iota(jnp.int32, (size, size), 0)
    return rows == lax.broadcasted_iota(jnp.int32, (size, size), 1)


def attend_kernel(qs_ref, k0_ref, v0_ref, k1_ref, v1_ref, o_ref, acc_ref, q_ref, *, rows, keys):
    step = pl.program_id(0)

    @pl.when(step == 0)
    def _():
        acc_ref[...] = jnp.zeros_like(acc_ref)
        groups, tok, cols = qs_ref.shape
        pair = lax.broadcasted_iota(jnp.int32, (tok, WIDTH), 1) // HEAD_DIM
        at = 0
        for g in range(groups):
            for h in range(cols // WIDTH):
                q = qs_ref[g, :, h * WIDTH : (h + 1) * WIDTH].astype(F32)
                for p in range(2):
                    q_ref[at : at + tok, :] = jnp.where(pair == p, q, 0.0).astype(BF)
                    at += tok

    ones = jnp.ones((keys, WIDTH), BF)
    for k_ref, v_ref in ((k0_ref, v0_ref), (k1_ref, v1_ref)):
        for j in range(k_ref.shape[0] // keys):
            k = k_ref[j * keys : (j + 1) * keys, :]
            v = jnp.concatenate([v_ref[j * keys : (j + 1) * keys, :], ones], axis=1)
            for r in range(q_ref.shape[0] // rows):
                part = pl.ds(r * rows, rows)
                s = contract_last(q_ref[part, :], k)
                e = jnp.exp2(s).astype(BF)
                acc_ref[part, :] += jnp.dot(e, v, preferred_element_type=F32)

    @pl.when(step == pl.num_programs(0) - 1)
    def _():
        groups, padded, _ = o_ref.shape
        count = acc_ref.shape[0] // groups
        eye = diagonal(WIDTH)
        for g in range(groups):
            o_ref[g, :count, :] = acc_ref[g * count : (g + 1) * count, :WIDTH].astype(BF)
            lines = []
            for j in range(count // WIDTH):
                start = g * count + j * WIDTH
                block = acc_ref[start : start + WIDTH, WIDTH:]
                lines.append(jnp.sum(jnp.where(eye, block, 0.0), axis=0, keepdims=True))
            lines.append(jnp.zeros((8 - len(lines), WIDTH), F32))
            sums = jnp.concatenate(lines, axis=0)
            high = sums.astype(BF).astype(F32)
            both = jnp.concatenate([high, sums - high], axis=0)
            o_ref[g, count:padded, :] = both.astype(BF)


def attend(q_all, kv_own, kv_other, block, rows, keys):
    groups, tok, cols = q_all.shape
    each, total = 2 * tok * (cols // WIDTH), kv_own.shape[0]
    count = groups * each
    half = [pl.BlockSpec((block, WIDTH), lambda i, h=h: (i, h)) for h in (0, 1)]
    return pl.pallas_call(
        functools.partial(attend_kernel, rows=rows, keys=keys),
        grid=(total // block,),
        in_specs=[pl.BlockSpec(q_all.shape, lambda i: (0, 0, 0))] + half + half,
        out_specs=pl.BlockSpec((groups, each + 16, WIDTH), lambda i: (0, 0, 0)),
        out_shape=jax.ShapeDtypeStruct((groups, each + 16, WIDTH), BF),
        scratch_shapes=[pltpu.VMEM((count, 2 * WIDTH), F32), pltpu.VMEM((count, WIDTH), BF)],
        cost_estimate=pl.CostEstimate(
            flops=12 * count * total * WIDTH,
            transcendentals=2 * count * total,
            bytes_accessed=total * 8 * WIDTH + count * 4 * WIDTH,
        ),
        name="attend",
    )(q_all, kv_own, kv_own, kv_other, kv_other)


def combine_kernel(parts_ref, lam_ref, gain_ref, out_ref, ratio_ref):
    count = parts_ref.shape[1] - 16
    total = parts_ref[0].astype(F32)
    for g in range(1, parts_ref.shape[0]):
        total = total + parts_ref[g].astype(F32)
    sums = total[count : count + 8] + total[count + 8 : count + 16]
    eye = diagonal(WIDTH)
    for j in range(count // WIDTH):
        line = jnp.broadcast_to(sums[j : j + 1], (WIDTH, WIDTH))
        column = jnp.sum(jnp.where(eye, line, 0.0), axis=1, keepdims=True)
        ratio_ref[j * WIDTH : (j + 1) * WIDTH, :] = total[j * WIDTH : (j + 1) * WIDTH] / column
    tok = out_ref.shape[0]
    for h in range(out_ref.shape[1] // WIDTH):
        start = 2 * h * tok
        first = ratio_ref[start : start + tok, :]
        second = ratio_ref[start + tok : start + 2 * tok, :]
        o = first - lam_ref[h : h + 1, :] * second
        o = rms_scale(o, gain_ref[...]) * (1.0 - LAMBDA_INIT)
        out_ref[:, h * WIDTH : (h + 1) * WIDTH] = o.astype(BF)


def combine(parts, lam, gain, tok, heads):
    count = parts.shape[1] - 16
    lam_rows = jnp.broadcast_to(jnp.pad(lam, (0, 8 - heads))[:, None], (8, WIDTH))
    return pl.pallas_call(
        combine_kernel,
        out_shape=jax.ShapeDtypeStruct((tok, heads * WIDTH), BF),
        scratch_shapes=[pltpu.VMEM((count, WIDTH), F32)],
        name="combine",
    )(parts, lam_rows, gain.reshape(1, WIDTH))


def local(
    tokens,
    norm_gain,
    query_weight,
    key_weight,
    value_weight,
    glu_value_weight,
    glu_gate_weight,
    query_gain,
    key_gain,
    lambdas,
    head_gain,
    conv_weight,
    channel_gain,
    attn_out_weight,
    conv_out_weight,
):
    n = lax.axis_size("y")
    heads = query_weight.shape[1] // WIDTH
    tok = tokens.shape[0]
    seg = tok // n
    channels = conv_weight.shape[1]

    swap = [(y * n + t, t * n + y) for y in range(n) for t in range(n)]
    weights = (query_weight, key_weight, value_weight, glu_value_weight, glu_gate_weight)
    weights = weights + (attn_out_weight, conv_out_weight)
    first = sum(w.shape[1] for w in weights[:3])
    shard = lax.ppermute(jnp.concatenate(weights, axis=1), PLANE, swap)
    small = jnp.concatenate(
        [
            conv_weight,
            channel_gain[None],
            jnp.pad(lambdas, (0, channels - heads))[None],
            jnp.zeros((7, channels), F32),
        ],
        axis=0,
    )
    small = lax.ppermute(small, PLANE, swap)
    conv_weight, channel_gain = small[:CONV_W], small[CONV_W]
    lambdas = small[CONV_W + 1, :heads]

    blocks = tokens.reshape(n, seg, tokens.shape[1])
    blocks = jnp.broadcast_to(blocks, (n, *blocks.shape)).reshape(n * n, seg, -1)
    mine = lax.all_to_all(blocks, PLANE, 0, 0, tiled=True)
    mine = mine.reshape(n, n, seg, -1)
    gathered = mine.transpose(0, 2, 1, 3).reshape(n, seg, -1).astype(F32)
    normed = rms_scale(gathered, norm_gain).astype(BF).reshape(tok, -1)

    by_z = lax.all_gather(shard, "z", axis=0)
    core = lax.axis_index("c")

    def whole(columns):
        rows = columns.reshape(-1, columns.shape[-1])
        own = copies_to(rows, "x")
        other = lax.ppermute(own, "c", [(0, 1), (1, 0)])
        both = jnp.stack([jnp.where(core == 0, own, other), jnp.where(core == 0, other, own)])
        both = both.reshape(2, 4, n, shard.shape[0], -1)
        return both.transpose(2, 1, 0, 3, 4).reshape(-1, columns.shape[-1])

    w_first = whole(by_z[..., :first])

    def project(w):
        return jnp.dot(normed, w, preferred_element_type=F32)

    q_cols, k_cols = query_weight.shape[1], key_weight.shape[1]
    keys = project(w_first[:, q_cols : q_cols + k_cols]).reshape(tok, -1, HEAD_DIM)
    key_rows = rms_scale(keys, key_gain).astype(BF).reshape(tok, k_cols)
    value_rows = project(w_first[:, q_cols + k_cols :]).astype(BF)
    kv = copies_to(jnp.concatenate([key_rows, value_rows], axis=1), "z")
    kv = kv.reshape(-1, kv.shape[-1])
    kv_other = lax.ppermute(kv, "c", [(0, 1), (1, 0)])
    w_rest = whole(by_z[..., first:])

    fold = math.log2(math.e) * HEAD_DIM ** (-0.5)
    queries = project(w_first[:, :q_cols]).reshape(tok, -1, HEAD_DIM)
    q_normed = rms_scale(queries, query_gain * fold).astype(BF).reshape(tok, q_cols)
    q_all = lax.all_gather(q_normed, "x", axis=0)
    parts = attend(q_all, kv, kv_other, 256, 896, 256)
    arrived = lax.all_to_all(parts, "x", 0, 0, tiled=True)
    att = combine(arrived, lambdas, head_gain, tok, heads)

    g_cols = glu_value_weight.shape[1]
    glu_value = project(w_rest[:, :g_cols])
    glu_gate = project(w_rest[:, g_cols : 2 * g_cols])
    glu = (glu_value * jax.nn.sigmoid(glu_gate)).astype(BF).reshape(n, seg, g_cols)
    size_z = lax.axis_size("z")
    t = lax.axis_index(TP)
    heads_rows, tails = glu[:, :REACH], glu[:, seg - REACH :]
    ring = [(i, (i + 1) % n) for i in range(n)]
    left = lax.ppermute(tails, TP, ring)
    right = lax.ppermute(heads_rows, TP, [(b, a) for a, b in ring])
    across = [(z * n + n - 1, (z + 1) * n) for z in range(size_z - 1)]
    before = lax.ppermute(tails[n - 1 :], TOK_RING, across)
    after = lax.ppermute(heads_rows[:1], TOK_RING, [(b, a) for a, b in across])
    left = jnp.where(t == 0, jnp.concatenate([before, left[:-1]], axis=0), left)
    right = jnp.where(t == n - 1, jnp.concatenate([right[1:], after], axis=0), right)
    padded = jnp.concatenate([left, glu, right], axis=1)
    conv_sum = jnp.zeros((n, seg, g_cols), F32)
    for offset in range(CONV_W):
        conv_sum = conv_sum + conv_weight[offset] * padded[:, offset : offset + seg].astype(F32)
    squares = jnp.sum(conv_sum * conv_sum, axis=2)
    for bit in (1, 2, 4):
        moved = lax.ppermute(squares, "y", [(i, i ^ bit) for i in range(n)])
        squares = squares + moved
    scaled = conv_sum * lax.rsqrt(squares / C_CH + EPS)[..., None] * channel_gain
    conv_out = jax.nn.silu(scaled).astype(BF).reshape(tok, g_cols)

    w_out = w_rest[:, 2 * g_cols :]
    term = contract_last(att, w_out[:, : att.shape[1]])
    term = term + contract_last(conv_out, w_out[:, att.shape[1] :])
    term = term.astype(BF).reshape(n, seg, -1)
    reduced = lax.all_to_all(term, "y", 0, 0, tiled=True)
    return reduced.astype(F32).sum(axis=0).astype(BF)


def solution(mesh):
    finer = Mesh(mesh.devices.reshape(8, 8, 4, 2), ("z", "y", "x", "c"))
    sp = ("z", "y")
    both, rows = P(sp, TP), P()
    placed = (both, rows) + (both,) * 5 + (rows, rows, P(TP), rows, P(None, TP), P(TP), both, both)
    return jax.shard_map(
        local, mesh=finer, in_specs=placed, out_specs=P(sp + TP, None), check_vma=False
    )
```

time: 251 us -> 280 us (1.12)
  the two profiles are of different devices: /device:TPU:1 before, /device:TPU:64 now
where the time goes in v2:
time: 280 us; the launch traced here: 278 us
  starting transfers between devices  90.3 us (32%)
  blocking collectives  77.1 us (28%)
  waiting for transfers between devices  42.4 us (15%)
  local copies, waits for them, and re-layouts  26.8 us (10%)
  Pallas kernels  20.4 us (7%)
  other arithmetic  10.5 us (4%)
  matrix products  10.2 us (4%)
    all_gather x1, blocking collectives, local(): by_z = lax.all_gather(shard, 'z', axis=0)  31.5 us
    all_to_all x1, blocking collectives, local(): reduced = lax.all_to_all(term, 'y', 0, 0, tiled=True)  28.6 us
    ppermute x2, starting transfers between devices, whole(): other = lax.ppermute(own, 'c', [(0, 1), (1, 0)])  28.1 us
    all_to_all x3, waiting for transfers between devices, copies_to(): return lax.all_to_all(copies, axis, 0, 0, tiled=True)  26.6 us
    all_to_all x3, starting transfers between devices, copies_to(): return lax.all_to_all(copies, axis, 0, 0, tiled=True)  25.8 us
    pallas_call x1, Pallas kernels, attend(): pl.pallas_call(functools.partial(attend_kernel, rows=rows, keys=keys), gr...  18.2 us
    all_gather x1, blocking collectives, local(): q_all = lax.all_gather(q_normed, 'x', axis=0)  17 us
    ppermute x3, starting transfers between devices, local(): moved = lax.ppermute(squares, 'y', [(i, i ^ bit) for i in range(n)])  12 us
  transfers between devices with their start and end apart: 17, of which 6 were waited for; matrix products, arithmetic and copies ran while one was open for 13% of the time, Pallas kernels for 7%

profile of v2, /device:TPU:64, one launch (start us, length us, event | category | flops | bytes accessed | tf_op | source)
XLA Modules:
  0.0 278.2 jit_solution(6599987068476317979)
XLA Ops:
  1.6 31.5 %all-gather = bf16[256,1344]{1,0:T(8,128)(2,1)S(1)} all-gather(bf16[32,1344]{1,0:T(8,128)(2,1)S(1)} %collective-permute-done), channel_id=2, replica_groups=mesh['z'=8,'y'=8,'x'=4,'c'=2] {'z'}, dimensions={0}, use_global_device_ids=true | all-gather | bytes 774144 | tf_op jit(solution)/shard_map/all_gather | solution.py:191
  34.2 16.4 %all-to-all-start.1 = ((bf16[4,256,512]{2,1,0:T(8,128)(2,1)}), bf16[4,256,512]{2,1,0:T(8,128)(2,1)}, u32[]{:S(2)}, u32[]{:S(2)}) async-start(bf16[4,256,512]{2,1,0:T(8,128)(2,1)} %broadcast_in_dim.17), calls=%async_computation.1 | async-start | bytes 2097152 | tf_op jit(solution)/shard_map/all_to_all | solution.py:36
  50.9 10.8 %all-to-all-done.1 = bf16[4,256,512]{2,1,0:T(8,128)(2,1)} async-done(((bf16[4,256,512]{2,1,0:T(8,128)(2,1)}), bf16[4,256,512]{2,1,0:T(8,128)(2,1)}, u32[]{:S(2)}, u32[]{:S(2)}) %all-to-all-start.1) | async-done | bytes 1048608 | tf_op jit(solution)/shard_map/all_to_all | solution.py:36
  62.9 4.5 %all-to-all-start.4 = ((bf16[4,256,832]{1,2,0:T(8,128)(2,1)}), bf16[4,256,832]{1,2,0:T(8,128)(2,1)}, u32[]{:S(2)}, u32[]{:S(2)}) async-start(bf16[4,256,832]{1,2,0:T(8,128)(2,1)} %broadcast_in_dim.41), calls=%async_computation.4 | async-start | bytes 3407872 | tf_op jit(solution)/shard_map/all_to_all | solution.py:36
  67.5 14.4 %all-to-all-done.4 = bf16[4,256,832]{1,2,0:T(8,128)(2,1)} async-done(((bf16[4,256,832]{1,2,0:T(8,128)(2,1)}), bf16[4,256,832]{1,2,0:T(8,128)(2,1)}, u32[]{:S(2)}, u32[]{:S(2)}) %all-to-all-start.4) | async-done | bytes 1703968 | tf_op jit(solution)/shard_map/all_to_all | solution.py:36
  83.0 8.7 %all-to-all-start = ((bf16[64,28,256]{2,1,0:T(8,128)(2,1)}), bf16[64,28,256]{2,1,0:T(8,128)(2,1)S(1)}, u32[]{:S(2)}, u32[]{:S(2)}) async-start(bf16[64,28,256]{2,1,0:T(8,128)(2,1)} %bitcast), calls=%async_computation | async-start | bytes 2097152 | tf_op jit(solution)/shard_map/all_to_all | solution.py:186
  92.8 26.2 %collective-permute-start.1 = (bf16[4,256,512]{2,1,0:T(8,128)(2,1)}, bf16[4,256,512]{2,1,0:T(8,128)(2,1)}, u32[]{:S(2)}, u32[]{:S(2)}) collective-permute-start(bf16[4,256,512]{2,1,0:T(8,128)(2,1)} %all-to-all-done.1), channel_id=1, source_target_pairs={{0,1},{1,0},{2,3},{3,2},{4,5},{5,4},{6,7},{7,6},{8,9},{9,8},{10,11... | collective-permute-start | bytes 3145736 | tf_op jit(solution)/shard_map/ppermute | solution.py:197
  119.0 1.9 collective-permute-start.4
  120.9 2.8 %copy.101 = bf16[4,256,832]{2,1,0:T(8,128)(2,1)S(1)} copy(bf16[4,256,832]{1,2,0:T(8,128)(2,1)} %all-to-all-done.4) | data formatting | bytes 3407872 | tf_op jit(solution)/shard_map/all_to_all | solution.py:36
  126.4 2.2 reshape.166
  131.4 1.7 broadcast_select_fusion.3
  136.4 2.0 slice_bitcast_fusion.1
  144.1 4.9 %all-to-all-start.2 = ((bf16[8,224,256]{2,1,0:T(8,128)(2,1)}), bf16[8,224,256]{2,1,0:T(8,128)(2,1)}, u32[]{:S(2)}, u32[]{:S(2)}) async-start(bf16[8,224,256]{2,1,0:T(8,128)(2,1)} %broadcast_in_dim.36), calls=%async_computation.2 | async-start | bytes 1835008 | tf_op jit(solution)/shard_map/all_to_all | solution.py:36
  149.0 2.0 multiply_reduce_fusion.1
  151.0 3.5 %copy.102 = bf16[4,256,832]{2,1,0:T(8,128)(2,1)} copy(bf16[4,256,832]{1,2,0:T(8,128)(2,1)} %collective-permute-done.4) | data formatting | bytes 3407872 | tf_op jit(solution)/shard_map/ppermute | solution.py:197
  154.5 1.8 broadcast_select_fusion.1
  161.2 7.6 %collective-permute-start.8 = (bf16[1,15,192]{2,1,0:T(8,128)(2,1)S(1)}, bf16[1,15,192]{2,1,0:T(8,128)(2,1)S(1)}, u32[]{:S(2)}, u32[]{:S(2)}) collective-permute-start(bf16[1,15,192]{2,1,0:T(8,128)(2,1)S(1)} %get-tuple-element.12), channel_id=1, source_target_pairs={{64,7},{128,71},{192,135},{256,199},{320,263},{384,327},{448,391},... | collective-permute-start | bytes 17288 | tf_op jit(solution)/shard_map/ppermute | solution.py:236
  168.9 4.1 %collective-permute-done.5 = bf16[1,15,192]{2,1,0:T(8,128)(2,1)S(1)} collective-permute-done((bf16[1,15,192]{2,1,0:T(8,128)(2,1)S(1)}, bf16[1,15,192]{2,1,0:T(8,128)(2,1)S(1)}, u32[]{:S(2)}, u32[]{:S(2)}) %collective-permute-start.5) | collective-permute-done | bytes 5792 | tf_op jit(solution)/shard_map/ppermute | solution.py:235
  174.5 1.9 collective-permute-start.2
  176.5 1.7 multiply_reduce_fusion
  178.2 1.9 collective-permute-start.9
  180.3 3.4 %collective-permute-done.9 = f32[8,28]{1,0:T(8,128)S(1)} collective-permute-done((f32[8,28]{1,0:T(8,128)S(1)}, f32[8,28]{1,0:T(8,128)S(1)}, u32[]{:S(2)}, u32[]{:S(2)}) %collective-permute-start.9) | collective-permute-done | bytes 928 | tf_op jit(solution)/shard_map/ppermute | solution.py:245
  183.7 6.0 %collective-permute-start.10 = (f32[8,28]{1,0:T(8,128)S(1)}, f32[8,28]{1,0:T(8,128)S(1)}, u32[]{:S(2)}, u32[]{:S(2)}) collective-permute-start(f32[8,28]{1,0:T(8,128)S(1)} %add.193), channel_id=1, source_target_pairs={{0,16},{8,24},{16,0},{24,8},{32,48},{40,56},{48,32},{56,40},{1,17}... | collective-permute-start | bytes 2696 | tf_op jit(solution)/shard_map/ppermute | solution.py:245
  189.7 17.0 %all_gather.11.qs_ref = bf16[4,224,256]{2,1,0:T(8,128)(2,1)} all-gather(bf16[1,224,256]{2,1,0:T(8,128)(2,1)S(1)} %copy.96), channel_id=1, replica_groups=mesh['z'=8,'y'=8,'x'=4,'c'=2] {'x'}, dimensions={0}, use_global_device_ids=true | all-gather | bytes 573440 | tf_op jit(solution)/shard_map/all_gather | solution.py:219
  206.7 4.1 %collective-permute-start.11 = (f32[8,28]{1,0:T(8,128)S(1)}, f32[8,28]{1,0:T(8,128)S(1)}, u32[]{:S(2)}, u32[]{:S(2)}) collective-permute-start(f32[8,28]{1,0:T(8,128)S(1)} %add.194), channel_id=1, source_target_pairs={{0,32},{8,40},{16,48},{24,56},{32,0},{40,8},{48,16},{56,24},{1,33}... | collective-permute-start | bytes 2696 | tf_op jit(solution)/shard_map/ppermute | solution.py:245
  211.7 18.2 %attend.1 = bf16[4,912,128]{2,1,0:T(8,128)(2,1)} custom-call(bf16[4,224,256]{2,1,0:T(8,128)(2,1)} %all_gather.11.qs_ref, bf16[1792,256]{1,0:T(8,128)(2,1)} %bitcast.17.k0_ref.v0_ref, bf16[1792,256]{1,0:T(8,128)(2,1)} %bitcast.17.k0_ref.v0_ref, bf16[1792,256]{1,0:T(8,128)(2,1)} %copy-done.10, bf16[1792,256]{1,0:T(8,128)(2,1)} %copy-done.10), custom_call_target="tpu_custom_call" | custom-call | flops 9865003008 | bytes 3670016 | tf_op jit(solution)/shard_map/attend/pallas_call | solution.py:95
  230.0 3.5 %all-to-all-start.3 = ((bf16[4,912,128]{2,1,0:T(8,128)(2,1)}), bf16[4,912,128]{2,1,0:T(8,128)(2,1)S(1)}, u32[]{:S(2)}, u32[]{:S(2)}) async-start(bf16[4,912,128]{2,1,0:T(8,128)(2,1)} %attend.1), calls=%async_computation.3 | async-start | bytes 1867776 | tf_op jit(solution)/shard_map/all_to_all | solution.py:221
  233.7 1.7 fusion.8
  235.4 8.3 %all-to-all-done.3.parts_ref = bf16[4,912,128]{2,1,0:T(8,128)(2,1)S(1)} async-done(((bf16[4,912,128]{2,1,0:T(8,128)(2,1)}), bf16[4,912,128]{2,1,0:T(8,128)(2,1)S(1)}, u32[]{:S(2)}, u32[]{:S(2)}) %all-to-all-start.3) | async-done | bytes 933920 | tf_op jit(solution)/shard_map/all_to_all | solution.py:221
  244.7 2.1 combine.1
  246.8 1.8 fusion
  248.8 28.6 %all_to_all.30 = bf16[8,28,2048]{2,1,0:T(8,128)(2,1)S(1)} all-to-all(bf16[8,28,2048]{2,1,0:T(8,128)(2,1)S(1)} %reshape.161), channel_id=1, replica_groups=mesh['z'=8,'y'=8,'x'=4,'c'=2] {'y'}, dimensions={0} | all-to-all | bytes 1835008 | tf_op jit(solution)/shard_map/all_to_all | solution.py:254
  (105 shorter events, 30.2 us)
Async XLA Ops:
  0.9 0.7 collective-permute-start
  34.2 27.4 %all-to-all-start.1 = ((bf16[4,256,512]{2,1,0:T(8,128)(2,1)}), bf16[4,256,512]{2,1,0:T(8,128)(2,1)}, u32[]{:S(2)}, u32[]{:S(2)}) async-start(bf16[4,256,512]{2,1,0:T(8,128)(2,1)} %broadcast_in_dim.17), calls=%async_computation.1 | async-start | bytes 2097152 | tf_op jit(solution)/shard_map/all_to_all | solution.py:36
  62.9 4.5 %copy-start.4 = (bf16[224,256]{1,0:T(8,128)(2,1)S(1)}, bf16[224,256]{1,0:T(8,128)(2,1)}, u32[]{:S(2)}) copy-start(bf16[224,256]{1,0:T(8,128)(2,1)} %param.15) | copy-start | bytes 344068
  62.9 19.0 %all-to-all-start.4 = ((bf16[4,256,832]{1,2,0:T(8,128)(2,1)}), bf16[4,256,832]{1,2,0:T(8,128)(2,1)}, u32[]{:S(2)}, u32[]{:S(2)}) async-start(bf16[4,256,832]{1,2,0:T(8,128)(2,1)} %broadcast_in_dim.41), calls=%async_computation.4 | async-start | bytes 3407872 | tf_op jit(solution)/shard_map/all_to_all | solution.py:36
  67.5 24.3 %copy-start.9 = (f32[2]{0:T(128)S(1)}, f32[2]{0:T(128)}, u32[]{:S(2)}) copy-start(f32[2]{0:T(128)} %param.24) | copy-start | bytes 28
  67.5 24.4 %copy-start.6 = (f32[31,192]{1,0:T(8,128)S(1)}, f32[31,192]{1,0:T(8,128)}, u32[]{:S(2)}) copy-start(f32[31,192]{1,0:T(8,128)} %param.26) | copy-start | bytes 71428
  67.5 24.4 %copy-start.7 = (f32[192]{0:T(256)S(1)}, f32[192]{0:T(256)}, u32[]{:S(2)}) copy-start(f32[192]{0:T(256)} %param.27) | copy-start | bytes 2308
  67.5 25.1 %copy-start.11 = (f32[64]{0:T(128)S(1)}, f32[64]{0:T(128)}, u32[]{:S(2)}) copy-start(f32[64]{0:T(128)} %param.22) | copy-start | bytes 772
  67.5 25.2 %copy-start.5 = (f32[2048]{0:T(1024)S(1)}, f32[2048]{0:T(1024)}, u32[]{:S(2)}) copy-start(f32[2048]{0:T(1024)} %param.16) | copy-start | bytes 24580
  83.0 40.7 %all-to-all-start = ((bf16[64,28,256]{2,1,0:T(8,128)(2,1)}), bf16[64,28,256]{2,1,0:T(8,128)(2,1)S(1)}, u32[]{:S(2)}, u32[]{:S(2)}) async-start(bf16[64,28,256]{2,1,0:T(8,128)(2,1)} %bitcast), calls=%async_computation | async-start | bytes 2097152 | tf_op jit(solution)/shard_map/all_to_all | solution.py:186
  92.0 0.7 collective-permute-start.3
  92.8 38.6 %collective-permute-start.1 = (bf16[4,256,512]{2,1,0:T(8,128)(2,1)}, bf16[4,256,512]{2,1,0:T(8,128)(2,1)}, u32[]{:S(2)}, u32[]{:S(2)}) collective-permute-start(bf16[4,256,512]{2,1,0:T(8,128)(2,1)} %all-to-all-done.1), channel_id=1, source_target_pairs={{0,1},{1,0},{2,3},{3,2},{4,5},{5,4},{6,7},{7,6},{8,9},{9,8},{10,11... | collective-permute-start | bytes 3145736 | tf_op jit(solution)/shard_map/ppermute | solution.py:197
  119.0 32.0 %collective-permute-start.4 = (bf16[4,256,832]{1,2,0:T(8,128)(2,1)}, bf16[4,256,832]{1,2,0:T(8,128)(2,1)}, u32[]{:S(2)}, u32[]{:S(2)}) collective-permute-start(bf16[4,256,832]{1,2,0:T(8,128)(2,1)} %all-to-all-done.4), channel_id=1, source_target_pairs={{0,1},{1,0},{2,3},{3,2},{4,5},{5,4},{6,7},{7,6},{8,9},{9,8},{10,11... | collective-permute-start | bytes 5111816 | tf_op jit(solution)/shard_map/ppermute | solution.py:197
  133.5 1.4 copy-start.1
  136.4 4.9 %copy-start.8 = (f32[64]{0:T(128)S(1)}, f32[64]{0:T(128)}, u32[]{:S(2)}) copy-start(f32[64]{0:T(128)} %param.23) | copy-start | bytes 772
  136.4 5.1 %copy-start.3 = (bf16[224,2048]{1,0:T(8,128)(2,1)S(1)}, bf16[224,2048]{1,0:T(8,128)(2,1)}, u32[]{:S(2)}) copy-start(bf16[224,2048]{1,0:T(8,128)(2,1)} %multiply_convert_fusion) | copy-start | bytes 2752516
  144.1 30.4 %all-to-all-start.2 = ((bf16[8,224,256]{2,1,0:T(8,128)(2,1)}), bf16[8,224,256]{2,1,0:T(8,128)(2,1)}, u32[]{:S(2)}, u32[]{:S(2)}) async-start(bf16[8,224,256]{2,1,0:T(8,128)(2,1)} %broadcast_in_dim.36), calls=%async_computation.2 | async-start | bytes 1835008 | tf_op jit(solution)/shard_map/all_to_all | solution.py:36
  157.4 1.8 copy-start
  159.9 13.1 %collective-permute-start.5 = (bf16[1,15,192]{2,1,0:T(8,128)(2,1)S(1)}, bf16[1,15,192]{2,1,0:T(8,128)(2,1)S(1)}, u32[]{:S(2)}, u32[]{:S(2)}) collective-permute-start(bf16[1,15,192]{2,1,0:T(8,128)(2,1)S(1)} %get-tuple-element.11), channel_id=1, source_target_pairs={{7,64},{71,128},{135,192},{199,256},{263,320},{327,384},{391,448},... | collective-permute-start | bytes 17288 | tf_op jit(solution)/shard_map/ppermute | solution.py:235
  161.2 7.7 %collective-permute-start.6 = (bf16[8,15,192]{2,1,0:T(8,128)(2,1)S(1)}, bf16[8,15,192]{2,1,0:T(8,128)(2,1)S(1)}, u32[]{:S(2)}, u32[]{:S(2)}) collective-permute-start(bf16[8,15,192]{2,1,0:T(8,128)(2,1)S(1)} %get-tuple-element.13), channel_id=1, source_target_pairs={{0,1},{1,2},{2,3},{3,4},{4,5},{5,6},{6,7},{7,0},{8,9},{9,10},{10,1... | collective-permute-start | bytes 138248 | tf_op jit(solution)/shard_map/ppermute | solution.py:232
  161.2 15.2 %collective-permute-start.8 = (bf16[1,15,192]{2,1,0:T(8,128)(2,1)S(1)}, bf16[1,15,192]{2,1,0:T(8,128)(2,1)S(1)}, u32[]{:S(2)}, u32[]{:S(2)}) collective-permute-start(bf16[1,15,192]{2,1,0:T(8,128)(2,1)S(1)} %get-tuple-element.12), channel_id=1, source_target_pairs={{64,7},{128,71},{192,135},{256,199},{320,263},{384,327},{448,391},... | collective-permute-start | bytes 17288 | tf_op jit(solution)/shard_map/ppermute | solution.py:236
  168.9 4.1 %collective-permute-start.7 = (bf16[8,15,192]{2,1,0:T(8,128)(2,1)S(1)}, bf16[8,15,192]{2,1,0:T(8,128)(2,1)S(1)}, u32[]{:S(2)}, u32[]{:S(2)}) collective-permute-start(bf16[8,15,192]{2,1,0:T(8,128)(2,1)S(1)} %get-tuple-element.14), channel_id=1, source_target_pairs={{1,0},{2,1},{3,2},{4,3},{5,4},{6,5},{7,6},{0,7},{9,8},{10,9},{11,1... | collective-permute-start | bytes 138248 | tf_op jit(solution)/shard_map/ppermute | solution.py:233
  174.5 36.3 %collective-permute-start.2 = (bf16[1792,256]{1,0:T(8,128)(2,1)}, bf16[1792,256]{1,0:T(8,128)(2,1)S(1)}, u32[]{:S(2)}, u32[]{:S(2)}) collective-permute-start(bf16[1792,256]{1,0:T(8,128)(2,1)} %bitcast.17.k0_ref.v0_ref), channel_id=1, source_target_pairs={{0,1},{1,0},{2,3},{3,2},{4,5},{5,4},{6,7},{7,6},{8,9},{9,8},{10,11... | collective-permute-start | bytes 2752520 | tf_op jit(solution)/shard_map/ppermute | solution.py:213
  178.2 5.5 %collective-permute-start.9 = (f32[8,28]{1,0:T(8,128)S(1)}, f32[8,28]{1,0:T(8,128)S(1)}, u32[]{:S(2)}, u32[]{:S(2)}) collective-permute-start(f32[8,28]{1,0:T(8,128)S(1)} %get-tuple-element.5), channel_id=1, source_target_pairs={{0,8},{8,0},{16,24},{24,16},{32,40},{40,32},{48,56},{56,48},{1,9},... | collective-permute-start | bytes 2696 | tf_op jit(solution)/shard_map/ppermute | solution.py:245
  183.7 23.0 %collective-permute-start.10 = (f32[8,28]{1,0:T(8,128)S(1)}, f32[8,28]{1,0:T(8,128)S(1)}, u32[]{:S(2)}, u32[]{:S(2)}) collective-permute-start(f32[8,28]{1,0:T(8,128)S(1)} %add.193), channel_id=1, source_target_pairs={{0,16},{8,24},{16,0},{24,8},{32,48},{40,56},{48,32},{56,40},{1,17}... | collective-permute-start | bytes 2696 | tf_op jit(solution)/shard_map/ppermute | solution.py:245
  206.7 26.8 %collective-permute-start.11 = (f32[8,28]{1,0:T(8,128)S(1)}, f32[8,28]{1,0:T(8,128)S(1)}, u32[]{:S(2)}, u32[]{:S(2)}) collective-permute-start(f32[8,28]{1,0:T(8,128)S(1)} %add.194), channel_id=1, source_target_pairs={{0,32},{8,40},{16,48},{24,56},{32,0},{40,8},{48,16},{56,24},{1,33}... | collective-permute-start | bytes 2696 | tf_op jit(solution)/shard_map/ppermute | solution.py:245
  210.8 1.0 copy-start.10
  230.0 13.8 %all-to-all-start.3 = ((bf16[4,912,128]{2,1,0:T(8,128)(2,1)}), bf16[4,912,128]{2,1,0:T(8,128)(2,1)S(1)}, u32[]{:S(2)}, u32[]{:S(2)}) async-start(bf16[4,912,128]{2,1,0:T(8,128)(2,1)} %attend.1), calls=%async_computation.3 | async-start | bytes 1867776 | tf_op jit(solution)/shard_map/all_to_all | solution.py:221
  243.7 0.9 copy-start.2

commit v3 on v2

--- a/solution.py
+++ b/solution.py
@@ -41,18 +41,20 @@
     return rows == lax.broadcasted_iota(jnp.int32, (size, size), 1)
 
 
-def attend_kernel(qs_ref, k0_ref, v0_ref, k1_ref, v1_ref, o_ref, acc_ref, q_ref, *, rows, keys):
+def attend_kernel(
+    qs_ref, k0_ref, v0_ref, k1_ref, v1_ref, o_ref, acc_ref, q_ref, *, tok, rows, keys
+):
     step = pl.program_id(0)
 
     @pl.when(step == 0)
     def _():
         acc_ref[...] = jnp.zeros_like(acc_ref)
-        groups, tok, cols = qs_ref.shape
+        groups = qs_ref.shape[0]
         pair = lax.broadcasted_iota(jnp.int32, (tok, WIDTH), 1) // HEAD_DIM
         at = 0
         for g in range(groups):
-            for h in range(cols // WIDTH):
-                q = qs_ref[g, :, h * WIDTH : (h + 1) * WIDTH].astype(F32)
+            for h in range(qs_ref.shape[2] // WIDTH):
+                q = qs_ref[g, :tok, h * WIDTH : (h + 1) * WIDTH].astype(F32)
                 for p in range(2):
                     q_ref[at : at + tok, :] = jnp.where(pair == p, q, 0.0).astype(BF)
                     at += tok
@@ -87,15 +89,15 @@
             o_ref[g, count:padded, :] = both.astype(BF)
 
 
-def attend(q_all, kv_own, kv_other, block, rows, keys):
-    groups, tok, cols = q_all.shape
+def attend(packed, tok, cols, kv_own, kv_other, block, rows, keys):
+    groups = packed.shape[0]
     each, total = 2 * tok * (cols // WIDTH), kv_own.shape[0]
     count = groups * each
     half = [pl.BlockSpec((block, WIDTH), lambda i, h=h: (i, h)) for h in (0, 1)]
     return pl.pallas_call(
-        functools.partial(attend_kernel, rows=rows, keys=keys),
+        functools.partial(attend_kernel, tok=tok, rows=rows, keys=keys),
         grid=(total // block,),
-        in_specs=[pl.BlockSpec(q_all.shape, lambda i: (0, 0, 0))] + half + half,
+        in_specs=[pl.BlockSpec((groups, packed.shape[1], cols), lambda i: (0, 0, 0))] + half + half,
         out_specs=pl.BlockSpec((groups, each + 16, WIDTH), lambda i: (0, 0, 0)),
         out_shape=jax.ShapeDtypeStruct((groups, each + 16, WIDTH), BF),
         scratch_shapes=[pltpu.VMEM((count, 2 * WIDTH), F32), pltpu.VMEM((count, WIDTH), BF)],
@@ -105,7 +107,7 @@
             bytes_accessed=total * 8 * WIDTH + count * 4 * WIDTH,
         ),
         name="attend",
-    )(q_all, kv_own, kv_own, kv_other, kv_other)
+    )(packed, kv_own, kv_own, kv_other, kv_other)
 
 
 def combine_kernel(parts_ref, lam_ref, gain_ref, out_ref, ratio_ref):
@@ -138,6 +140,106 @@
         scratch_shapes=[pltpu.VMEM((count, WIDTH), F32)],
         name="combine",
     )(parts, lam_rows, gain.reshape(1, WIDTH))
+
+
+def natural_rows(core, own_ref, other_ref, z, cols):
+    blocks = []
+    for x in range(own_ref.shape[0]):
+        own = own_ref[x, 32 * z : 32 * z + 32, cols]
+        other = other_ref[x, 32 * z : 32 * z + 32, cols]
+        blocks.append(jnp.where(core == 0, own, other))
+        blocks.append(jnp.where(core == 0, other, own))
+    return jnp.concatenate(blocks, axis=0)
+
+
+def project(core, x_ref, own_ref, other_ref, cols):
+    acc = None
+    for z in range(own_ref.shape[1] // 32):
+        rhs = natural_rows(core, own_ref, other_ref, z, cols)
+        part = jnp.dot(x_ref[:, 256 * z : 256 * z + 256], rhs, preferred_element_type=F32)
+        acc = part if acc is None else acc + part
+    return acc
+
+
+def qkv_kernel(core_ref, x_ref, own_ref, other_ref, qg_ref, kg_ref, q_ref, kv_ref):
+    acc = project(core_ref[0], x_ref, own_ref, other_ref, slice(0, own_ref.shape[2]))
+    low = lax.broadcasted_iota(jnp.int32, (x_ref.shape[0], WIDTH), 1) < HEAD_DIM
+
+    def normed(block, gain):
+        squares = block * block
+        first = jnp.sum(jnp.where(low, squares, 0.0), axis=1, keepdims=True)
+        second = jnp.sum(jnp.where(low, 0.0, squares), axis=1, keepdims=True)
+        first = lax.rsqrt(first / HEAD_DIM + EPS)
+        second = lax.rsqrt(second / HEAD_DIM + EPS)
+        return (block * jnp.where(low, first, second) * gain).astype(BF)
+
+    q_cols = q_ref.shape[1]
+    for at in range(0, q_cols, WIDTH):
+        q_ref[:, at : at + WIDTH] = normed(acc[:, at : at + WIDTH], qg_ref[...])
+    kv_ref[:, :WIDTH] = normed(acc[:, q_cols : q_cols + WIDTH], kg_ref[...])
+    kv_ref[:, WIDTH:] = acc[:, q_cols + WIDTH :].astype(BF)
+
+
+SMEM = pl.BlockSpec(memory_space=pltpu.SMEM)
+VMEM = pl.BlockSpec(memory_space=pltpu.VMEM)
+
+
+def qkv(core, x, own, other, query_gain, key_gain):
+    tok, q_cols = x.shape[0], own.shape[2] - 2 * WIDTH
+    return pl.pallas_call(
+        qkv_kernel,
+        in_specs=[SMEM] + [VMEM] * 5,
+        out_specs=[VMEM, VMEM],
+        out_shape=[
+            jax.ShapeDtypeStruct((tok, q_cols), BF),
+            jax.ShapeDtypeStruct((tok, 2 * WIDTH), BF),
+        ],
+        name="qkv",
+    )(core, x, own, other, jnp.tile(query_gain, 2)[None], jnp.tile(key_gain, 2)[None])
+
+
+def glu_kernel(core_ref, x_ref, own_ref, other_ref, out_ref, *, start):
+    channels = out_ref.shape[2]
+    cols = slice(start, start + 2 * channels)
+    acc = project(core_ref[0], x_ref, own_ref, other_ref, cols)
+    value, gate = acc[:, :channels], acc[:, channels:]
+    glu = value * (1.0 / (1.0 + jnp.exp(-gate)))
+    seg = out_ref.shape[1]
+    for y in range(out_ref.shape[0]):
+        out_ref[y] = glu[seg * y : seg * y + seg].astype(BF)
+
+
+def glu_of(core, x, own, other, start, channels, n):
+    return pl.pallas_call(
+        functools.partial(glu_kernel, start=start),
+        in_specs=[SMEM] + [VMEM] * 3,
+        out_specs=VMEM,
+        out_shape=jax.ShapeDtypeStruct((n, x.shape[0] // n, channels), BF),
+        name="glu",
+    )(core, x, own, other)
+
+
+def out_kernel(core_ref, att_ref, conv_ref, own_ref, other_ref, out_ref, *, start):
+    cols = slice(start, own_ref.shape[2])
+    act = jnp.concatenate([att_ref[...], conv_ref[...]], axis=1)
+    seg = out_ref.shape[1]
+    for z in range(own_ref.shape[1] // 32):
+        rhs = natural_rows(core_ref[0], own_ref, other_ref, z, cols)
+        term = contract_last(act, rhs)
+        for y in range(out_ref.shape[0]):
+            block = term[seg * y : seg * y + seg]
+            out_ref[y, :, 256 * z : 256 * z + 256] = block.astype(BF)
+
+
+def out_of(core, att, conv, own, other, start, n):
+    width = own.shape[0] * own.shape[1] * 2
+    return pl.pallas_call(
+        functools.partial(out_kernel, start=start),
+        in_specs=[SMEM] + [VMEM] * 4,
+        out_specs=VMEM,
+        out_shape=jax.ShapeDtypeStruct((n, att.shape[0] // n, width), BF),
+        name="out",
+    )(core, att, conv, own, other)
 
 
 def local(
@@ -189,42 +291,28 @@
     normed = rms_scale(gathered, norm_gain).astype(BF).reshape(tok, -1)
 
     by_z = lax.all_gather(shard, "z", axis=0)
-    core = lax.axis_index("c")
-
-    def whole(columns):
-        rows = columns.reshape(-1, columns.shape[-1])
-        own = copies_to(rows, "x")
-        other = lax.ppermute(own, "c", [(0, 1), (1, 0)])
-        both = jnp.stack([jnp.where(core == 0, own, other), jnp.where(core == 0, other, own)])
-        both = both.reshape(2, 4, n, shard.shape[0], -1)
-        return both.transpose(2, 1, 0, 3, 4).reshape(-1, columns.shape[-1])
-
-    w_first = whole(by_z[..., :first])
-
-    def project(w):
-        return jnp.dot(normed, w, preferred_element_type=F32)
-
-    q_cols, k_cols = query_weight.shape[1], key_weight.shape[1]
-    keys = project(w_first[:, q_cols : q_cols + k_cols]).reshape(tok, -1, HEAD_DIM)
-    key_rows = rms_scale(keys, key_gain).astype(BF).reshape(tok, k_cols)
-    value_rows = project(w_first[:, q_cols + k_cols :]).astype(BF)
-    kv = copies_to(jnp.concatenate([key_rows, value_rows], axis=1), "z")
-    kv = kv.reshape(-1, kv.shape[-1])
-    kv_other = lax.ppermute(kv, "c", [(0, 1), (1, 0)])
-    w_rest = whole(by_z[..., first:])
-
+    core = lax.axis_index("c").astype(jnp.int32)[None]
+    mates = [(0, 1), (1, 0)]
+    by_z = by_z.reshape(-1, by_z.shape[2])
+    wa = copies_to(by_z[:, :first], "x")
+    wa_other = lax.ppermute(wa, "c", mates)
     fold = math.log2(math.e) * HEAD_DIM ** (-0.5)
-    queries = project(w_first[:, :q_cols]).reshape(tok, -1, HEAD_DIM)
-    q_normed = rms_scale(queries, query_gain * fold).astype(BF).reshape(tok, q_cols)
-    q_all = lax.all_gather(q_normed, "x", axis=0)
-    parts = attend(q_all, kv, kv_other, 256, 896, 256)
+    q, kv = qkv(core, normed, wa, wa_other, query_gain * fold, key_gain)
+
+    q_cols = q.shape[1]
+    rest = jnp.concatenate(
+        [jnp.pad(q, ((0, by_z.shape[0] - tok), (0, 0))), by_z[:, first:]], axis=1
+    )
+    rest = copies_to(rest, "x")
+    kv = lax.all_gather(kv, "z", axis=0, tiled=True)
+    kv_other = lax.ppermute(kv, "c", mates)
+    rest_other = lax.ppermute(rest, "c", mates)
+    parts = attend(rest, tok, q_cols, kv, kv_other, 256, 896, 256)
     arrived = lax.all_to_all(parts, "x", 0, 0, tiled=True)
     att = combine(arrived, lambdas, head_gain, tok, heads)
 
     g_cols = glu_value_weight.shape[1]
-    glu_value = project(w_rest[:, :g_cols])
-    glu_gate = project(w_rest[:, g_cols : 2 * g_cols])
-    glu = (glu_value * jax.nn.sigmoid(glu_gate)).astype(BF).reshape(n, seg, g_cols)
+    glu = glu_of(core, normed, rest, rest_other, q_cols, g_cols, n)
     size_z = lax.axis_size("z")
     t = lax.axis_index(TP)
     heads_rows, tails = glu[:, :REACH], glu[:, seg - REACH :]
@@ -232,25 +320,22 @@
     left = lax.ppermute(tails, TP, ring)
     right = lax.ppermute(heads_rows, TP, [(b, a) for a, b in ring])
     across = [(z * n + n - 1, (z + 1) * n) for z in range(size_z - 1)]
-    before = lax.ppermute(tails[n - 1 :], TOK_RING, across)
-    after = lax.ppermute(heads_rows[:1], TOK_RING, [(b, a) for a, b in across])
-    left = jnp.where(t == 0, jnp.concatenate([before, left[:-1]], axis=0), left)
-    right = jnp.where(t == n - 1, jnp.concatenate([right[1:], after], axis=0), right)
+    across = [(z * n + n - 1, (z + 1) * n) for z in range(size_z - 1)]
+    across = across + [(b, a) for a, b in across]
+    edge = jnp.where(t == 0, heads_rows[:1], tails[n - 1 :])
+    edge = lax.ppermute(edge, TOK_RING, across)
+    left = jnp.where(t == 0, jnp.concatenate([edge, left[:-1]], axis=0), left)
+    right = jnp.where(t == n - 1, jnp.concatenate([right[1:], edge], axis=0), right)
     padded = jnp.concatenate([left, glu, right], axis=1)
     conv_sum = jnp.zeros((n, seg, g_cols), F32)
     for offset in range(CONV_W):
         conv_sum = conv_sum + conv_weight[offset] * padded[:, offset : offset + seg].astype(F32)
     squares = jnp.sum(conv_sum * conv_sum, axis=2)
-    for bit in (1, 2, 4):
-        moved = lax.ppermute(squares, "y", [(i, i ^ bit) for i in range(n)])
-        squares = squares + moved
+    squares = jnp.sum(copies_to(squares, "y"), axis=0)
     scaled = conv_sum * lax.rsqrt(squares / C_CH + EPS)[..., None] * channel_gain
     conv_out = jax.nn.silu(scaled).astype(BF).reshape(tok, g_cols)
 
-    w_out = w_rest[:, 2 * g_cols :]
-    term = contract_last(att, w_out[:, : att.shape[1]])
-    term = term + contract_last(conv_out, w_out[:, att.shape[1] :])
-    term = term.astype(BF).reshape(n, seg, -1)
+    term = out_of(core, att, conv_out, rest, rest_other, q_cols + 2 * g_cols, n)
     reduced = lax.all_to_all(term, "y", 0, 0, tiled=True)
     return reduced.astype(F32).sum(axis=0).astype(BF)
 

time: 280 us -> 281 us (level)
  the two profiles are of different devices: /device:TPU:64 before, /device:TPU:1 now
where the time goes in v3:
time: 281 us; the launch traced here: 277 us
  blocking collectives  106 us (38%)
  starting transfers between devices  64.5 us (23%)
  waiting for transfers between devices  46.4 us (17%)
  Pallas kernels  32.2 us (11%)
  local copies, waits for them, and re-layouts  16.5 us (6%)
  other arithmetic  10.9 us (4%)
    all_to_all x1, blocking collectives, local(): reduced = lax.all_to_all(term, 'y', 0, 0, tiled=True)  28.9 us
    all_to_all x1, blocking collectives, copies_to(): return lax.all_to_all(copies, axis, 0, 0, tiled=True)  28.8 us
    all_gather x1, blocking collectives, local(): by_z = lax.all_gather(shard, 'z', axis=0)  26.9 us
    all_to_all x1, waiting for transfers between devices, local(): mine = lax.all_to_all(blocks, PLANE, 0, 0, tiled=True)  24.5 us
    all_gather x1, blocking collectives, local(): kv = lax.all_gather(kv, 'z', axis=0, tiled=True)  21.3 us
    pallas_call x1, Pallas kernels, attend(): pl.pallas_call(functools.partial(attend_kernel, tok=tok, rows=rows, keys=...  18.2 us
    all_to_all x1, starting transfers between devices, local(): mine = lax.all_to_all(blocks, PLANE, 0, 0, tiled=True)  17.3 us
    all_to_all x2, starting transfers between devices, copies_to(): return lax.all_to_all(copies, axis, 0, 0, tiled=True)  13.8 us
  transfers between devices with their start and end apart: 12, of which 7 were waited for; matrix products, arithmetic and copies ran while one was open for 7% of the time, Pallas kernels for 9%

profile of v3, /device:TPU:1, one launch (start us, length us, event | category | flops | bytes accessed | tf_op | source)
XLA Modules:
  0.0 276.7 jit_solution(13944236663131695980)
XLA Ops:
  0.9 4.6 %collective-permute-start = (bf16[32,1344]{1,0:T(8,128)(2,1)S(1)}, bf16[32,1344]{1,0:T(8,128)(2,1)S(1)}, u32[]{:S(2)}, u32[]{:S(2)}) collective-permute-start(bf16[32,1344]{1,0:T(8,128)(2,1)S(1)} %concatenate.50), channel_id=1, source_target_pairs={{0,0},{1,8},{2,16},{3,24},{4,32},{5,40},{6,48},{7,56},{8,1},{9,9},... | collective-permute-start | bytes 258056 | tf_op jit(solution)/shard_map/ppermute | solution.py:272
  5.5 2.2 collective-permute-done
  7.7 26.9 %all-gather = bf16[256,1344]{1,0:T(8,128)(2,1)S(1)} all-gather(bf16[32,1344]{1,0:T(8,128)(2,1)S(1)} %collective-permute-done), channel_id=2, replica_groups=mesh['z'=8,'y'=8,'x'=4,'c'=2] {'z'}, dimensions={0}, use_global_device_ids=true | all-gather | bytes 774144 | tf_op jit(solution)/shard_map/all_gather | solution.py:293
  34.6 1.1 broadcast_in_dim.35
  35.7 9.7 %all-to-all-start.1 = ((bf16[4,256,512]{2,1,0:T(8,128)(2,1)}), bf16[4,256,512]{2,1,0:T(8,128)(2,1)}, u32[]{:S(2)}, u32[]{:S(2)}) async-start(bf16[4,256,512]{2,1,0:T(8,128)(2,1)} %broadcast_in_dim.35), calls=%async_computation.1 | async-start | bytes 2097152 | tf_op jit(solution)/shard_map/all_to_all | solution.py:36
  45.5 9.8 %all-to-all-done.1.own_ref = bf16[4,256,512]{2,1,0:T(8,128)(2,1)} async-done(((bf16[4,256,512]{2,1,0:T(8,128)(2,1)}), bf16[4,256,512]{2,1,0:T(8,128)(2,1)}, u32[]{:S(2)}, u32[]{:S(2)}) %all-to-all-start.1) | async-done | bytes 1048608 | tf_op jit(solution)/shard_map/all_to_all | solution.py:36
  55.3 1.1 broadcast_in_dim.34
  56.4 17.3 %all-to-all-start = ((bf16[64,28,256]{2,1,0:T(8,128)(2,1)}), bf16[64,28,256]{2,1,0:T(8,128)(2,1)S(1)}, u32[]{:S(2)}, u32[]{:S(2)}) async-start(bf16[64,28,256]{2,1,0:T(8,128)(2,1)} %bitcast.1), calls=%async_computation | async-start | bytes 2097152 | tf_op jit(solution)/shard_map/all_to_all | solution.py:288
  75.0 2.4 collective-permute-start.1
  77.3 24.5 %all-to-all-done = bf16[64,28,256]{2,1,0:T(8,128)(2,1)S(1)} async-done(((bf16[64,28,256]{2,1,0:T(8,128)(2,1)}), bf16[64,28,256]{2,1,0:T(8,128)(2,1)S(1)}, u32[]{:S(2)}, u32[]{:S(2)}) %all-to-all-start) | async-done | bytes 917536 | tf_op jit(solution)/shard_map/all_to_all | solution.py:288
  104.1 1.2 multiply_convert_fusion.x_ref
  105.3 3.4 %qkv.1 = (bf16[224,256]{1,0:T(8,128)(2,1)}, bf16[224,256]{1,0:T(8,128)(2,1)}) custom-call(s32[1]{0:T(128)} %bitcast.core_ref, bf16[224,2048]{1,0:T(8,128)(2,1)} %multiply_convert_fusion.x_ref, bf16[4,256,512]{2,1,0:T(8,128)(2,1)} %all-to-all-done.1.own_ref, bf16[4,256,512]{2,1,0:T(8,128)(2,1)} %collective-permute-done.1.other_ref, ...), custom_call_target="tpu_custom_call" | custom-call | tf_op jit(solution)/shard_map/qkv/pallas_call | solution.py:189
  110.1 28.8 %all_to_all.30 = bf16[4,256,1088]{1,2,0:T(8,128)(2,1)S(1)} all-to-all(bf16[4,256,1088]{1,2,0:T(8,128)(2,1)S(1)} %broadcast_in_dim.36), channel_id=1, replica_groups=mesh['z'=8,'y'=8,'x'=4,'c'=2] {'x'}, dimensions={0} | all-to-all | bytes 4456448 | tf_op jit(solution)/shard_map/all_to_all | solution.py:36
  138.9 5.1 %collective-permute-start.4 = (bf16[4,256,1088]{1,2,0:T(8,128)(2,1)S(1)}, bf16[4,256,1088]{1,2,0:T(8,128)(2,1)}, u32[]{:S(2)}, u32[]{:S(2)}) collective-permute-start(bf16[4,256,1088]{1,2,0:T(8,128)(2,1)S(1)} %all_to_all.30), channel_id=1, source_target_pairs={{0,1},{1,0},{2,3},{3,2},{4,5},{5,4},{6,7},{7,6},{8,9},{9,8},{10,11... | collective-permute-start | bytes 6684680 | tf_op jit(solution)/shard_map/ppermute | solution.py:309
  144.0 21.3 %all_gather.11.k0_ref.v0_ref = bf16[1792,256]{1,0:T(8,128)(2,1)S(1)} all-gather(bf16[224,256]{1,0:T(8,128)(2,1)S(1)} %copy-done.4), channel_id=1, replica_groups=mesh['z'=8,'y'=8,'x'=4,'c'=2] {'z'}, dimensions={0}, use_global_device_ids=true | all-gather | bytes 1032192 | tf_op jit(solution)/shard_map/all_gather | solution.py:307
  165.3 7.2 %collective-permute-start.2 = (bf16[1792,256]{1,0:T(8,128)(2,1)S(1)}, bf16[1792,256]{1,0:T(8,128)(2,1)}, u32[]{:S(2)}, u32[]{:S(2)}) collective-permute-start(bf16[1792,256]{1,0:T(8,128)(2,1)S(1)} %all_gather.11.k0_ref.v0_ref), channel_id=1, source_target_pairs={{0,1},{1,0},{2,3},{3,2},{4,5},{5,4},{6,7},{7,6},{8,9},{9,8},{10,11... | collective-permute-start | bytes 2752520 | tf_op jit(solution)/shard_map/ppermute | solution.py:308
  172.7 2.8 %collective-permute-start.3 = (f32[40,192]{1,0:T(8,128)S(1)}, f32[40,192]{1,0:T(8,128)S(1)}, u32[]{:S(2)}, u32[]{:S(2)}) collective-permute-start(f32[40,192]{1,0:T(8,128)S(1)} %maximum_maximum_fusion), channel_id=1, source_target_pairs={{0,0},{1,8},{2,16},{3,24},{4,32},{5,40},{6,48},{7,56},{8,1},{9,9},... | collective-permute-start | bytes 92168 | tf_op jit(solution)/shard_map/ppermute | solution.py:282
  175.6 2.4 collective-permute-done.3
  178.0 2.6 copy.39.qs_ref.own_ref
  180.6 18.2 %attend.1 = bf16[4,912,128]{2,1,0:T(8,128)(2,1)} custom-call(bf16[4,256,1088]{2,1,0:T(8,128)(2,1)} %copy.39.qs_ref.own_ref, bf16[1792,256]{1,0:T(8,128)(2,1)} %copy-done.2, bf16[1792,256]{1,0:T(8,128)(2,1)} %copy-done.2, bf16[1792,256]{1,0:T(8,128)(2,1)} %collective-permute-done.2.k1_ref.v1_ref, bf16[1792,256]{1,0:T(8,128)(2,1)} %collective-permute-done.2.k1_ref.v1_ref), custom_call_target="tpu_custom_call" | custom-call | flops 9865003008 | bytes 3670016 | tf_op jit(solution)/shard_map/attend/pallas_call | solution.py:97
  198.9 7.4 %all-to-all-start.3 = ((bf16[4,912,128]{2,1,0:T(8,128)(2,1)}), bf16[4,912,128]{2,1,0:T(8,128)(2,1)S(1)}, u32[]{:S(2)}, u32[]{:S(2)}) async-start(bf16[4,912,128]{2,1,0:T(8,128)(2,1)} %attend.1), calls=%async_computation.3 | async-start | bytes 1867776 | tf_op jit(solution)/shard_map/all_to_all | solution.py:311
  206.3 4.3 %copy.41.other_ref = bf16[4,256,1088]{2,1,0:T(8,128)(2,1)} copy(bf16[4,256,1088]{1,2,0:T(8,128)(2,1)} %collective-permute-done.4) | data formatting | bytes 4456448 | tf_op jit(solution)/shard_map/ppermute | solution.py:309
  210.6 4.0 %glu.1 = bf16[8,28,192]{2,1,0:T(8,128)(2,1)} custom-call(s32[1]{0:T(128)} %bitcast.core_ref, bf16[224,2048]{1,0:T(8,128)(2,1)} %multiply_convert_fusion.x_ref, bf16[4,256,1088]{2,1,0:T(8,128)(2,1)} %copy.39.qs_ref.own_ref, bf16[4,256,1088]{2,1,0:T(8,128)(2,1)} %copy.41.other_ref), custom_call_target="tpu_custom_call" | custom-call | tf_op jit(solution)/shard_map/glu/pallas_call | solution.py:213
  216.9 3.2 %collective-permute-start.6 = (bf16[8,15,192]{2,1,0:T(8,128)(2,1)S(1)}, bf16[8,15,192]{2,1,0:T(8,128)(2,1)S(1)}, u32[]{:S(2)}, u32[]{:S(2)}) collective-permute-start(bf16[8,15,192]{2,1,0:T(8,128)(2,1)S(1)} %get-tuple-element.11), channel_id=1, source_target_pairs={{0,1},{1,2},{2,3},{3,4},{4,5},{5,6},{6,7},{7,0},{8,9},{9,10},{10,1... | collective-permute-start | bytes 138248 | tf_op jit(solution)/shard_map/ppermute | solution.py:320
  220.2 1.3 collective-permute-done.6
  221.5 2.4 collective-permute-done.7
  223.9 5.2 %multiply_reduce_fusion = (f32[8,28]{1,0:T(8,128)S(1)}, f32[8,28,192]{2,1,0:T(8,128)S(1)}) fusion(bf16[8,15,192]{2,1,0:T(8,128)(2,1)S(1)} %get-tuple-element.46, bf16[8,28,192]{2,1,0:T(8,128)(2,1)} %glu.1, f32[192]{0:T(256)S(1)} %bitcast.51, f32[192]{0:T(256)S(1)} %bitcast.52, f32[192]{0:T(256)S(1)} %bitcast.53, f32[192]{0:T(256)S(1)} %bitcast.54, ...), kind=kLoop, calls=%fused_computation.64 | loop fusion | flops 7913248 | bytes 374912 | tf_op jit(solution)/shard_map/reduce_sum | solution.py:333
  229.8 4.1 %all-to-all-start.4 = ((f32[8,1,224]{2,1,0:T(1,128)}), f32[8,1,224]{2,1,0:T(1,128)S(1)}, u32[]{:S(2)}, u32[]{:S(2)}) async-start(f32[8,1,224]{2,1,0:T(1,128)} %reshape.92), calls=%async_computation.4 | async-start | bytes 16384 | tf_op jit(solution)/shard_map/all_to_all | solution.py:36
  234.6 2.1 combine.1.att_ref
  236.7 3.8 %all-to-all-done.4 = f32[8,1,224]{2,1,0:T(1,128)S(1)} async-done(((f32[8,1,224]{2,1,0:T(1,128)}), f32[8,1,224]{2,1,0:T(1,128)S(1)}, u32[]{:S(2)}, u32[]{:S(2)}) %all-to-all-start.4) | async-done | bytes 7200 | tf_op jit(solution)/shard_map/all_to_all | solution.py:36
  242.6 4.3 %out.1 = bf16[8,28,2048]{2,1,0:T(8,128)(2,1)} custom-call(s32[1]{0:T(128)} %bitcast.core_ref, bf16[224,256]{1,0:T(8,128)(2,1)} %combine.1.att_ref, bf16[224,192]{1,0:T(8,128)(2,1)} %reshape.87.conv_ref, bf16[4,256,1088]{2,1,0:T(8,128)(2,1)} %copy.39.qs_ref.own_ref, bf16[4,256,1088]{2,1,0:T(8,128)(2,1)} %copy.41.other_ref), custom_call_target="tpu_custom_call" | custom-call | tf_op jit(solution)/shard_map/out/pallas_call | solution.py:236
  246.9 28.9 %all_to_all.31 = bf16[8,28,2048]{2,1,0:T(8,128)(2,1)S(1)} all-to-all(bf16[8,28,2048]{2,1,0:T(8,128)(2,1)} %out.1), channel_id=1, replica_groups=mesh['z'=8,'y'=8,'x'=4,'c'=2] {'y'}, dimensions={0} | all-to-all | bytes 1835008 | tf_op jit(solution)/shard_map/all_to_all | solution.py:339
  (74 shorter events, 12.6 us)
Async XLA Ops:
  0.9 6.8 %collective-permute-start = (bf16[32,1344]{1,0:T(8,128)(2,1)S(1)}, bf16[32,1344]{1,0:T(8,128)(2,1)S(1)}, u32[]{:S(2)}, u32[]{:S(2)}) collective-permute-start(bf16[32,1344]{1,0:T(8,128)(2,1)S(1)} %concatenate.50), channel_id=1, source_target_pairs={{0,0},{1,8},{2,16},{3,24},{4,32},{5,40},{6,48},{7,56},{8,1},{9,9},... | collective-permute-start | bytes 258056 | tf_op jit(solution)/shard_map/ppermute | solution.py:272
  34.6 40.3 %copy-start.1 = (bf16[256,1344]{1,0:T(8,128)(2,1)}, bf16[256,1344]{1,0:T(8,128)(2,1)S(1)}, u32[]{:S(2)}) copy-start(bf16[256,1344]{1,0:T(8,128)(2,1)S(1)} %all-gather) | copy-start | bytes 2064388
  34.6 10.8 %copy-start.3 = (bf16[224,256]{1,0:T(8,128)(2,1)S(1)}, bf16[224,256]{1,0:T(8,128)(2,1)}, u32[]{:S(2)}) copy-start(bf16[224,256]{1,0:T(8,128)(2,1)} %param.15) | copy-start | bytes 344068
  35.7 19.5 %all-to-all-start.1 = ((bf16[4,256,512]{2,1,0:T(8,128)(2,1)}), bf16[4,256,512]{2,1,0:T(8,128)(2,1)}, u32[]{:S(2)}, u32[]{:S(2)}) async-start(bf16[4,256,512]{2,1,0:T(8,128)(2,1)} %broadcast_in_dim.35), calls=%async_computation.1 | async-start | bytes 2097152 | tf_op jit(solution)/shard_map/all_to_all | solution.py:36
  45.4 28.2 %copy-start.9 = (f32[64]{0:T(128)S(1)}, f32[64]{0:T(128)}, u32[]{:S(2)}) copy-start(f32[64]{0:T(128)} %param.22) | copy-start | bytes 772
  45.4 28.9 %copy-start.10 = (f32[64]{0:T(128)S(1)}, f32[64]{0:T(128)}, u32[]{:S(2)}) copy-start(f32[64]{0:T(128)} %param.23) | copy-start | bytes 772
  56.4 45.4 %all-to-all-start = ((bf16[64,28,256]{2,1,0:T(8,128)(2,1)}), bf16[64,28,256]{2,1,0:T(8,128)(2,1)S(1)}, u32[]{:S(2)}, u32[]{:S(2)}) async-start(bf16[64,28,256]{2,1,0:T(8,128)(2,1)} %bitcast.1), calls=%async_computation | async-start | bytes 2097152 | tf_op jit(solution)/shard_map/all_to_all | solution.py:288
  75.0 30.4 %collective-permute-start.1 = (bf16[4,256,512]{2,1,0:T(8,128)(2,1)}, bf16[4,256,512]{2,1,0:T(8,128)(2,1)}, u32[]{:S(2)}, u32[]{:S(2)}) collective-permute-start(bf16[4,256,512]{2,1,0:T(8,128)(2,1)} %all-to-all-done.1.own_ref), channel_id=1, source_target_pairs={{0,1},{1,0},{2,3},{3,2},{4,5},{5,4},{6,7},{7,6},{8,9},{9,8},{10,11... | collective-permute-start | bytes 3145736 | tf_op jit(solution)/shard_map/ppermute | solution.py:298
  102.5 1.6 copy-start.6
  105.3 3.4 %slice-start = ((bf16[256,1344]{1,0:T(8,128)(2,1)}), bf16[256,832]{1,0:T(8,128)(2,1)S(1)}, s32[]{:S(2)}) async-start(bf16[256,1344]{1,0:T(8,128)(2,1)} %copy-done.1), calls=%async_computation.6 | async-start | bytes 917504 | tf_op jit(solution)/shard_map/slice | solution.py:304
  110.1 33.9 %copy-start.4 = (bf16[224,256]{1,0:T(8,128)(2,1)S(1)}, bf16[224,256]{1,0:T(8,128)(2,1)}, u32[]{:S(2)}) copy-start(bf16[224,256]{1,0:T(8,128)(2,1)} %get-tuple-element.8) | copy-start | bytes 344068
  110.1 62.4 %copy-start.8 = (f32[2]{0:T(128)S(1)}, f32[2]{0:T(128)}, u32[]{:S(2)}) copy-start(f32[2]{0:T(128)} %param.24) | copy-start | bytes 28
  110.1 62.5 %copy-start.5 = (f32[31,192]{1,0:T(8,128)S(1)}, f32[31,192]{1,0:T(8,128)}, u32[]{:S(2)}) copy-start(f32[31,192]{1,0:T(8,128)} %param.26) | copy-start | bytes 71428
  110.1 62.5 %copy-start.7 = (f32[192]{0:T(256)S(1)}, f32[192]{0:T(256)}, u32[]{:S(2)}) copy-start(f32[192]{0:T(256)} %param.27) | copy-start | bytes 2308
  138.9 67.4 %collective-permute-start.4 = (bf16[4,256,1088]{1,2,0:T(8,128)(2,1)S(1)}, bf16[4,256,1088]{1,2,0:T(8,128)(2,1)}, u32[]{:S(2)}, u32[]{:S(2)}) collective-permute-start(bf16[4,256,1088]{1,2,0:T(8,128)(2,1)S(1)} %all_to_all.30), channel_id=1, source_target_pairs={{0,1},{1,0},{2,3},{3,2},{4,5},{5,4},{6,7},{7,6},{8,9},{9,8},{10,11... | collective-permute-start | bytes 6684680 | tf_op jit(solution)/shard_map/ppermute | solution.py:309
  165.3 15.4 %copy-start.2 = (bf16[1792,256]{1,0:T(8,128)(2,1)}, bf16[1792,256]{1,0:T(8,128)(2,1)S(1)}, u32[]{:S(2)}) copy-start(bf16[1792,256]{1,0:T(8,128)(2,1)S(1)} %all_gather.11.k0_ref.v0_ref) | copy-start | bytes 2752516
  165.3 15.4 %collective-permute-start.2 = (bf16[1792,256]{1,0:T(8,128)(2,1)S(1)}, bf16[1792,256]{1,0:T(8,128)(2,1)}, u32[]{:S(2)}, u32[]{:S(2)}) collective-permute-start(bf16[1792,256]{1,0:T(8,128)(2,1)S(1)} %all_gather.11.k0_ref.v0_ref), channel_id=1, source_target_pairs={{0,1},{1,0},{2,3},{3,2},{4,5},{5,4},{6,7},{7,6},{8,9},{9,8},{10,11... | collective-permute-start | bytes 2752520 | tf_op jit(solution)/shard_map/ppermute | solution.py:308
  172.7 5.3 %collective-permute-start.3 = (f32[40,192]{1,0:T(8,128)S(1)}, f32[40,192]{1,0:T(8,128)S(1)}, u32[]{:S(2)}, u32[]{:S(2)}) collective-permute-start(f32[40,192]{1,0:T(8,128)S(1)} %maximum_maximum_fusion), channel_id=1, source_target_pairs={{0,0},{1,8},{2,16},{3,24},{4,32},{5,40},{6,48},{7,56},{8,1},{9,9},... | collective-permute-start | bytes 92168 | tf_op jit(solution)/shard_map/ppermute | solution.py:282
  198.9 30.9 %all-to-all-start.3 = ((bf16[4,912,128]{2,1,0:T(8,128)(2,1)}), bf16[4,912,128]{2,1,0:T(8,128)(2,1)S(1)}, u32[]{:S(2)}, u32[]{:S(2)}) async-start(bf16[4,912,128]{2,1,0:T(8,128)(2,1)} %attend.1), calls=%async_computation.3 | async-start | bytes 1867776 | tf_op jit(solution)/shard_map/all_to_all | solution.py:311
  216.3 7.6 %collective-permute-start.5 = (bf16[1,15,192]{2,1,0:T(8,128)(2,1)S(1)}, bf16[1,15,192]{2,1,0:T(8,128)(2,1)S(1)}, u32[]{:S(2)}, u32[]{:S(2)}) collective-permute-start(bf16[1,15,192]{2,1,0:T(8,128)(2,1)S(1)} %slice_select_fusion), channel_id=1, source_target_pairs={{7,64},{71,128},{135,192},{199,256},{263,320},{327,384},{391,448},... | collective-permute-start | bytes 17288 | tf_op jit(solution)/shard_map/ppermute | solution.py:326
  216.9 4.6 %collective-permute-start.6 = (bf16[8,15,192]{2,1,0:T(8,128)(2,1)S(1)}, bf16[8,15,192]{2,1,0:T(8,128)(2,1)S(1)}, u32[]{:S(2)}, u32[]{:S(2)}) collective-permute-start(bf16[8,15,192]{2,1,0:T(8,128)(2,1)S(1)} %get-tuple-element.11), channel_id=1, source_target_pairs={{0,1},{1,2},{2,3},{3,4},{4,5},{5,6},{6,7},{7,0},{8,9},{9,10},{10,1... | collective-permute-start | bytes 138248 | tf_op jit(solution)/shard_map/ppermute | solution.py:320
  220.2 3.7 %collective-permute-start.7 = (bf16[8,15,192]{2,1,0:T(8,128)(2,1)S(1)}, bf16[8,15,192]{2,1,0:T(8,128)(2,1)S(1)}, u32[]{:S(2)}, u32[]{:S(2)}) collective-permute-start(bf16[8,15,192]{2,1,0:T(8,128)(2,1)S(1)} %get-tuple-element.12), channel_id=1, source_target_pairs={{1,0},{2,1},{3,2},{4,3},{5,4},{6,5},{7,6},{0,7},{9,8},{10,9},{11,1... | collective-permute-start | bytes 138248 | tf_op jit(solution)/shard_map/ppermute | solution.py:321
  229.8 4.8 %copy-start = (bf16[4,912,128]{2,1,0:T(8,128)(2,1)}, bf16[4,912,128]{2,1,0:T(8,128)(2,1)S(1)}, u32[]{:S(2)}) copy-start(bf16[4,912,128]{2,1,0:T(8,128)(2,1)S(1)} %all-to-all-done.3.parts_ref) | copy-start | bytes 2801668
  229.8 10.7 %all-to-all-start.4 = ((f32[8,1,224]{2,1,0:T(1,128)}), f32[8,1,224]{2,1,0:T(1,128)S(1)}, u32[]{:S(2)}, u32[]{:S(2)}) async-start(f32[8,1,224]{2,1,0:T(1,128)} %reshape.92), calls=%async_computation.4 | async-start | bytes 16384 | tf_op jit(solution)/shard_map/all_to_all | solution.py:36

commit v4 on v3

--- a/solution.py
+++ b/solution.py
@@ -161,7 +161,7 @@
     return acc
 
 
-def qkv_kernel(core_ref, x_ref, own_ref, other_ref, qg_ref, kg_ref, q_ref, kv_ref):
+def qkv_kernel(core_ref, x_ref, own_ref, other_ref, qg_ref, kg_ref, _, q_ref, kv_ref):
     acc = project(core_ref[0], x_ref, own_ref, other_ref, slice(0, own_ref.shape[2]))
     low = lax.broadcasted_iota(jnp.int32, (x_ref.shape[0], WIDTH), 1) < HEAD_DIM
 
@@ -173,9 +173,12 @@
         second = lax.rsqrt(second / HEAD_DIM + EPS)
         return (block * jnp.where(low, first, second) * gain).astype(BF)
 
-    q_cols = q_ref.shape[1]
+    tok, q_cols = x_ref.shape[0], q_ref.shape[2]
     for at in range(0, q_cols, WIDTH):
-        q_ref[:, at : at + WIDTH] = normed(acc[:, at : at + WIDTH], qg_ref[...])
+        q = normed(acc[:, at : at + WIDTH], qg_ref[...])
+        for g in range(q_ref.shape[0]):
+            q_ref[g, :tok, at : at + WIDTH] = q
+    q_ref[:, tok:, :] = jnp.zeros((q_ref.shape[0], q_ref.shape[1] - tok, q_cols), BF)
     kv_ref[:, :WIDTH] = normed(acc[:, q_cols : q_cols + WIDTH], kg_ref[...])
     kv_ref[:, WIDTH:] = acc[:, q_cols + WIDTH :].astype(BF)
 
@@ -184,18 +187,20 @@
 VMEM = pl.BlockSpec(memory_space=pltpu.VMEM)
 
 
-def qkv(core, x, own, other, query_gain, key_gain):
+def qkv(core, x, own, other, query_gain, key_gain, packed):
     tok, q_cols = x.shape[0], own.shape[2] - 2 * WIDTH
     return pl.pallas_call(
         qkv_kernel,
-        in_specs=[SMEM] + [VMEM] * 5,
-        out_specs=[VMEM, VMEM],
+        grid=(1,),
+        in_specs=[SMEM] + [VMEM] * 5 + [pl.BlockSpec(memory_space=pl.ANY)],
+        out_specs=[pl.BlockSpec((*packed.shape[:2], q_cols), lambda i: (0, 0, 0)), VMEM],
         out_shape=[
-            jax.ShapeDtypeStruct((tok, q_cols), BF),
+            jax.ShapeDtypeStruct(packed.shape, BF),
             jax.ShapeDtypeStruct((tok, 2 * WIDTH), BF),
         ],
+        input_output_aliases={6: 0},
         name="qkv",
-    )(core, x, own, other, jnp.tile(query_gain, 2)[None], jnp.tile(key_gain, 2)[None])
+    )(core, x, own, other, jnp.tile(query_gain, 2)[None], jnp.tile(key_gain, 2)[None], packed)
 
 
 def glu_kernel(core_ref, x_ref, own_ref, other_ref, out_ref, *, start):
@@ -219,8 +224,44 @@
     )(core, x, own, other)
 
 
+def conv_kernel(
+    t_ref, glu_ref, left_ref, right_ref, edge_ref, w_ref, sum_ref, sq_ref, pad_ref
+):
+    n, seg, _ = glu_ref.shape
+    t = t_ref[0]
+    for y in range(n):
+        inner = edge_ref[0] if y == 0 else left_ref[y - 1]
+        pad_ref[y, :REACH] = jnp.where(t == 0, inner, left_ref[y]).astype(F32)
+        pad_ref[y, REACH : REACH + seg] = glu_ref[y].astype(F32)
+        inner = edge_ref[0] if y == n - 1 else right_ref[y + 1]
+        pad_ref[y, REACH + seg : 2 * REACH + seg] = jnp.where(
+            t == n - 1, inner, right_ref[y]
+        ).astype(F32)
+    for y in range(n):
+        acc = jnp.zeros((seg, glu_ref.shape[2]), F32)
+        for j in range(CONV_W):
+            acc = acc + w_ref[j : j + 1, :] * pad_ref[y, j : j + seg]
+        sum_ref[y] = acc
+        sq_ref[y] = jnp.sum(acc * acc, axis=1, keepdims=True)
+
+
+def conv_of(t, glu, left, right, edge, weight):
+    n, seg, channels = glu.shape
+    return pl.pallas_call(
+        conv_kernel,
+        in_specs=[SMEM] + [VMEM] * 5,
+        out_specs=[VMEM, VMEM],
+        out_shape=[
+            jax.ShapeDtypeStruct((n, seg, channels), F32),
+            jax.ShapeDtypeStruct((n, seg, 1), F32),
+        ],
+        scratch_shapes=[pltpu.VMEM((n, 64, channels), F32)],
+        name="conv",
+    )(t, glu, left, right, edge, weight)
+
+
 def out_kernel(core_ref, att_ref, conv_ref, own_ref, other_ref, out_ref, *, start):
-    cols = slice(start, own_ref.shape[2])
+    cols = slice(start, start + att_ref.shape[1] + conv_ref.shape[1])
     act = jnp.concatenate([att_ref[...], conv_ref[...]], axis=1)
     seg = out_ref.shape[1]
     for z in range(own_ref.shape[1] // 32):
@@ -269,19 +310,23 @@
     weights = (query_weight, key_weight, value_weight, glu_value_weight, glu_gate_weight)
     weights = weights + (attn_out_weight, conv_out_weight)
     first = sum(w.shape[1] for w in weights[:3])
-    shard = lax.ppermute(jnp.concatenate(weights, axis=1), PLANE, swap)
-    small = jnp.concatenate(
-        [
-            conv_weight,
-            channel_gain[None],
-            jnp.pad(lambdas, (0, channels - heads))[None],
-            jnp.zeros((7, channels), F32),
-        ],
-        axis=0,
+    small = jnp.concatenate([conv_weight, channel_gain[None]], axis=0)
+    lam = jnp.pad(lambdas[None], ((0, small.shape[0] - 1), (0, WIDTH - heads)))
+    small = jnp.concatenate([small, lam], axis=1)
+    terms = []
+    for _ in range(3):
+        term = lax.reduce_precision(small, 8, 7)
+        small = small - term
+        terms.append(term.astype(BF))
+    columns = sum(w.shape[1] for w in weights)
+    shard = lax.ppermute(jnp.concatenate(weights + tuple(terms), axis=1), PLANE, swap)
+    span = channels + WIDTH
+    small = sum(
+        shard[:, columns + i * span : columns + (i + 1) * span].astype(F32) for i in (2, 1, 0)
     )
-    small = lax.ppermute(small, PLANE, swap)
-    conv_weight, channel_gain = small[:CONV_W], small[CONV_W]
-    lambdas = small[CONV_W + 1, :heads]
+    shard = shard[:, :columns]
+    conv_weight, channel_gain = small[:CONV_W, :channels], small[CONV_W, :channels]
+    lambdas = small[0, channels : channels + heads]
 
     blocks = tokens.reshape(n, seg, tokens.shape[1])
     blocks = jnp.broadcast_to(blocks, (n, *blocks.shape)).reshape(n * n, seg, -1)
@@ -297,17 +342,16 @@
     wa = copies_to(by_z[:, :first], "x")
     wa_other = lax.ppermute(wa, "c", mates)
     fold = math.log2(math.e) * HEAD_DIM ** (-0.5)
-    q, kv = qkv(core, normed, wa, wa_other, query_gain * fold, key_gain)
-
-    q_cols = q.shape[1]
-    rest = jnp.concatenate(
-        [jnp.pad(q, ((0, by_z.shape[0] - tok), (0, 0))), by_z[:, first:]], axis=1
-    )
-    rest = copies_to(rest, "x")
+    q_cols = query_weight.shape[1]
+    late = columns - first
+    rest = jnp.pad(by_z[:, first:], ((0, 0), (q_cols, -(q_cols + late) % WIDTH)))
+    rest = jnp.broadcast_to(rest, (lax.axis_size("x"), *rest.shape))
+    rest, kv = qkv(core, normed, wa, wa_other, query_gain * fold, key_gain, rest)
+    rest = lax.all_to_all(rest, "x", 0, 0, tiled=True)
     kv = lax.all_gather(kv, "z", axis=0, tiled=True)
     kv_other = lax.ppermute(kv, "c", mates)
     rest_other = lax.ppermute(rest, "c", mates)
-    parts = attend(rest, tok, q_cols, kv, kv_other, 256, 896, 256)
+    parts = attend(rest, tok, q_cols, kv, kv_other, 1792, 896, 256)
     arrived = lax.all_to_all(parts, "x", 0, 0, tiled=True)
     att = combine(arrived, lambdas, head_gain, tok, heads)
 
@@ -324,13 +368,8 @@
     across = across + [(b, a) for a, b in across]
     edge = jnp.where(t == 0, heads_rows[:1], tails[n - 1 :])
     edge = lax.ppermute(edge, TOK_RING, across)
-    left = jnp.where(t == 0, jnp.concatenate([edge, left[:-1]], axis=0), left)
-    right = jnp.where(t == n - 1, jnp.concatenate([right[1:], edge], axis=0), right)
-    padded = jnp.concatenate([left, glu, right], axis=1)
-    conv_sum = jnp.zeros((n, seg, g_cols), F32)
-    for offset in range(CONV_W):
-        conv_sum = conv_sum + conv_weight[offset] * padded[:, offset : offset + seg].astype(F32)
-    squares = jnp.sum(conv_sum * conv_sum, axis=2)
+    conv_sum, squares = conv_of(t.astype(jnp.int32)[None], glu, left, right, edge, conv_weight)
+    squares = squares.reshape(n, seg)
     squares = jnp.sum(copies_to(squares, "y"), axis=0)
     scaled = conv_sum * lax.rsqrt(squares / C_CH + EPS)[..., None] * channel_gain
     conv_out = jax.nn.silu(scaled).astype(BF).reshape(tok, g_cols)

time: 281 us -> 271 us (0.964)
  the two profiles are of different devices: /device:TPU:1 before, /device:TPU:3 now
where the time goes in v4:
time: 271 us; the launch traced here: 270 us
  blocking collectives  110 us (41%)
  starting transfers between devices  58.8 us (22%)
  waiting for transfers between devices  47.5 us (18%)
  Pallas kernels  33.5 us (12%)
  local copies, waits for them, and re-layouts  12.3 us (5%)
  other arithmetic  7.61 us (3%)
    all_to_all x1, blocking collectives, local(): reduced = lax.all_to_all(term, 'y', 0, 0, tiled=True)  32.7 us
    all_to_all x1, blocking collectives, local(): rest = lax.all_to_all(rest, 'x', 0, 0, tiled=True)  30.7 us
    all_gather x1, blocking collectives, local(): by_z = lax.all_gather(shard, 'z', axis=0)  25.9 us
    all_to_all x1, waiting for transfers between devices, local(): mine = lax.all_to_all(blocks, PLANE, 0, 0, tiled=True)  23.8 us
    all_gather x1, blocking collectives, local(): kv = lax.all_gather(kv, 'z', axis=0, tiled=True)  21 us
    pallas_call x1, Pallas kernels, attend(): pl.pallas_call(functools.partial(attend_kernel, tok=tok, rows=rows, keys=...  16.5 us
    all_to_all x2, starting transfers between devices, copies_to(): return lax.all_to_all(copies, axis, 0, 0, tiled=True)  16.2 us
    all_to_all x1, starting transfers between devices, local(): mine = lax.all_to_all(blocks, PLANE, 0, 0, tiled=True)  15.2 us
  transfers between devices with their start and end apart: 11, of which 6 were waited for; matrix products, arithmetic and copies ran while one was open for 4% of the time, Pallas kernels for 10%

profile of v4, /device:TPU:3, one launch (start us, length us, event | category | flops | bytes accessed | tf_op | source)
XLA Modules:
  0.0 270.3 jit_solution(10079218536993145652)
XLA Ops:
  1.8 5.8 %collective-permute-start = (bf16[32,2304]{1,0:T(8,128)(2,1)S(1)}, bf16[32,2304]{1,0:T(8,128)(2,1)S(1)}, u32[]{:S(2)}, u32[]{:S(2)}) collective-permute-start(bf16[32,2304]{1,0:T(8,128)(2,1)S(1)} %concatenate.11), channel_id=1, source_target_pairs={{0,0},{1,8},{2,16},{3,24},{4,32},{5,40},{6,48},{7,56},{8,1},{9,9},... | collective-permute-start | bytes 442376 | tf_op jit(solution)/shard_map/ppermute | solution.py:322
  7.6 4.6 %collective-permute-done = bf16[32,2304]{1,0:T(8,128)(2,1)S(1)} collective-permute-done((bf16[32,2304]{1,0:T(8,128)(2,1)S(1)}, bf16[32,2304]{1,0:T(8,128)(2,1)S(1)}, u32[]{:S(2)}, u32[]{:S(2)}) %collective-permute-start) | collective-permute-done | bytes 147488 | tf_op jit(solution)/shard_map/ppermute | solution.py:322
  12.2 25.9 %all-gather = bf16[256,1344]{1,0:T(8,128)(2,1)S(1)} all-gather(bf16[32,1344]{1,0:T(8,128)(2,1)S(1)} %slice.54), channel_id=2, replica_groups=mesh['z'=8,'y'=8,'x'=4,'c'=2] {'z'}, dimensions={0}, use_global_device_ids=true | all-gather | bytes 774144 | tf_op jit(solution)/shard_map/all_gather | solution.py:338
  38.1 1.1 broadcast_in_dim.37
  39.2 12.1 %all-to-all-start.1 = ((bf16[4,256,512]{2,1,0:T(8,128)(2,1)}), bf16[4,256,512]{2,1,0:T(8,128)(2,1)S(1)}, u32[]{:S(2)}, u32[]{:S(2)}) async-start(bf16[4,256,512]{2,1,0:T(8,128)(2,1)} %broadcast_in_dim.37), calls=%async_computation.1 | async-start | bytes 2097152 | tf_op jit(solution)/shard_map/all_to_all | solution.py:36
  51.3 8.6 %all-to-all-done.1.own_ref = bf16[4,256,512]{2,1,0:T(8,128)(2,1)S(1)} async-done(((bf16[4,256,512]{2,1,0:T(8,128)(2,1)}), bf16[4,256,512]{2,1,0:T(8,128)(2,1)S(1)}, u32[]{:S(2)}, u32[]{:S(2)}) %all-to-all-start.1) | async-done | bytes 1048608 | tf_op jit(solution)/shard_map/all_to_all | solution.py:36
  59.9 1.2 broadcast_in_dim.34
  61.2 15.2 %all-to-all-start = ((bf16[64,28,256]{2,1,0:T(8,128)(2,1)}), bf16[64,28,256]{2,1,0:T(8,128)(2,1)S(1)}, u32[]{:S(2)}, u32[]{:S(2)}) async-start(bf16[64,28,256]{2,1,0:T(8,128)(2,1)} %bitcast.1), calls=%async_computation | async-start | bytes 2097152 | tf_op jit(solution)/shard_map/all_to_all | solution.py:333
  77.7 2.3 collective-permute-start.1
  80.0 23.8 %all-to-all-done = bf16[64,28,256]{2,1,0:T(8,128)(2,1)S(1)} async-done(((bf16[64,28,256]{2,1,0:T(8,128)(2,1)}), bf16[64,28,256]{2,1,0:T(8,128)(2,1)S(1)}, u32[]{:S(2)}, u32[]{:S(2)}) %all-to-all-start) | async-done | bytes 917536 | tf_op jit(solution)/shard_map/all_to_all | solution.py:333
  106.1 1.2 multiply_convert_fusion.x_ref
  107.3 1.6 broadcast_in_dim.38._
  108.9 3.5 %qkv.1 = (bf16[4,256,1152]{2,1,0:T(8,128)(2,1)}, bf16[224,256]{1,0:T(8,128)(2,1)}) custom-call(s32[1]{0:T(128)} %bitcast.core_ref, bf16[224,2048]{1,0:T(8,128)(2,1)} %multiply_convert_fusion.x_ref, bf16[4,256,512]{2,1,0:T(8,128)(2,1)} %copy-done.1, bf16[4,256,512]{2,1,0:T(8,128)(2,1)} %collective-permute-done.1.other_ref, ...), custom_call_target="tpu_custom_call", output_to_operand_aliasing={{0}: (6, {})} | custom-call | tf_op jit(solution)/shard_map/qkv/pallas_call | solution.py:192
  112.4 30.7 %all_to_all.30.qs_ref.own_ref = bf16[4,256,1152]{2,1,0:T(8,128)(2,1)S(1)} all-to-all(bf16[4,256,1152]{2,1,0:T(8,128)(2,1)} %get-tuple-element.9), channel_id=1, replica_groups=mesh['z'=8,'y'=8,'x'=4,'c'=2] {'x'}, dimensions={0} | all-to-all | bytes 4718592 | tf_op jit(solution)/shard_map/all_to_all | solution.py:350
  143.1 4.6 %collective-permute-start.3 = (bf16[4,256,1152]{2,1,0:T(8,128)(2,1)S(1)}, bf16[4,256,1152]{2,1,0:T(8,128)(2,1)}, u32[]{:S(2)}, u32[]{:S(2)}) collective-permute-start(bf16[4,256,1152]{2,1,0:T(8,128)(2,1)S(1)} %all_to_all.30.qs_ref.own_ref), channel_id=1, source_target_pairs={{0,1},{1,0},{2,3},{3,2},{4,5},{5,4},{6,7},{7,6},{8,9},{9,8},{10,11... | collective-permute-start | bytes 7077896 | tf_op jit(solution)/shard_map/ppermute | solution.py:353
  147.7 21.0 %all_gather.11.k0_ref.v0_ref = bf16[1792,256]{1,0:T(8,128)(2,1)S(1)} all-gather(bf16[224,256]{1,0:T(8,128)(2,1)S(1)} %copy-done.5), channel_id=1, replica_groups=mesh['z'=8,'y'=8,'x'=4,'c'=2] {'z'}, dimensions={0}, use_global_device_ids=true | all-gather | bytes 1032192 | tf_op jit(solution)/shard_map/all_gather | solution.py:351
  168.7 7.7 %collective-permute-start.2 = (bf16[1792,256]{1,0:T(8,128)(2,1)S(1)}, bf16[1792,256]{1,0:T(8,128)(2,1)}, u32[]{:S(2)}, u32[]{:S(2)}) collective-permute-start(bf16[1792,256]{1,0:T(8,128)(2,1)S(1)} %all_gather.11.k0_ref.v0_ref), channel_id=1, source_target_pairs={{0,1},{1,0},{2,3},{3,2},{4,5},{5,4},{6,7},{7,6},{8,9},{9,8},{10,11... | collective-permute-start | bytes 2752520 | tf_op jit(solution)/shard_map/ppermute | solution.py:352
  176.4 2.0 collective-permute-done.2.k1_ref.v1_ref
  178.4 16.5 %attend.1 = bf16[4,912,128]{2,1,0:T(8,128)(2,1)} custom-call(bf16[4,256,1152]{2,1,0:T(8,128)(2,1)} %copy-done, bf16[1792,256]{1,0:T(8,128)(2,1)} %copy-done.3, bf16[1792,256]{1,0:T(8,128)(2,1)} %copy-done.3, bf16[1792,256]{1,0:T(8,128)(2,1)} %collective-permute-done.2.k1_ref.v1_ref, bf16[1792,256]{1,0:T(8,128)(2,1)} %collective-permute-done.2.k1_ref.v1_ref), custom_call_target="tpu_custom_call" | custom-call | flops 9865003008 | bytes 3670016 | tf_op jit(solution)/shard_map/attend/pallas_call | solution.py:97
  194.9 4.7 %all-to-all-start.3 = ((bf16[4,912,128]{2,1,0:T(8,128)(2,1)}), bf16[4,912,128]{2,1,0:T(8,128)(2,1)S(1)}, u32[]{:S(2)}, u32[]{:S(2)}) async-start(bf16[4,912,128]{2,1,0:T(8,128)(2,1)} %attend.1), calls=%async_computation.3 | async-start | bytes 1867776 | tf_op jit(solution)/shard_map/all_to_all | solution.py:355
  199.6 4.0 %glu.1.glu_ref = bf16[8,28,192]{2,1,0:T(8,128)(2,1)} custom-call(s32[1]{0:T(128)} %bitcast.core_ref, bf16[224,2048]{1,0:T(8,128)(2,1)} %multiply_convert_fusion.x_ref, bf16[4,256,1152]{2,1,0:T(8,128)(2,1)} %copy-done, bf16[4,256,1152]{2,1,0:T(8,128)(2,1)} %collective-permute-done.3.other_ref), custom_call_target="tpu_custom_call" | custom-call | tf_op jit(solution)/shard_map/glu/pallas_call | solution.py:218
  205.0 1.0 fusion.3
  206.7 1.1 collective-permute-start.4
  208.5 4.7 %collective-permute-done.5.right_ref = bf16[8,15,192]{2,1,0:T(8,128)(2,1)S(1)} collective-permute-done((bf16[8,15,192]{2,1,0:T(8,128)(2,1)S(1)}, bf16[8,15,192]{2,1,0:T(8,128)(2,1)S(1)}, u32[]{:S(2)}, u32[]{:S(2)}) %collective-permute-start.5) | collective-permute-done | bytes 46112 | tf_op jit(solution)/shard_map/ppermute | solution.py:365
  213.9 3.1 %conv.1 = (f32[8,28,192]{2,1,0:T(8,128)}, f32[8,28,1]{2,1,0:T(8,128)}) custom-call(s32[1]{0:T(128)} %bitcast.9.t_ref, bf16[8,28,192]{2,1,0:T(8,128)(2,1)} %glu.1.glu_ref, bf16[8,15,192]{2,1,0:T(8,128)(2,1)} %copy-done.7, bf16[8,15,192]{2,1,0:T(8,128)(2,1)} %copy-done.6, bf16[1,15,192]{2,1,0:T(8,128)(2,1)} %copy-done.9, f32[31,192]{1,0:T(8,128)} %slice.65.w_ref), custom_call_target="tpu_custom_call" | custom-call | tf_op jit(solution)/shard_map/conv/pallas_call | solution.py:250
  216.9 1.0 reduce.5
  218.7 4.1 %all-to-all-start.4 = ((f32[8,1,224]{2,1,0:T(1,128)}), f32[8,1,224]{2,1,0:T(1,128)S(1)}, u32[]{:S(2)}, u32[]{:S(2)}) async-start(f32[8,1,224]{2,1,0:T(1,128)} %reshape.66), calls=%async_computation.4 | async-start | bytes 16384 | tf_op jit(solution)/shard_map/all_to_all | solution.py:36
  223.5 2.1 combine.1.att_ref
  225.7 3.7 %all-to-all-done.4 = f32[8,1,224]{2,1,0:T(1,128)S(1)} async-done(((f32[8,1,224]{2,1,0:T(1,128)}), f32[8,1,224]{2,1,0:T(1,128)S(1)}, u32[]{:S(2)}, u32[]{:S(2)}) %all-to-all-start.4) | async-done | bytes 7200 | tf_op jit(solution)/shard_map/all_to_all | solution.py:36
  230.7 1.1 multiply_convert_fusion.1
  232.5 4.3 %out.1 = bf16[8,28,2048]{2,1,0:T(8,128)(2,1)} custom-call(s32[1]{0:T(128)} %bitcast.core_ref, bf16[224,256]{1,0:T(8,128)(2,1)} %combine.1.att_ref, bf16[224,192]{1,0:T(8,128)(2,1)} %reshape.60.conv_ref, bf16[4,256,1152]{2,1,0:T(8,128)(2,1)} %copy-done, bf16[4,256,1152]{2,1,0:T(8,128)(2,1)} %collective-permute-done.3.other_ref), custom_call_target="tpu_custom_call" | custom-call | tf_op jit(solution)/shard_map/out/pallas_call | solution.py:277
  236.8 32.7 %all_to_all.31 = bf16[8,28,2048]{2,1,0:T(8,128)(2,1)S(1)} all-to-all(bf16[8,28,2048]{2,1,0:T(8,128)(2,1)} %out.1), channel_id=1, replica_groups=mesh['z'=8,'y'=8,'x'=4,'c'=2] {'y'}, dimensions={0} | all-to-all | bytes 1835008 | tf_op jit(solution)/shard_map/all_to_all | solution.py:378
  (67 shorter events, 13.1 us)
Async XLA Ops:
  1.8 10.4 %collective-permute-start = (bf16[32,2304]{1,0:T(8,128)(2,1)S(1)}, bf16[32,2304]{1,0:T(8,128)(2,1)S(1)}, u32[]{:S(2)}, u32[]{:S(2)}) collective-permute-start(bf16[32,2304]{1,0:T(8,128)(2,1)S(1)} %concatenate.11), channel_id=1, source_target_pairs={{0,0},{1,8},{2,16},{3,24},{4,32},{5,40},{6,48},{7,56},{8,1},{9,9},... | collective-permute-start | bytes 442376 | tf_op jit(solution)/shard_map/ppermute | solution.py:322
  38.1 13.2 %copy-start.4 = (bf16[224,256]{1,0:T(8,128)(2,1)S(1)}, bf16[224,256]{1,0:T(8,128)(2,1)}, u32[]{:S(2)}) copy-start(bf16[224,256]{1,0:T(8,128)(2,1)} %param.15) | copy-start | bytes 344068
  39.2 20.8 %all-to-all-start.1 = ((bf16[4,256,512]{2,1,0:T(8,128)(2,1)}), bf16[4,256,512]{2,1,0:T(8,128)(2,1)S(1)}, u32[]{:S(2)}, u32[]{:S(2)}) async-start(bf16[4,256,512]{2,1,0:T(8,128)(2,1)} %broadcast_in_dim.37), calls=%async_computation.1 | async-start | bytes 2097152 | tf_op jit(solution)/shard_map/all_to_all | solution.py:36
  51.3 25.0 %copy-start.10 = (f32[64]{0:T(128)S(1)}, f32[64]{0:T(128)}, u32[]{:S(2)}) copy-start(f32[64]{0:T(128)} %param.22) | copy-start | bytes 772
  51.3 25.7 %copy-start.11 = (f32[64]{0:T(128)S(1)}, f32[64]{0:T(128)}, u32[]{:S(2)}) copy-start(f32[64]{0:T(128)} %param.23) | copy-start | bytes 772
  59.9 17.8 %copy-start.1 = (bf16[4,256,512]{2,1,0:T(8,128)(2,1)}, bf16[4,256,512]{2,1,0:T(8,128)(2,1)S(1)}, u32[]{:S(2)}) copy-start(bf16[4,256,512]{2,1,0:T(8,128)(2,1)S(1)} %all-to-all-done.1.own_ref) | copy-start | bytes 3145732
  61.2 42.7 %all-to-all-start = ((bf16[64,28,256]{2,1,0:T(8,128)(2,1)}), bf16[64,28,256]{2,1,0:T(8,128)(2,1)S(1)}, u32[]{:S(2)}, u32[]{:S(2)}) async-start(bf16[64,28,256]{2,1,0:T(8,128)(2,1)} %bitcast.1), calls=%async_computation | async-start | bytes 2097152 | tf_op jit(solution)/shard_map/all_to_all | solution.py:333
  77.7 29.6 %collective-permute-start.1 = (bf16[4,256,512]{2,1,0:T(8,128)(2,1)S(1)}, bf16[4,256,512]{2,1,0:T(8,128)(2,1)}, u32[]{:S(2)}, u32[]{:S(2)}) collective-permute-start(bf16[4,256,512]{2,1,0:T(8,128)(2,1)S(1)} %all-to-all-done.1.own_ref), channel_id=1, source_target_pairs={{0,1},{1,0},{2,3},{3,2},{4,5},{5,4},{6,7},{7,6},{8,9},{9,8},{10,11... | collective-permute-start | bytes 3145736 | tf_op jit(solution)/shard_map/ppermute | solution.py:343
  105.4 0.8 copy-start.8
  112.4 35.3 %copy-start.5 = (bf16[224,256]{1,0:T(8,128)(2,1)S(1)}, bf16[224,256]{1,0:T(8,128)(2,1)}, u32[]{:S(2)}) copy-start(bf16[224,256]{1,0:T(8,128)(2,1)} %get-tuple-element.10) | copy-start | bytes 344068
  143.1 35.3 %copy-start = (bf16[4,256,1152]{2,1,0:T(8,128)(2,1)}, bf16[4,256,1152]{2,1,0:T(8,128)(2,1)S(1)}, u32[]{:S(2)}) copy-start(bf16[4,256,1152]{2,1,0:T(8,128)(2,1)S(1)} %all_to_all.30.qs_ref.own_ref) | copy-start | bytes 7077892
  143.1 56.5 %collective-permute-start.3 = (bf16[4,256,1152]{2,1,0:T(8,128)(2,1)S(1)}, bf16[4,256,1152]{2,1,0:T(8,128)(2,1)}, u32[]{:S(2)}, u32[]{:S(2)}) collective-permute-start(bf16[4,256,1152]{2,1,0:T(8,128)(2,1)S(1)} %all_to_all.30.qs_ref.own_ref), channel_id=1, source_target_pairs={{0,1},{1,0},{2,3},{3,2},{4,5},{5,4},{6,7},{7,6},{8,9},{9,8},{10,11... | collective-permute-start | bytes 7077896 | tf_op jit(solution)/shard_map/ppermute | solution.py:353
  168.7 9.7 %copy-start.3 = (bf16[1792,256]{1,0:T(8,128)(2,1)}, bf16[1792,256]{1,0:T(8,128)(2,1)S(1)}, u32[]{:S(2)}) copy-start(bf16[1792,256]{1,0:T(8,128)(2,1)S(1)} %all_gather.11.k0_ref.v0_ref) | copy-start | bytes 2752516
  168.7 9.7 %collective-permute-start.2 = (bf16[1792,256]{1,0:T(8,128)(2,1)S(1)}, bf16[1792,256]{1,0:T(8,128)(2,1)}, u32[]{:S(2)}, u32[]{:S(2)}) collective-permute-start(bf16[1792,256]{1,0:T(8,128)(2,1)S(1)} %all_gather.11.k0_ref.v0_ref), channel_id=1, source_target_pairs={{0,1},{1,0},{2,3},{3,2},{4,5},{5,4},{6,7},{7,6},{8,9},{9,8},{10,11... | collective-permute-start | bytes 2752520 | tf_op jit(solution)/shard_map/ppermute | solution.py:352
  194.9 23.7 %all-to-all-start.3 = ((bf16[4,912,128]{2,1,0:T(8,128)(2,1)}), bf16[4,912,128]{2,1,0:T(8,128)(2,1)S(1)}, u32[]{:S(2)}, u32[]{:S(2)}) async-start(bf16[4,912,128]{2,1,0:T(8,128)(2,1)} %attend.1), calls=%async_computation.3 | async-start | bytes 1867776 | tf_op jit(solution)/shard_map/all_to_all | solution.py:355
  204.4 4.1 %collective-permute-start.6 = (bf16[1,15,192]{2,1,0:T(8,128)(2,1)S(1)}, bf16[1,15,192]{2,1,0:T(8,128)(2,1)S(1)}, u32[]{:S(2)}, u32[]{:S(2)}) collective-permute-start(bf16[1,15,192]{2,1,0:T(8,128)(2,1)S(1)} %slice_select_fusion), channel_id=1, source_target_pairs={{7,64},{71,128},{135,192},{199,256},{263,320},{327,384},{391,448},... | collective-permute-start | bytes 17288 | tf_op jit(solution)/shard_map/ppermute | solution.py:370
  206.0 7.2 %collective-permute-start.5 = (bf16[8,15,192]{2,1,0:T(8,128)(2,1)S(1)}, bf16[8,15,192]{2,1,0:T(8,128)(2,1)S(1)}, u32[]{:S(2)}, u32[]{:S(2)}) collective-permute-start(bf16[8,15,192]{2,1,0:T(8,128)(2,1)S(1)} %get-tuple-element.13), channel_id=1, source_target_pairs={{1,0},{2,1},{3,2},{4,3},{5,4},{6,5},{7,6},{0,7},{9,8},{10,9},{11,1... | collective-permute-start | bytes 138248 | tf_op jit(solution)/shard_map/ppermute | solution.py:365
  206.7 6.6 %collective-permute-start.4 = (bf16[8,15,192]{2,1,0:T(8,128)(2,1)S(1)}, bf16[8,15,192]{2,1,0:T(8,128)(2,1)S(1)}, u32[]{:S(2)}, u32[]{:S(2)}) collective-permute-start(bf16[8,15,192]{2,1,0:T(8,128)(2,1)S(1)} %get-tuple-element.14), channel_id=1, source_target_pairs={{0,1},{1,2},{2,3},{3,4},{4,5},{5,6},{6,7},{7,0},{8,9},{9,10},{10,1... | collective-permute-start | bytes 138248 | tf_op jit(solution)/shard_map/ppermute | solution.py:364
  208.5 4.8 %copy-start.9 = (bf16[1,15,192]{2,1,0:T(8,128)(2,1)}, bf16[1,15,192]{2,1,0:T(8,128)(2,1)S(1)}, u32[]{:S(2)}) copy-start(bf16[1,15,192]{2,1,0:T(8,128)(2,1)S(1)} %collective-permute-done.6.edge_ref) | copy-start | bytes 17284
  213.2 0.6 copy-start.6
  213.2 0.6 copy-start.7
  218.7 4.9 %copy-start.2 = (bf16[4,912,128]{2,1,0:T(8,128)(2,1)}, bf16[4,912,128]{2,1,0:T(8,128)(2,1)S(1)}, u32[]{:S(2)}) copy-start(bf16[4,912,128]{2,1,0:T(8,128)(2,1)S(1)} %all-to-all-done.3.parts_ref) | copy-start | bytes 2801668
  218.7 10.7 %all-to-all-start.4 = ((f32[8,1,224]{2,1,0:T(1,128)}), f32[8,1,224]{2,1,0:T(1,128)S(1)}, u32[]{:S(2)}, u32[]{:S(2)}) async-start(f32[8,1,224]{2,1,0:T(1,128)} %reshape.66), calls=%async_computation.4 | async-start | bytes 16384 | tf_op jit(solution)/shard_map/all_to_all | solution.py:36

commit v5 on v4

--- a/solution.py
+++ b/solution.py
@@ -203,25 +203,42 @@
     )(core, x, own, other, jnp.tile(query_gain, 2)[None], jnp.tile(key_gain, 2)[None], packed)
 
 
-def glu_kernel(core_ref, x_ref, own_ref, other_ref, out_ref, *, start):
-    channels = out_ref.shape[2]
+def glu_kernel(
+    core_ref, t_ref, x_ref, own_ref, other_ref, out_ref, head_ref, tail_ref, edge_ref, *, start
+):
+    n, seg, channels = out_ref.shape
     cols = slice(start, start + 2 * channels)
     acc = project(core_ref[0], x_ref, own_ref, other_ref, cols)
     value, gate = acc[:, :channels], acc[:, channels:]
     glu = value * (1.0 / (1.0 + jnp.exp(-gate)))
-    seg = out_ref.shape[1]
-    for y in range(out_ref.shape[0]):
-        out_ref[y] = glu[seg * y : seg * y + seg].astype(BF)
-
-
-def glu_of(core, x, own, other, start, channels, n):
+    for y in range(n):
+        rows = glu[seg * y : seg * y + seg]
+        out_ref[y] = rows.astype(BF)
+        head_ref[y] = rows[:REACH].astype(BF)
+        tail_ref[y] = rows[seg - REACH :].astype(BF)
+    first, last = glu[:REACH], glu[n * seg - REACH :]
+    edge_ref[0] = jnp.where(t_ref[0] == 0, first, last).astype(BF)
+
+
+def glu_of(core, t, x, own, other, start, channels, n):
+    reach = jax.ShapeDtypeStruct((n, REACH, channels), BF)
     return pl.pallas_call(
         functools.partial(glu_kernel, start=start),
-        in_specs=[SMEM] + [VMEM] * 3,
-        out_specs=VMEM,
-        out_shape=jax.ShapeDtypeStruct((n, x.shape[0] // n, channels), BF),
+        in_specs=[SMEM] * 2 + [VMEM] * 3,
+        out_specs=[VMEM] * 4,
+        out_shape=[
+            jax.ShapeDtypeStruct((n, x.shape[0] // n, channels), BF),
+            reach,
+            reach,
+            jax.ShapeDtypeStruct((1, REACH, channels), BF),
+        ],
         name="glu",
-    )(core, x, own, other)
+    )(core, t, x, own, other)
+
+
+def wide_eye(rows):
+    eye = lax.broadcasted_iota(jnp.int32, (rows, WIDTH), 0)
+    return eye == lax.broadcasted_iota(jnp.int32, (rows, WIDTH), 1)
 
 
 def conv_kernel(
@@ -237,12 +254,17 @@
         pad_ref[y, REACH + seg : 2 * REACH + seg] = jnp.where(
             t == n - 1, inner, right_ref[y]
         ).astype(F32)
+    lines = []
     for y in range(n):
         acc = jnp.zeros((seg, glu_ref.shape[2]), F32)
         for j in range(CONV_W):
             acc = acc + w_ref[j : j + 1, :] * pad_ref[y, j : j + seg]
         sum_ref[y] = acc
-        sq_ref[y] = jnp.sum(acc * acc, axis=1, keepdims=True)
+        column = jnp.sum(acc * acc, axis=1, keepdims=True)
+        lines.append(jnp.sum(jnp.where(wide_eye(seg), column, 0.0), axis=0, keepdims=True))
+    lines = jnp.concatenate(lines, axis=0)
+    for g in range(sq_ref.shape[0]):
+        sq_ref[g] = lines
 
 
 def conv_of(t, glu, left, right, edge, weight):
@@ -253,34 +275,47 @@
         out_specs=[VMEM, VMEM],
         out_shape=[
             jax.ShapeDtypeStruct((n, seg, channels), F32),
-            jax.ShapeDtypeStruct((n, seg, 1), F32),
+            jax.ShapeDtypeStruct((n, n, WIDTH), F32),
         ],
         scratch_shapes=[pltpu.VMEM((n, 64, channels), F32)],
         name="conv",
     )(t, glu, left, right, edge, weight)
 
 
-def out_kernel(core_ref, att_ref, conv_ref, own_ref, other_ref, out_ref, *, start):
-    cols = slice(start, start + att_ref.shape[1] + conv_ref.shape[1])
-    act = jnp.concatenate([att_ref[...], conv_ref[...]], axis=1)
-    seg = out_ref.shape[1]
+def out_kernel(
+    core_ref, att_ref, conv_ref, sq_ref, gain_ref, own_ref, other_ref, out_ref, act_ref, *, start
+):
+    n, seg, _ = out_ref.shape
+    channels = conv_ref.shape[2]
+    cols = slice(start, start + att_ref.shape[1] + channels)
+    squares = sq_ref[0]
+    for g in range(1, n):
+        squares = squares + sq_ref[g]
+    for y in range(n):
+        line = jnp.broadcast_to(squares[y : y + 1], (seg, WIDTH))
+        column = jnp.sum(jnp.where(wide_eye(seg), line, 0.0), axis=1, keepdims=True)
+        scaled = conv_ref[y] * lax.rsqrt(column / C_CH + EPS) * gain_ref[...]
+        act_ref[seg * y : seg * y + seg, :] = scaled * (1.0 / (1.0 + jnp.exp(-scaled)))
+    act = jnp.concatenate([att_ref[...], act_ref[...].astype(BF)], axis=1)
     for z in range(own_ref.shape[1] // 32):
         rhs = natural_rows(core_ref[0], own_ref, other_ref, z, cols)
         term = contract_last(act, rhs)
-        for y in range(out_ref.shape[0]):
+        for y in range(n):
             block = term[seg * y : seg * y + seg]
             out_ref[y, :, 256 * z : 256 * z + 256] = block.astype(BF)
 
 
-def out_of(core, att, conv, own, other, start, n):
+def out_of(core, att, conv, squares, gain, own, other, start):
+    n, seg, channels = conv.shape
     width = own.shape[0] * own.shape[1] * 2
     return pl.pallas_call(
         functools.partial(out_kernel, start=start),
-        in_specs=[SMEM] + [VMEM] * 4,
+        in_specs=[SMEM] + [VMEM] * 6,
         out_specs=VMEM,
-        out_shape=jax.ShapeDtypeStruct((n, att.shape[0] // n, width), BF),
+        out_shape=jax.ShapeDtypeStruct((n, seg, width), BF),
+        scratch_shapes=[pltpu.VMEM((n * seg, channels), F32)],
         name="out",
-    )(core, att, conv, own, other)
+    )(core, att, conv, squares, gain[None], own, other)
 
 
 def local(
@@ -306,27 +341,24 @@
     seg = tok // n
     channels = conv_weight.shape[1]
 
-    swap = [(y * n + t, t * n + y) for y in range(n) for t in range(n)]
+    row_of = [t // 2 + (n // 2) * (t % 2) for t in range(n)]
+    swap = [(y * n + t, row_of[t] * n + y) for y in range(n) for t in range(n)]
     weights = (query_weight, key_weight, value_weight, glu_value_weight, glu_gate_weight)
     weights = weights + (attn_out_weight, conv_out_weight)
     first = sum(w.shape[1] for w in weights[:3])
-    small = jnp.concatenate([conv_weight, channel_gain[None]], axis=0)
-    lam = jnp.pad(lambdas[None], ((0, small.shape[0] - 1), (0, WIDTH - heads)))
-    small = jnp.concatenate([small, lam], axis=1)
-    terms = []
-    for _ in range(3):
-        term = lax.reduce_precision(small, 8, 7)
-        small = small - term
-        terms.append(term.astype(BF))
     columns = sum(w.shape[1] for w in weights)
-    shard = lax.ppermute(jnp.concatenate(weights + tuple(terms), axis=1), PLANE, swap)
-    span = channels + WIDTH
-    small = sum(
-        shard[:, columns + i * span : columns + (i + 1) * span].astype(F32) for i in (2, 1, 0)
+    shard = lax.ppermute(jnp.concatenate(weights, axis=1), PLANE, swap)
+    small = jnp.concatenate(
+        [
+            conv_weight,
+            channel_gain[None],
+            jnp.pad(lambdas, (0, channels - heads))[None],
+            jnp.zeros((7, channels), F32),
+        ],
+        axis=0,
     )
-    shard = shard[:, :columns]
-    conv_weight, channel_gain = small[:CONV_W, :channels], small[CONV_W, :channels]
-    lambdas = small[0, channels : channels + heads]
+    small = lax.ppermute(small, PLANE, swap)
+    lambdas = small[CONV_W + 1, :heads]
 
     blocks = tokens.reshape(n, seg, tokens.shape[1])
     blocks = jnp.broadcast_to(blocks, (n, *blocks.shape)).reshape(n * n, seg, -1)
@@ -356,25 +388,23 @@
     att = combine(arrived, lambdas, head_gain, tok, heads)
 
     g_cols = glu_value_weight.shape[1]
-    glu = glu_of(core, normed, rest, rest_other, q_cols, g_cols, n)
+    t = lax.axis_index(TP).astype(jnp.int32)[None]
+    glu, heads_rows, tails, edge = glu_of(
+        core, t, normed, rest, rest_other, q_cols, g_cols, n
+    )
     size_z = lax.axis_size("z")
-    t = lax.axis_index(TP)
-    heads_rows, tails = glu[:, :REACH], glu[:, seg - REACH :]
     ring = [(i, (i + 1) % n) for i in range(n)]
     left = lax.ppermute(tails, TP, ring)
     right = lax.ppermute(heads_rows, TP, [(b, a) for a, b in ring])
     across = [(z * n + n - 1, (z + 1) * n) for z in range(size_z - 1)]
     across = [(z * n + n - 1, (z + 1) * n) for z in range(size_z - 1)]
     across = across + [(b, a) for a, b in across]
-    edge = jnp.where(t == 0, heads_rows[:1], tails[n - 1 :])
     edge = lax.ppermute(edge, TOK_RING, across)
-    conv_sum, squares = conv_of(t.astype(jnp.int32)[None], glu, left, right, edge, conv_weight)
-    squares = squares.reshape(n, seg)
-    squares = jnp.sum(copies_to(squares, "y"), axis=0)
-    scaled = conv_sum * lax.rsqrt(squares / C_CH + EPS)[..., None] * channel_gain
-    conv_out = jax.nn.silu(scaled).astype(BF).reshape(tok, g_cols)
-
-    term = out_of(core, att, conv_out, rest, rest_other, q_cols + 2 * g_cols, n)
+    conv_sum, squares = conv_of(t, glu, left, right, edge, small[:CONV_W])
+    squares = lax.all_to_all(squares, "y", 0, 0, tiled=True)
+    term = out_of(
+        core, att, conv_sum, squares, small[CONV_W], rest, rest_other, q_cols + 2 * g_cols
+    )
     reduced = lax.all_to_all(term, "y", 0, 0, tiled=True)
     return reduced.astype(F32).sum(axis=0).astype(BF)
 

time: 271 us -> 266 us (0.982)
  the two profiles are of different devices: /device:TPU:3 before, /device:TPU:1 now
where the time goes in v5:
time: 266 us; the launch traced here: 261 us
  blocking collectives  109 us (41%)
  starting transfers between devices  62.3 us (23%)
  waiting for transfers between devices  42.4 us (16%)
  Pallas kernels  33.6 us (13%)
  local copies, waits for them, and re-layouts  10.4 us (4%)
  other arithmetic  3.24 us (1%)
    all_to_all x1, blocking collectives, local(): rest = lax.all_to_all(rest, 'x', 0, 0, tiled=True)  31.2 us
    all_to_all x1, blocking collectives, local(): reduced = lax.all_to_all(term, 'y', 0, 0, tiled=True)  29.2 us
    all_gather x1, blocking collectives, local(): by_z = lax.all_gather(shard, 'z', axis=0)  27.1 us
    all_to_all x1, waiting for transfers between devices, local(): mine = lax.all_to_all(blocks, PLANE, 0, 0, tiled=True)  24.4 us
    all_gather x1, blocking collectives, local(): kv = lax.all_gather(kv, 'z', axis=0, tiled=True)  21.3 us
    pallas_call x1, Pallas kernels, attend(): pl.pallas_call(functools.partial(attend_kernel, tok=tok, rows=rows, keys=...  16.5 us
    all_to_all x1, starting transfers between devices, local(): mine = lax.all_to_all(blocks, PLANE, 0, 0, tiled=True)  14.9 us
    all_to_all x1, waiting for transfers between devices, copies_to(): return lax.all_to_all(copies, axis, 0, 0, tiled=True)  9.8 us
  transfers between devices with their start and end apart: 12, of which 7 were waited for; matrix products, arithmetic and copies ran while one was open for 3% of the time, Pallas kernels for 10%

profile of v5, /device:TPU:1, one launch (start us, length us, event | category | flops | bytes accessed | tf_op | source)
XLA Modules:
  0.0 260.9 jit_solution(17509067347583372881)
XLA Ops:
  0.0 0.9 concatenate.6
  0.9 8.8 %collective-permute-start = (bf16[32,1344]{1,0:T(8,128)(2,1)S(1)}, bf16[32,1344]{1,0:T(8,128)(2,1)S(1)}, u32[]{:S(2)}, u32[]{:S(2)}) collective-permute-start(bf16[32,1344]{1,0:T(8,128)(2,1)S(1)} %concatenate.6), channel_id=1, source_target_pairs={{0,0},{1,32},{2,8},{3,40},{4,16},{5,48},{6,24},{7,56},{8,1},{9,33}... | collective-permute-start | bytes 258056 | tf_op jit(solution)/shard_map/ppermute | solution.py:350
  9.7 1.5 collective-permute-done
  11.3 27.1 %all-gather = bf16[256,1344]{1,0:T(8,128)(2,1)S(1)} all-gather(bf16[32,1344]{1,0:T(8,128)(2,1)S(1)} %collective-permute-done), channel_id=2, replica_groups=mesh['z'=8,'y'=8,'x'=4,'c'=2] {'z'}, dimensions={0}, use_global_device_ids=true | all-gather | bytes 774144 | tf_op jit(solution)/shard_map/all_gather | solution.py:370
  38.4 1.1 broadcast_in_dim.34
  39.5 5.5 %all-to-all-start.1 = ((bf16[4,256,512]{2,1,0:T(8,128)(2,1)}), bf16[4,256,512]{2,1,0:T(8,128)(2,1)}, u32[]{:S(2)}, u32[]{:S(2)}) async-start(bf16[4,256,512]{2,1,0:T(8,128)(2,1)} %broadcast_in_dim.34), calls=%async_computation.1 | async-start | bytes 2097152 | tf_op jit(solution)/shard_map/all_to_all | solution.py:36
  45.0 9.8 %all-to-all-done.1.own_ref = bf16[4,256,512]{2,1,0:T(8,128)(2,1)} async-done(((bf16[4,256,512]{2,1,0:T(8,128)(2,1)}), bf16[4,256,512]{2,1,0:T(8,128)(2,1)}, u32[]{:S(2)}, u32[]{:S(2)}) %all-to-all-start.1) | async-done | bytes 1048608 | tf_op jit(solution)/shard_map/all_to_all | solution.py:36
  54.8 1.1 broadcast_in_dim.33
  55.9 14.9 %all-to-all-start = ((bf16[64,28,256]{2,1,0:T(8,128)(2,1)}), bf16[64,28,256]{2,1,0:T(8,128)(2,1)S(1)}, u32[]{:S(2)}, u32[]{:S(2)}) async-start(bf16[64,28,256]{2,1,0:T(8,128)(2,1)} %bitcast.1), calls=%async_computation | async-start | bytes 2097152 | tf_op jit(solution)/shard_map/all_to_all | solution.py:365
  72.2 2.4 collective-permute-start.1
  74.5 24.4 %all-to-all-done = bf16[64,28,256]{2,1,0:T(8,128)(2,1)S(1)} async-done(((bf16[64,28,256]{2,1,0:T(8,128)(2,1)}), bf16[64,28,256]{2,1,0:T(8,128)(2,1)S(1)}, u32[]{:S(2)}, u32[]{:S(2)}) %all-to-all-start) | async-done | bytes 917536 | tf_op jit(solution)/shard_map/all_to_all | solution.py:365
  99.7 0.7 copy.24
  101.2 1.2 multiply_convert_fusion.x_ref
  102.4 1.6 broadcast_in_dim.35._
  104.0 3.5 %qkv.1 = (bf16[4,256,1152]{2,1,0:T(8,128)(2,1)}, bf16[224,256]{1,0:T(8,128)(2,1)}) custom-call(s32[1]{0:T(128)} %bitcast.core_ref, bf16[224,2048]{1,0:T(8,128)(2,1)} %multiply_convert_fusion.x_ref, bf16[4,256,512]{2,1,0:T(8,128)(2,1)} %all-to-all-done.1.own_ref, ...), custom_call_target="tpu_custom_call", output_to_operand_aliasing={{0}: (6, {})} | custom-call | tf_op jit(solution)/shard_map/qkv/pallas_call | solution.py:192
  107.6 31.2 %all_to_all.30.qs_ref.own_ref = bf16[4,256,1152]{2,1,0:T(8,128)(2,1)S(1)} all-to-all(bf16[4,256,1152]{2,1,0:T(8,128)(2,1)} %get-tuple-element.13), channel_id=1, replica_groups=mesh['z'=8,'y'=8,'x'=4,'c'=2] {'x'}, dimensions={0} | all-to-all | bytes 4718592 | tf_op jit(solution)/shard_map/all_to_all | solution.py:382
  138.7 4.6 %collective-permute-start.4 = (bf16[4,256,1152]{2,1,0:T(8,128)(2,1)S(1)}, bf16[4,256,1152]{2,1,0:T(8,128)(2,1)}, u32[]{:S(2)}, u32[]{:S(2)}) collective-permute-start(bf16[4,256,1152]{2,1,0:T(8,128)(2,1)S(1)} %all_to_all.30.qs_ref.own_ref), channel_id=1, source_target_pairs={{0,1},{1,0},{2,3},{3,2},{4,5},{5,4},{6,7},{7,6},{8,9},{9,8},{10,11... | collective-permute-start | bytes 7077896 | tf_op jit(solution)/shard_map/ppermute | solution.py:385
  143.3 21.3 %all_gather.11.k0_ref.v0_ref = bf16[1792,256]{1,0:T(8,128)(2,1)S(1)} all-gather(bf16[224,256]{1,0:T(8,128)(2,1)S(1)} %copy-done.5), channel_id=1, replica_groups=mesh['z'=8,'y'=8,'x'=4,'c'=2] {'z'}, dimensions={0}, use_global_device_ids=true | all-gather | bytes 1032192 | tf_op jit(solution)/shard_map/all_gather | solution.py:383
  164.6 7.4 %collective-permute-start.2 = (bf16[1792,256]{1,0:T(8,128)(2,1)S(1)}, bf16[1792,256]{1,0:T(8,128)(2,1)}, u32[]{:S(2)}, u32[]{:S(2)}) collective-permute-start(bf16[1792,256]{1,0:T(8,128)(2,1)S(1)} %all_gather.11.k0_ref.v0_ref), channel_id=1, source_target_pairs={{0,1},{1,0},{2,3},{3,2},{4,5},{5,4},{6,7},{7,6},{8,9},{9,8},{10,11... | collective-permute-start | bytes 2752520 | tf_op jit(solution)/shard_map/ppermute | solution.py:384
  172.0 2.0 collective-permute-done.2.k1_ref.v1_ref
  174.0 16.5 %attend.1 = bf16[4,912,128]{2,1,0:T(8,128)(2,1)} custom-call(bf16[4,256,1152]{2,1,0:T(8,128)(2,1)} %copy-done, bf16[1792,256]{1,0:T(8,128)(2,1)} %copy-done.2, bf16[1792,256]{1,0:T(8,128)(2,1)} %copy-done.2, bf16[1792,256]{1,0:T(8,128)(2,1)} %collective-permute-done.2.k1_ref.v1_ref, bf16[1792,256]{1,0:T(8,128)(2,1)} %collective-permute-done.2.k1_ref.v1_ref), custom_call_target="tpu_custom_call" | custom-call | flops 9865003008 | bytes 3670016 | tf_op jit(solution)/shard_map/attend/pallas_call | solution.py:97
  190.5 3.6 %all-to-all-start.3 = ((bf16[4,912,128]{2,1,0:T(8,128)(2,1)}), bf16[4,912,128]{2,1,0:T(8,128)(2,1)S(1)}, u32[]{:S(2)}, u32[]{:S(2)}) async-start(bf16[4,912,128]{2,1,0:T(8,128)(2,1)} %attend.1), calls=%async_computation.3 | async-start | bytes 1867776 | tf_op jit(solution)/shard_map/all_to_all | solution.py:387
  194.3 4.1 %glu.1 = (bf16[8,28,192]{2,1,0:T(8,128)(2,1)}, bf16[8,15,192]{2,1,0:T(8,128)(2,1)}, bf16[8,15,192]{2,1,0:T(8,128)(2,1)}, bf16[1,15,192]{2,1,0:T(8,128)(2,1)}) custom-call(s32[1]{0:T(128)} %bitcast.core_ref, s32[1]{0:T(128)} %bitcast.9.t_ref, bf16[224,2048]{1,0:T(8,128)(2,1)} %multiply_convert_fusion.x_ref, bf16[4,256,1152]{2,1,0:T(8,128)(2,1)} %copy-done, ...), custom_call_target="tpu_custom_call" | custom-call | tf_op jit(solution)/shard_map/glu/pallas_call | solution.py:225
  198.4 1.9 collective-permute-start.5
  200.4 5.0 %collective-permute-start.3 = (f32[40,192]{1,0:T(8,128)S(1)}, f32[40,192]{1,0:T(8,128)S(1)}, u32[]{:S(2)}, u32[]{:S(2)}) collective-permute-start(f32[40,192]{1,0:T(8,128)S(1)} %maximum_maximum_fusion), channel_id=1, source_target_pairs={{0,0},{1,32},{2,8},{3,40},{4,16},{5,48},{6,24},{7,56},{8,1},{9,33}... | collective-permute-start | bytes 92168 | tf_op jit(solution)/shard_map/ppermute | solution.py:360
  208.4 3.0 %conv.1 = (f32[8,28,192]{2,1,0:T(8,128)}, f32[8,8,128]{2,1,0:T(8,128)}) custom-call(s32[1]{0:T(128)} %bitcast.9.t_ref, bf16[8,28,192]{2,1,0:T(8,128)(2,1)} %get-tuple-element.15.glu_ref, bf16[8,15,192]{2,1,0:T(8,128)(2,1)} %copy-done.6, bf16[8,15,192]{2,1,0:T(8,128)(2,1)} %copy-done.7, bf16[1,15,192]{2,1,0:T(8,128)(2,1)} %copy-done.10, f32[31,192]{1,0:T(8,128)} %slice.23.w_ref), custom_call_target="tpu_custom_call" | custom-call | tf_op jit(solution)/shard_map/conv/pallas_call | solution.py:272
  211.4 7.6 %all-to-all-start.4 = ((f32[8,8,128]{2,1,0:T(8,128)}), f32[8,8,128]{2,1,0:T(8,128)S(1)}, u32[]{:S(2)}, u32[]{:S(2)}) async-start(f32[8,8,128]{2,1,0:T(8,128)} %get-tuple-element.20), calls=%async_computation.4 | async-start | bytes 65536 | tf_op jit(solution)/shard_map/all_to_all | solution.py:404
  220.2 2.1 combine.1.att_ref
  222.3 3.5 %all-to-all-done.4.sq_ref = f32[8,8,128]{2,1,0:T(8,128)S(1)} async-done(((f32[8,8,128]{2,1,0:T(8,128)}), f32[8,8,128]{2,1,0:T(8,128)S(1)}, u32[]{:S(2)}, u32[]{:S(2)}) %all-to-all-start.4) | async-done | bytes 32800 | tf_op jit(solution)/shard_map/all_to_all | solution.py:404
  226.4 4.4 %out.1 = bf16[8,28,2048]{2,1,0:T(8,128)(2,1)} custom-call(s32[1]{0:T(128)} %bitcast.core_ref, bf16[224,256]{1,0:T(8,128)(2,1)} %combine.1.att_ref, f32[8,28,192]{2,1,0:T(8,128)} %get-tuple-element.19.conv_ref, f32[8,8,128]{2,1,0:T(8,128)} %copy-done.3, f32[1,192]{1,0:T(1,128)} %slice.24.gain_ref, bf16[4,256,1152]{2,1,0:T(8,128)(2,1)} %copy-done, ...), custom_call_target="tpu_custom_call" | custom-call | tf_op jit(solution)/shard_map/out/pallas_call | solution.py:311
  230.9 29.2 %all_to_all.31 = bf16[8,28,2048]{2,1,0:T(8,128)(2,1)S(1)} all-to-all(bf16[8,28,2048]{2,1,0:T(8,128)(2,1)} %out.1), channel_id=1, replica_groups=mesh['z'=8,'y'=8,'x'=4,'c'=2] {'y'}, dimensions={0} | all-to-all | bytes 1835008 | tf_op jit(solution)/shard_map/all_to_all | solution.py:408
  260.1 0.8 reduce_sum.31
  (64 shorter events, 7.9 us)
Async XLA Ops:
  0.9 10.4 %collective-permute-start = (bf16[32,1344]{1,0:T(8,128)(2,1)S(1)}, bf16[32,1344]{1,0:T(8,128)(2,1)S(1)}, u32[]{:S(2)}, u32[]{:S(2)}) collective-permute-start(bf16[32,1344]{1,0:T(8,128)(2,1)S(1)} %concatenate.6), channel_id=1, source_target_pairs={{0,0},{1,32},{2,8},{3,40},{4,16},{5,48},{6,24},{7,56},{8,1},{9,33}... | collective-permute-start | bytes 258056 | tf_op jit(solution)/shard_map/ppermute | solution.py:350
  38.4 6.6 %copy-start.4 = (bf16[224,256]{1,0:T(8,128)(2,1)S(1)}, bf16[224,256]{1,0:T(8,128)(2,1)}, u32[]{:S(2)}) copy-start(bf16[224,256]{1,0:T(8,128)(2,1)} %param.15) | copy-start | bytes 344068
  39.5 15.3 %all-to-all-start.1 = ((bf16[4,256,512]{2,1,0:T(8,128)(2,1)}), bf16[4,256,512]{2,1,0:T(8,128)(2,1)}, u32[]{:S(2)}, u32[]{:S(2)}) async-start(bf16[4,256,512]{2,1,0:T(8,128)(2,1)} %broadcast_in_dim.34), calls=%async_computation.1 | async-start | bytes 2097152 | tf_op jit(solution)/shard_map/all_to_all | solution.py:36
  45.0 25.9 %copy-start.13 = (f32[64]{0:T(128)S(1)}, f32[64]{0:T(128)}, u32[]{:S(2)}) copy-start(f32[64]{0:T(128)} %param.22) | copy-start | bytes 772
  45.0 26.4 %copy-start.14 = (f32[64]{0:T(128)S(1)}, f32[64]{0:T(128)}, u32[]{:S(2)}) copy-start(f32[64]{0:T(128)} %param.23) | copy-start | bytes 772
  55.9 43.0 %all-to-all-start = ((bf16[64,28,256]{2,1,0:T(8,128)(2,1)}), bf16[64,28,256]{2,1,0:T(8,128)(2,1)S(1)}, u32[]{:S(2)}, u32[]{:S(2)}) async-start(bf16[64,28,256]{2,1,0:T(8,128)(2,1)} %bitcast.1), calls=%async_computation | async-start | bytes 2097152 | tf_op jit(solution)/shard_map/all_to_all | solution.py:365
  72.2 30.3 %collective-permute-start.1 = (bf16[4,256,512]{2,1,0:T(8,128)(2,1)}, bf16[4,256,512]{2,1,0:T(8,128)(2,1)}, u32[]{:S(2)}, u32[]{:S(2)}) collective-permute-start(bf16[4,256,512]{2,1,0:T(8,128)(2,1)} %all-to-all-done.1.own_ref), channel_id=1, source_target_pairs={{0,1},{1,0},{2,3},{3,2},{4,5},{5,4},{6,7},{7,6},{8,9},{9,8},{10,11... | collective-permute-start | bytes 3145736 | tf_op jit(solution)/shard_map/ppermute | solution.py:375
  99.7 1.6 copy-start.9
  107.6 35.7 %copy-start.5 = (bf16[224,256]{1,0:T(8,128)(2,1)S(1)}, bf16[224,256]{1,0:T(8,128)(2,1)}, u32[]{:S(2)}) copy-start(bf16[224,256]{1,0:T(8,128)(2,1)} %get-tuple-element.14) | copy-start | bytes 344068
  138.7 35.3 %copy-start = (bf16[4,256,1152]{2,1,0:T(8,128)(2,1)}, bf16[4,256,1152]{2,1,0:T(8,128)(2,1)S(1)}, u32[]{:S(2)}) copy-start(bf16[4,256,1152]{2,1,0:T(8,128)(2,1)S(1)} %all_to_all.30.qs_ref.own_ref) | copy-start | bytes 7077892
  138.7 55.6 %collective-permute-start.4 = (bf16[4,256,1152]{2,1,0:T(8,128)(2,1)S(1)}, bf16[4,256,1152]{2,1,0:T(8,128)(2,1)}, u32[]{:S(2)}, u32[]{:S(2)}) collective-permute-start(bf16[4,256,1152]{2,1,0:T(8,128)(2,1)S(1)} %all_to_all.30.qs_ref.own_ref), channel_id=1, source_target_pairs={{0,1},{1,0},{2,3},{3,2},{4,5},{5,4},{6,7},{7,6},{8,9},{9,8},{10,11... | collective-permute-start | bytes 7077896 | tf_op jit(solution)/shard_map/ppermute | solution.py:385
  164.6 9.5 %copy-start.2 = (bf16[1792,256]{1,0:T(8,128)(2,1)}, bf16[1792,256]{1,0:T(8,128)(2,1)S(1)}, u32[]{:S(2)}) copy-start(bf16[1792,256]{1,0:T(8,128)(2,1)S(1)} %all_gather.11.k0_ref.v0_ref) | copy-start | bytes 2752516
  164.6 9.5 %collective-permute-start.2 = (bf16[1792,256]{1,0:T(8,128)(2,1)S(1)}, bf16[1792,256]{1,0:T(8,128)(2,1)}, u32[]{:S(2)}, u32[]{:S(2)}) collective-permute-start(bf16[1792,256]{1,0:T(8,128)(2,1)S(1)} %all_gather.11.k0_ref.v0_ref), channel_id=1, source_target_pairs={{0,1},{1,0},{2,3},{3,2},{4,5},{5,4},{6,7},{7,6},{8,9},{9,8},{10,11... | collective-permute-start | bytes 2752520 | tf_op jit(solution)/shard_map/ppermute | solution.py:384
  190.5 3.7 %copy-start.12 = (f32[2]{0:T(128)S(1)}, f32[2]{0:T(128)}, u32[]{:S(2)}) copy-start(f32[2]{0:T(128)} %param.24) | copy-start | bytes 28
  190.5 20.9 %all-to-all-start.3 = ((bf16[4,912,128]{2,1,0:T(8,128)(2,1)}), bf16[4,912,128]{2,1,0:T(8,128)(2,1)S(1)}, u32[]{:S(2)}, u32[]{:S(2)}) async-start(bf16[4,912,128]{2,1,0:T(8,128)(2,1)} %attend.1), calls=%async_computation.3 | async-start | bytes 1867776 | tf_op jit(solution)/shard_map/all_to_all | solution.py:387
  194.3 6.0 %copy-start.8 = (f32[31,192]{1,0:T(8,128)S(1)}, f32[31,192]{1,0:T(8,128)}, u32[]{:S(2)}) copy-start(f32[31,192]{1,0:T(8,128)} %param.26) | copy-start | bytes 71428
  194.3 6.0 %copy-start.11 = (f32[192]{0:T(256)S(1)}, f32[192]{0:T(256)}, u32[]{:S(2)}) copy-start(f32[192]{0:T(256)} %param.27) | copy-start | bytes 2308
  198.4 9.0 %collective-permute-start.5 = (bf16[8,15,192]{2,1,0:T(8,128)(2,1)}, bf16[8,15,192]{2,1,0:T(8,128)(2,1)S(1)}, u32[]{:S(2)}, u32[]{:S(2)}) collective-permute-start(bf16[8,15,192]{2,1,0:T(8,128)(2,1)} %get-tuple-element.16), channel_id=1, source_target_pairs={{0,1},{1,2},{2,3},{3,4},{4,5},{5,6},{6,7},{7,0},{8,9},{9,10},{10,1... | collective-permute-start | bytes 138248 | tf_op jit(solution)/shard_map/ppermute | solution.py:397
  200.3 7.5 %collective-permute-start.6 = (bf16[8,15,192]{2,1,0:T(8,128)(2,1)}, bf16[8,15,192]{2,1,0:T(8,128)(2,1)S(1)}, u32[]{:S(2)}, u32[]{:S(2)}) collective-permute-start(bf16[8,15,192]{2,1,0:T(8,128)(2,1)} %get-tuple-element.17), channel_id=1, source_target_pairs={{1,0},{2,1},{3,2},{4,3},{5,4},{6,5},{7,6},{0,7},{9,8},{10,9},{11,1... | collective-permute-start | bytes 138248 | tf_op jit(solution)/shard_map/ppermute | solution.py:398
  200.4 6.4 %collective-permute-start.3 = (f32[40,192]{1,0:T(8,128)S(1)}, f32[40,192]{1,0:T(8,128)S(1)}, u32[]{:S(2)}, u32[]{:S(2)}) collective-permute-start(f32[40,192]{1,0:T(8,128)S(1)} %maximum_maximum_fusion), channel_id=1, source_target_pairs={{0,0},{1,32},{2,8},{3,40},{4,16},{5,48},{6,24},{7,56},{8,1},{9,33}... | collective-permute-start | bytes 92168 | tf_op jit(solution)/shard_map/ppermute | solution.py:360
  205.4 2.0 collective-permute-start.7
  207.4 0.6 copy-start.10
  207.4 0.6 copy-start.6
  207.8 0.6 copy-start.7
  211.4 8.8 %copy-start.1 = (bf16[4,912,128]{2,1,0:T(8,128)(2,1)}, bf16[4,912,128]{2,1,0:T(8,128)(2,1)S(1)}, u32[]{:S(2)}) copy-start(bf16[4,912,128]{2,1,0:T(8,128)(2,1)S(1)} %all-to-all-done.3.parts_ref) | copy-start | bytes 2801668
  211.4 14.4 %all-to-all-start.4 = ((f32[8,8,128]{2,1,0:T(8,128)}), f32[8,8,128]{2,1,0:T(8,128)S(1)}, u32[]{:S(2)}, u32[]{:S(2)}) async-start(f32[8,8,128]{2,1,0:T(8,128)} %get-tuple-element.20), calls=%async_computation.4 | async-start | bytes 65536 | tf_op jit(solution)/shard_map/all_to_all | solution.py:404
  225.8 0.6 copy-start.3

commit v6 on v5

--- a/solution.py
+++ b/solution.py
@@ -21,6 +21,8 @@
 TP = ("x", "c")
 PLANE = ("y", "x", "c")
 TOK_RING = ("z", "x", "c")
+SMEM = pl.BlockSpec(memory_space=pltpu.SMEM)
+VMEM = pl.BlockSpec(memory_space=pltpu.VMEM)
 
 
 def rms_scale(values, gain):
@@ -39,6 +41,56 @@
 def diagonal(size):
     rows = lax.broadcasted_iota(jnp.int32, (size, size), 0)
     return rows == lax.broadcasted_iota(jnp.int32, (size, size), 1)
+
+
+def pack_kernel(x_ref, out_ref):
+    seg = out_ref.shape[1] // 2
+    n = x_ref.shape[0] // seg
+    for t in range(n):
+        rows = x_ref[seg * t : seg * t + seg, :]
+        for y in range(n):
+            out_ref[n * y + t, :seg, :] = rows[:, :WIDTH]
+            out_ref[n * y + t, seg:, :] = rows[:, WIDTH:]
+
+
+def norm_kernel(x_ref, gain_ref, out_ref):
+    n = out_ref.shape[1] // (2 * WIDTH)
+    seg = x_ref.shape[1] // 2
+    for y in range(out_ref.shape[0] // seg):
+        blocks = []
+        for t in range(n):
+            block = x_ref[n * y + t].astype(F32)
+            blocks += [block[:seg], block[seg:]]
+        squares = blocks[0] * blocks[0]
+        for block in blocks[1:]:
+            squares = squares + block * block
+        mean = jnp.sum(squares, axis=1, keepdims=True) / out_ref.shape[1]
+        scale = lax.rsqrt(mean + EPS)
+        for b, block in enumerate(blocks):
+            cols = slice(WIDTH * b, WIDTH * b + WIDTH)
+            normed = block * scale * gain_ref[:, cols]
+            out_ref[seg * y : seg * y + seg, cols] = normed.astype(BF)
+
+
+def pack(tokens, n):
+    tok, _ = tokens.shape
+    return pl.pallas_call(
+        pack_kernel,
+        in_specs=[VMEM],
+        out_specs=VMEM,
+        out_shape=jax.ShapeDtypeStruct((n * n, 2 * tok // n, WIDTH), BF),
+        name="pack",
+    )(tokens)
+
+
+def norm_of(blocks, gain, n):
+    return pl.pallas_call(
+        norm_kernel,
+        in_specs=[VMEM, VMEM],
+        out_specs=VMEM,
+        out_shape=jax.ShapeDtypeStruct((n * blocks.shape[1] // 2, gain.shape[0]), BF),
+        name="norm",
+    )(blocks, gain[None])
 
 
 def attend_kernel(
@@ -97,7 +149,7 @@
     return pl.pallas_call(
         functools.partial(attend_kernel, tok=tok, rows=rows, keys=keys),
         grid=(total // block,),
-        in_specs=[pl.BlockSpec((groups, packed.shape[1], cols), lambda i: (0, 0, 0))] + half + half,
+        in_specs=[pl.BlockSpec((groups, packed.shape[1], cols), lambda i: (0, 0, 2))] + half + half,
         out_specs=pl.BlockSpec((groups, each + 16, WIDTH), lambda i: (0, 0, 0)),
         out_shape=jax.ShapeDtypeStruct((groups, each + 16, WIDTH), BF),
         scratch_shapes=[pltpu.VMEM((count, 2 * WIDTH), F32), pltpu.VMEM((count, WIDTH), BF)],
@@ -183,17 +235,13 @@
     kv_ref[:, WIDTH:] = acc[:, q_cols + WIDTH :].astype(BF)
 
 
-SMEM = pl.BlockSpec(memory_space=pltpu.SMEM)
-VMEM = pl.BlockSpec(memory_space=pltpu.VMEM)
-
-
 def qkv(core, x, own, other, query_gain, key_gain, packed):
     tok, q_cols = x.shape[0], own.shape[2] - 2 * WIDTH
     return pl.pallas_call(
         qkv_kernel,
         grid=(1,),
         in_specs=[SMEM] + [VMEM] * 5 + [pl.BlockSpec(memory_space=pl.ANY)],
-        out_specs=[pl.BlockSpec((*packed.shape[:2], q_cols), lambda i: (0, 0, 0)), VMEM],
+        out_specs=[pl.BlockSpec((*packed.shape[:2], q_cols), lambda i: (0, 0, 2)), VMEM],
         out_shape=[
             jax.ShapeDtypeStruct(packed.shape, BF),
             jax.ShapeDtypeStruct((tok, 2 * WIDTH), BF),
@@ -204,10 +252,10 @@
 
 
 def glu_kernel(
-    core_ref, t_ref, x_ref, own_ref, other_ref, out_ref, head_ref, tail_ref, edge_ref, *, start
+    core_ref, t_ref, x_ref, own_ref, other_ref, out_ref, head_ref, tail_ref, edge_ref
 ):
     n, seg, channels = out_ref.shape
-    cols = slice(start, start + 2 * channels)
+    cols = slice(0, 2 * channels)
     acc = project(core_ref[0], x_ref, own_ref, other_ref, cols)
     value, gate = acc[:, :channels], acc[:, channels:]
     glu = value * (1.0 / (1.0 + jnp.exp(-gate)))
@@ -220,11 +268,14 @@
     edge_ref[0] = jnp.where(t_ref[0] == 0, first, last).astype(BF)
 
 
-def glu_of(core, t, x, own, other, start, channels, n):
+def glu_of(core, t, x, own, other, channels, n):
     reach = jax.ShapeDtypeStruct((n, REACH, channels), BF)
     return pl.pallas_call(
-        functools.partial(glu_kernel, start=start),
-        in_specs=[SMEM] * 2 + [VMEM] * 3,
+        glu_kernel,
+        grid=(1,),
+        in_specs=[SMEM] * 2
+        + [VMEM]
+        + [pl.BlockSpec((*own.shape[:2], 2 * channels), lambda i: (0, 0, 2))] * 2,
         out_specs=[VMEM] * 4,
         out_shape=[
             jax.ShapeDtypeStruct((n, x.shape[0] // n, channels), BF),
@@ -283,11 +334,10 @@
 
 
 def out_kernel(
-    core_ref, att_ref, conv_ref, sq_ref, gain_ref, own_ref, other_ref, out_ref, act_ref, *, start
+    core_ref, att_ref, conv_ref, sq_ref, gain_ref, own_ref, other_ref, out_ref, act_ref
 ):
-    n, seg, _ = out_ref.shape
-    channels = conv_ref.shape[2]
-    cols = slice(start, start + att_ref.shape[1] + channels)
+    n, seg, channels = conv_ref.shape
+    cols = slice(0, att_ref.shape[1] + channels)
     squares = sq_ref[0]
     for g in range(1, n):
         squares = squares + sq_ref[g]
@@ -301,21 +351,44 @@
         rhs = natural_rows(core_ref[0], own_ref, other_ref, z, cols)
         term = contract_last(act, rhs)
         for y in range(n):
-            block = term[seg * y : seg * y + seg]
-            out_ref[y, :, 256 * z : 256 * z + 256] = block.astype(BF)
-
-
-def out_of(core, att, conv, squares, gain, own, other, start):
+            block = term[seg * y : seg * y + seg].astype(BF)
+            at = 2 * z * seg
+            out_ref[y, at : at + seg, :] = block[:, :WIDTH]
+            out_ref[y, at + seg : at + 2 * seg, :] = block[:, WIDTH:]
+
+
+def out_of(core, att, conv, squares, gain, own, other, pad):
     n, seg, channels = conv.shape
     width = own.shape[0] * own.shape[1] * 2
-    return pl.pallas_call(
-        functools.partial(out_kernel, start=start),
-        in_specs=[SMEM] + [VMEM] * 6,
+    late = (*own.shape[:2], att.shape[1] + channels + pad)
+    return pl.pallas_call(
+        out_kernel,
+        grid=(1,),
+        in_specs=[SMEM] + [VMEM] * 4 + [pl.BlockSpec(late, lambda i: (0, 0, 0))] * 2,
         out_specs=VMEM,
-        out_shape=jax.ShapeDtypeStruct((n, seg, width), BF),
+        out_shape=jax.ShapeDtypeStruct((n, seg * width // WIDTH, WIDTH), BF),
         scratch_shapes=[pltpu.VMEM((n * seg, channels), F32)],
         name="out",
     )(core, att, conv, squares, gain[None], own, other)
+
+
+def sum_kernel(x_ref, out_ref):
+    seg = out_ref.shape[0]
+    for b in range(out_ref.shape[1] // WIDTH):
+        total = x_ref[0, seg * b : seg * b + seg, :].astype(F32)
+        for g in range(1, x_ref.shape[0]):
+            total = total + x_ref[g, seg * b : seg * b + seg, :].astype(F32)
+        out_ref[:, WIDTH * b : WIDTH * b + WIDTH] = total.astype(BF)
+
+
+def sum_of(parts, seg):
+    return pl.pallas_call(
+        sum_kernel,
+        in_specs=[VMEM],
+        out_specs=VMEM,
+        out_shape=jax.ShapeDtypeStruct((seg, parts.shape[1] // seg * WIDTH), BF),
+        name="sum",
+    )(parts)
 
 
 def local(
@@ -360,12 +433,9 @@
     small = lax.ppermute(small, PLANE, swap)
     lambdas = small[CONV_W + 1, :heads]
 
-    blocks = tokens.reshape(n, seg, tokens.shape[1])
-    blocks = jnp.broadcast_to(blocks, (n, *blocks.shape)).reshape(n * n, seg, -1)
+    blocks = pack(tokens, n)
     mine = lax.all_to_all(blocks, PLANE, 0, 0, tiled=True)
-    mine = mine.reshape(n, n, seg, -1)
-    gathered = mine.transpose(0, 2, 1, 3).reshape(n, seg, -1).astype(F32)
-    normed = rms_scale(gathered, norm_gain).astype(BF).reshape(tok, -1)
+    normed = norm_of(mine, norm_gain, n)
 
     by_z = lax.all_gather(shard, "z", axis=0)
     core = lax.axis_index("c").astype(jnp.int32)[None]
@@ -375,8 +445,11 @@
     wa_other = lax.ppermute(wa, "c", mates)
     fold = math.log2(math.e) * HEAD_DIM ** (-0.5)
     q_cols = query_weight.shape[1]
-    late = columns - first
-    rest = jnp.pad(by_z[:, first:], ((0, 0), (q_cols, -(q_cols + late) % WIDTH)))
+    g_cols = glu_value_weight.shape[1]
+    late = first + 2 * g_cols
+    pad = -(columns - late) % q_cols
+    gap = jnp.zeros((by_z.shape[0], pad + q_cols), BF)
+    rest = jnp.concatenate([by_z[:, late:], gap, by_z[:, first:late]], axis=1)
     rest = jnp.broadcast_to(rest, (lax.axis_size("x"), *rest.shape))
     rest, kv = qkv(core, normed, wa, wa_other, query_gain * fold, key_gain, rest)
     rest = lax.all_to_all(rest, "x", 0, 0, tiled=True)
@@ -387,10 +460,9 @@
     arrived = lax.all_to_all(parts, "x", 0, 0, tiled=True)
     att = combine(arrived, lambdas, head_gain, tok, heads)
 
-    g_cols = glu_value_weight.shape[1]
     t = lax.axis_index(TP).astype(jnp.int32)[None]
     glu, heads_rows, tails, edge = glu_of(
-        core, t, normed, rest, rest_other, q_cols, g_cols, n
+        core, t, normed, rest, rest_other, g_cols, n
     )
     size_z = lax.axis_size("z")
     ring = [(i, (i + 1) % n) for i in range(n)]
@@ -403,10 +475,10 @@
     conv_sum, squares = conv_of(t, glu, left, right, edge, small[:CONV_W])
     squares = lax.all_to_all(squares, "y", 0, 0, tiled=True)
     term = out_of(
-        core, att, conv_sum, squares, small[CONV_W], rest, rest_other, q_cols + 2 * g_cols
+        core, att, conv_sum, squares, small[CONV_W], rest, rest_other, pad
     )
     reduced = lax.all_to_all(term, "y", 0, 0, tiled=True)
-    return reduced.astype(F32).sum(axis=0).astype(BF)
+    return sum_of(reduced, seg)
 
 
 def solution(mesh):

time: 266 us -> 259 us (0.974)
  Pallas kernels: 33.6 us -> 38.4 us
  waiting for transfers between devices: 42.4 us -> 38.5 us
  other arithmetic: 3.24 us -> 0.08 us
    pallas_call x2 -> x5, Pallas kernels: 8.52 us -> 13.3 us  [the longest x1 3.55 us: out_of(): pl.pallas_call(out_kernel, grid=(1,), in_specs=[SMEM] + [VMEM] * 4 + [pl....]
    all_to_all x1, waiting for transfers between devices: 24.4 us -> 21.5 us  [local(): mine = lax.all_to_all(blocks, PLANE, 0, 0, tiled=True)]
  transfers between devices with their start and end apart: 12 -> 12, of which waited for: 7 -> 7; matrix products, arithmetic and copies ran while one was open for 3% -> 1% of each run, Pallas kernels for 10% -> 12%
where the time goes in v6:
time: 259 us; the launch traced here: 255 us
  blocking collectives  107 us (41%)
  starting transfers between devices  61.2 us (24%)
  waiting for transfers between devices  38.5 us (15%)
  Pallas kernels  38.4 us (15%)
  local copies, waits for them, and re-layouts  9.38 us (4%)
    all_to_all x1, blocking collectives, local(): rest = lax.all_to_all(rest, 'x', 0, 0, tiled=True)  31.3 us
    all_to_all x1, blocking collectives, local(): reduced = lax.all_to_all(term, 'y', 0, 0, tiled=True)  27.4 us
    all_gather x1, blocking collectives, local(): by_z = lax.all_gather(shard, 'z', axis=0)  27.1 us
    all_to_all x1, waiting for transfers between devices, local(): mine = lax.all_to_all(blocks, PLANE, 0, 0, tiled=True)  21.5 us
    all_gather x1, blocking collectives, local(): kv = lax.all_gather(kv, 'z', axis=0, tiled=True)  21.3 us
    pallas_call x1, Pallas kernels, attend(): pl.pallas_call(functools.partial(attend_kernel, tok=tok, rows=rows, keys=...  16.5 us
    all_to_all x1, starting transfers between devices, local(): mine = lax.all_to_all(blocks, PLANE, 0, 0, tiled=True)  14.9 us
    ppermute x1, starting transfers between devices, local(): shard = lax.ppermute(jnp.concatenate(weights, axis=1), PLANE, swap)  8.83 us
  transfers between devices with their start and end apart: 12, of which 7 were waited for; matrix products, arithmetic and copies ran while one was open for 1% of the time, Pallas kernels for 12%

profile of v6, /device:TPU:1, one launch (start us, length us, event | category | flops | bytes accessed | tf_op | source)
XLA Modules:
  0.0 254.8 jit_solution(16825367374490232165)
XLA Ops:
  0.9 8.8 %collective-permute-start = (bf16[32,1344]{1,0:T(8,128)(2,1)S(1)}, bf16[32,1344]{1,0:T(8,128)(2,1)S(1)}, u32[]{:S(2)}, u32[]{:S(2)}) collective-permute-start(bf16[32,1344]{1,0:T(8,128)(2,1)S(1)} %concatenate.9), channel_id=1, source_target_pairs={{0,0},{1,32},{2,8},{3,40},{4,16},{5,48},{6,24},{7,56},{8,1},{9,33}... | collective-permute-start | bytes 258056 | tf_op jit(solution)/shard_map/ppermute | solution.py:423
  9.7 1.5 collective-permute-done
  11.3 27.1 %all-gather = bf16[256,1344]{1,0:T(8,128)(2,1)S(1)} all-gather(bf16[32,1344]{1,0:T(8,128)(2,1)S(1)} %collective-permute-done), channel_id=2, replica_groups=mesh['z'=8,'y'=8,'x'=4,'c'=2] {'z'}, dimensions={0}, use_global_device_ids=true | all-gather | bytes 774144 | tf_op jit(solution)/shard_map/all_gather | solution.py:440
  38.4 1.1 broadcast_in_dim.35
  39.4 5.6 %all-to-all-start.1 = ((bf16[4,256,512]{2,1,0:T(8,128)(2,1)}), bf16[4,256,512]{2,1,0:T(8,128)(2,1)S(1)}, u32[]{:S(2)}, u32[]{:S(2)}) async-start(bf16[4,256,512]{2,1,0:T(8,128)(2,1)} %broadcast_in_dim.35), calls=%async_computation.1 | async-start | bytes 2097152 | tf_op jit(solution)/shard_map/all_to_all | solution.py:38
  45.1 2.0 pack.1
  47.0 7.8 %all-to-all-done.1.own_ref = bf16[4,256,512]{2,1,0:T(8,128)(2,1)S(1)} async-done(((bf16[4,256,512]{2,1,0:T(8,128)(2,1)}), bf16[4,256,512]{2,1,0:T(8,128)(2,1)S(1)}, u32[]{:S(2)}, u32[]{:S(2)}) %all-to-all-start.1) | async-done | bytes 1048608 | tf_op jit(solution)/shard_map/all_to_all | solution.py:38
  54.8 14.9 %all-to-all-start = ((bf16[64,56,128]{2,1,0:T(8,128)(2,1)}), bf16[64,56,128]{2,1,0:T(8,128)(2,1)S(1)}, u32[]{:S(2)}, u32[]{:S(2)}) async-start(bf16[64,56,128]{2,1,0:T(8,128)(2,1)} %pack.1), calls=%async_computation | async-start | bytes 1835008 | tf_op jit(solution)/shard_map/all_to_all | solution.py:437
  69.7 2.4 collective-permute-start.1
  73.8 21.5 %all-to-all-done.x_ref = bf16[64,56,128]{2,1,0:T(8,128)(2,1)S(1)} async-done(((bf16[64,56,128]{2,1,0:T(8,128)(2,1)}), bf16[64,56,128]{2,1,0:T(8,128)(2,1)S(1)}, u32[]{:S(2)}, u32[]{:S(2)}) %all-to-all-start) | async-done | bytes 917536 | tf_op jit(solution)/shard_map/all_to_all | solution.py:437
  95.3 0.9 copy-done.3
  96.2 2.7 %norm.1.x_ref = bf16[224,2048]{1,0:T(8,128)(2,1)} custom-call(bf16[64,56,128]{2,1,0:T(8,128)(2,1)} %copy-done.3, f32[1,2048]{1,0:T(1,128)} %bitcast.8), custom_call_target="tpu_custom_call" | custom-call | tf_op jit(solution)/shard_map/norm/pallas_call | solution.py:87
  98.9 1.6 broadcast_in_dim.37._
  100.5 3.5 %qkv.1 = (bf16[4,256,1152]{2,1,0:T(8,128)(2,1)}, bf16[224,256]{1,0:T(8,128)(2,1)}) custom-call(s32[1]{0:T(128)} %bitcast.core_ref, bf16[224,2048]{1,0:T(8,128)(2,1)} %norm.1.x_ref, bf16[4,256,512]{2,1,0:T(8,128)(2,1)} %copy-done.1, bf16[4,256,512]{2,1,0:T(8,128)(2,1)} %collective-permute-done.1.other_ref, ...), custom_call_target="tpu_custom_call", output_to_operand_aliasing={{0}: (6, {})} | custom-call | tf_op jit(solution)/shard_map/qkv/pallas_call | solution.py:240
  104.1 31.3 %all_to_all.30.qs_ref.own_ref = bf16[4,256,1152]{2,1,0:T(8,128)(2,1)S(1)} all-to-all(bf16[4,256,1152]{2,1,0:T(8,128)(2,1)} %get-tuple-element.13), channel_id=1, replica_groups=mesh['z'=8,'y'=8,'x'=4,'c'=2] {'x'}, dimensions={0} | all-to-all | bytes 4718592 | tf_op jit(solution)/shard_map/all_to_all | solution.py:455
  135.3 4.5 %collective-permute-start.4 = (bf16[4,256,1152]{2,1,0:T(8,128)(2,1)S(1)}, bf16[4,256,1152]{2,1,0:T(8,128)(2,1)}, u32[]{:S(2)}, u32[]{:S(2)}) collective-permute-start(bf16[4,256,1152]{2,1,0:T(8,128)(2,1)S(1)} %all_to_all.30.qs_ref.own_ref), channel_id=1, source_target_pairs={{0,1},{1,0},{2,3},{3,2},{4,5},{5,4},{6,7},{7,6},{8,9},{9,8},{10,11... | collective-permute-start | bytes 7077896 | tf_op jit(solution)/shard_map/ppermute | solution.py:458
  139.8 21.3 %all_gather.11.k0_ref.v0_ref = bf16[1792,256]{1,0:T(8,128)(2,1)S(1)} all-gather(bf16[224,256]{1,0:T(8,128)(2,1)S(1)} %copy-done.6), channel_id=1, replica_groups=mesh['z'=8,'y'=8,'x'=4,'c'=2] {'z'}, dimensions={0}, use_global_device_ids=true | all-gather | bytes 1032192 | tf_op jit(solution)/shard_map/all_gather | solution.py:456
  161.1 7.6 %collective-permute-start.2 = (bf16[1792,256]{1,0:T(8,128)(2,1)S(1)}, bf16[1792,256]{1,0:T(8,128)(2,1)}, u32[]{:S(2)}, u32[]{:S(2)}) collective-permute-start(bf16[1792,256]{1,0:T(8,128)(2,1)S(1)} %all_gather.11.k0_ref.v0_ref), channel_id=1, source_target_pairs={{0,1},{1,0},{2,3},{3,2},{4,5},{5,4},{6,7},{7,6},{8,9},{9,8},{10,11... | collective-permute-start | bytes 2752520 | tf_op jit(solution)/shard_map/ppermute | solution.py:457
  168.6 2.0 collective-permute-done.2.k1_ref.v1_ref
  170.7 16.5 %attend.1 = bf16[4,912,128]{2,1,0:T(8,128)(2,1)} custom-call(bf16[4,256,1152]{2,1,0:T(8,128)(2,1)} %copy-done, bf16[1792,256]{1,0:T(8,128)(2,1)} %copy-done.4, bf16[1792,256]{1,0:T(8,128)(2,1)} %copy-done.4, bf16[1792,256]{1,0:T(8,128)(2,1)} %collective-permute-done.2.k1_ref.v1_ref, bf16[1792,256]{1,0:T(8,128)(2,1)} %collective-permute-done.2.k1_ref.v1_ref), custom_call_target="tpu_custom_call" | custom-call | flops 9865003008 | bytes 3670016 | tf_op jit(solution)/shard_map/attend/pallas_call | solution.py:149
  187.1 3.5 %all-to-all-start.3 = ((bf16[4,912,128]{2,1,0:T(8,128)(2,1)}), bf16[4,912,128]{2,1,0:T(8,128)(2,1)S(1)}, u32[]{:S(2)}, u32[]{:S(2)}) async-start(bf16[4,912,128]{2,1,0:T(8,128)(2,1)} %attend.1), calls=%async_computation.3 | async-start | bytes 1867776 | tf_op jit(solution)/shard_map/all_to_all | solution.py:460
  190.8 3.1 %glu.1 = (bf16[8,28,192]{2,1,0:T(8,128)(2,1)}, bf16[8,15,192]{2,1,0:T(8,128)(2,1)}, bf16[8,15,192]{2,1,0:T(8,128)(2,1)}, bf16[1,15,192]{2,1,0:T(8,128)(2,1)}) custom-call(s32[1]{0:T(128)} %bitcast.core_ref, s32[1]{0:T(128)} %bitcast.6.t_ref, bf16[224,2048]{1,0:T(8,128)(2,1)} %norm.1.x_ref, bf16[4,256,1152]{2,1,0:T(8,128)(2,1)} %copy-done, ...), custom_call_target="tpu_custom_call" | custom-call | tf_op jit(solution)/shard_map/glu/pallas_call | solution.py:273
  193.9 1.9 collective-permute-start.5
  195.9 4.9 %collective-permute-start.3 = (f32[40,192]{1,0:T(8,128)S(1)}, f32[40,192]{1,0:T(8,128)S(1)}, u32[]{:S(2)}, u32[]{:S(2)}) collective-permute-start(f32[40,192]{1,0:T(8,128)S(1)} %maximum_maximum_fusion), channel_id=1, source_target_pairs={{0,0},{1,32},{2,8},{3,40},{4,16},{5,48},{6,24},{7,56},{8,1},{9,33}... | collective-permute-start | bytes 92168 | tf_op jit(solution)/shard_map/ppermute | solution.py:433
  202.8 1.5 collective-permute-done.6.right_ref
  204.9 3.0 %conv.1 = (f32[8,28,192]{2,1,0:T(8,128)}, f32[8,8,128]{2,1,0:T(8,128)}) custom-call(s32[1]{0:T(128)} %bitcast.6.t_ref, bf16[8,28,192]{2,1,0:T(8,128)(2,1)} %get-tuple-element.15.glu_ref, bf16[8,15,192]{2,1,0:T(8,128)(2,1)} %copy-done.7, bf16[8,15,192]{2,1,0:T(8,128)(2,1)} %copy-done.8, bf16[1,15,192]{2,1,0:T(8,128)(2,1)} %copy-done.10, f32[31,192]{1,0:T(8,128)} %slice.28.w_ref), custom_call_target="tpu_custom_call" | custom-call | tf_op jit(solution)/shard_map/conv/pallas_call | solution.py:323
  207.9 6.4 %all-to-all-start.4 = ((f32[8,8,128]{2,1,0:T(8,128)}), f32[8,8,128]{2,1,0:T(8,128)S(1)}, u32[]{:S(2)}, u32[]{:S(2)}) async-start(f32[8,8,128]{2,1,0:T(8,128)} %get-tuple-element.20), calls=%async_computation.4 | async-start | bytes 65536 | tf_op jit(solution)/shard_map/all_to_all | solution.py:476
  215.6 2.1 combine.1.att_ref
  217.7 3.5 %all-to-all-done.4.sq_ref = f32[8,8,128]{2,1,0:T(8,128)S(1)} async-done(((f32[8,8,128]{2,1,0:T(8,128)}), f32[8,8,128]{2,1,0:T(8,128)S(1)}, u32[]{:S(2)}, u32[]{:S(2)}) %all-to-all-start.4) | async-done | bytes 32800 | tf_op jit(solution)/shard_map/all_to_all | solution.py:476
  221.8 3.5 %out.1 = bf16[8,448,128]{2,1,0:T(8,128)(2,1)} custom-call(s32[1]{0:T(128)} %bitcast.core_ref, bf16[224,256]{1,0:T(8,128)(2,1)} %combine.1.att_ref, f32[8,28,192]{2,1,0:T(8,128)} %get-tuple-element.19.conv_ref, f32[8,8,128]{2,1,0:T(8,128)} %copy-done.5, f32[1,192]{1,0:T(1,128)} %slice.29.gain_ref, bf16[4,256,1152]{2,1,0:T(8,128)(2,1)} %copy-done, ...), custom_call_target="tpu_custom_call" | custom-call | tf_op jit(solution)/shard_map/out/pallas_call | solution.py:364
  225.3 27.4 %all_to_all.31.x_ref = bf16[8,448,128]{2,1,0:T(8,128)(2,1)} all-to-all(bf16[8,448,128]{2,1,0:T(8,128)(2,1)} %out.1), channel_id=1, replica_groups=mesh['z'=8,'y'=8,'x'=4,'c'=2] {'y'}, dimensions={0} | all-to-all | bytes 1835008 | tf_op jit(solution)/shard_map/all_to_all | solution.py:480
  252.8 2.0 sum.1
  (57 shorter events, 7.2 us)
Async XLA Ops:
  0.9 10.4 %collective-permute-start = (bf16[32,1344]{1,0:T(8,128)(2,1)S(1)}, bf16[32,1344]{1,0:T(8,128)(2,1)S(1)}, u32[]{:S(2)}, u32[]{:S(2)}) collective-permute-start(bf16[32,1344]{1,0:T(8,128)(2,1)S(1)} %concatenate.9), channel_id=1, source_target_pairs={{0,0},{1,32},{2,8},{3,40},{4,16},{5,48},{6,24},{7,56},{8,1},{9,33}... | collective-permute-start | bytes 258056 | tf_op jit(solution)/shard_map/ppermute | solution.py:423
  39.4 32.6 %copy-start.13 = (f32[64]{0:T(128)S(1)}, f32[64]{0:T(128)}, u32[]{:S(2)}) copy-start(f32[64]{0:T(128)} %param.22) | copy-start | bytes 772
  39.4 33.2 %copy-start.14 = (f32[64]{0:T(128)S(1)}, f32[64]{0:T(128)}, u32[]{:S(2)}) copy-start(f32[64]{0:T(128)} %param.23) | copy-start | bytes 772
  39.4 15.4 %all-to-all-start.1 = ((bf16[4,256,512]{2,1,0:T(8,128)(2,1)}), bf16[4,256,512]{2,1,0:T(8,128)(2,1)S(1)}, u32[]{:S(2)}, u32[]{:S(2)}) async-start(bf16[4,256,512]{2,1,0:T(8,128)(2,1)} %broadcast_in_dim.35), calls=%async_computation.1 | async-start | bytes 2097152 | tf_op jit(solution)/shard_map/all_to_all | solution.py:38
  54.8 44.1 %copy-start.1 = (bf16[4,256,512]{2,1,0:T(8,128)(2,1)}, bf16[4,256,512]{2,1,0:T(8,128)(2,1)S(1)}, u32[]{:S(2)}) copy-start(bf16[4,256,512]{2,1,0:T(8,128)(2,1)S(1)} %all-to-all-done.1.own_ref) | copy-start | bytes 3145732
  54.8 40.5 %all-to-all-start = ((bf16[64,56,128]{2,1,0:T(8,128)(2,1)}), bf16[64,56,128]{2,1,0:T(8,128)(2,1)S(1)}, u32[]{:S(2)}, u32[]{:S(2)}) async-start(bf16[64,56,128]{2,1,0:T(8,128)(2,1)} %pack.1), calls=%async_computation | async-start | bytes 1835008 | tf_op jit(solution)/shard_map/all_to_all | solution.py:437
  69.7 29.3 %collective-permute-start.1 = (bf16[4,256,512]{2,1,0:T(8,128)(2,1)S(1)}, bf16[4,256,512]{2,1,0:T(8,128)(2,1)}, u32[]{:S(2)}, u32[]{:S(2)}) collective-permute-start(bf16[4,256,512]{2,1,0:T(8,128)(2,1)S(1)} %all-to-all-done.1.own_ref), channel_id=1, source_target_pairs={{0,1},{1,0},{2,3},{3,2},{4,5},{5,4},{6,7},{7,6},{8,9},{9,8},{10,11... | collective-permute-start | bytes 3145736 | tf_op jit(solution)/shard_map/ppermute | solution.py:445
  95.3 0.9 copy-start.3
  104.0 35.7 %copy-start.6 = (bf16[224,256]{1,0:T(8,128)(2,1)S(1)}, bf16[224,256]{1,0:T(8,128)(2,1)}, u32[]{:S(2)}) copy-start(bf16[224,256]{1,0:T(8,128)(2,1)} %get-tuple-element.14) | copy-start | bytes 344068
  135.3 35.3 %copy-start = (bf16[4,256,1152]{2,1,0:T(8,128)(2,1)}, bf16[4,256,1152]{2,1,0:T(8,128)(2,1)S(1)}, u32[]{:S(2)}) copy-start(bf16[4,256,1152]{2,1,0:T(8,128)(2,1)S(1)} %all_to_all.30.qs_ref.own_ref) | copy-start | bytes 7077892
  135.3 55.5 %collective-permute-start.4 = (bf16[4,256,1152]{2,1,0:T(8,128)(2,1)S(1)}, bf16[4,256,1152]{2,1,0:T(8,128)(2,1)}, u32[]{:S(2)}, u32[]{:S(2)}) collective-permute-start(bf16[4,256,1152]{2,1,0:T(8,128)(2,1)S(1)} %all_to_all.30.qs_ref.own_ref), channel_id=1, source_target_pairs={{0,1},{1,0},{2,3},{3,2},{4,5},{5,4},{6,7},{7,6},{8,9},{9,8},{10,11... | collective-permute-start | bytes 7077896 | tf_op jit(solution)/shard_map/ppermute | solution.py:458
  161.1 9.6 %copy-start.4 = (bf16[1792,256]{1,0:T(8,128)(2,1)}, bf16[1792,256]{1,0:T(8,128)(2,1)S(1)}, u32[]{:S(2)}) copy-start(bf16[1792,256]{1,0:T(8,128)(2,1)S(1)} %all_gather.11.k0_ref.v0_ref) | copy-start | bytes 2752516
  161.1 29.6 %copy-start.12 = (f32[2]{0:T(128)S(1)}, f32[2]{0:T(128)}, u32[]{:S(2)}) copy-start(f32[2]{0:T(128)} %param.24) | copy-start | bytes 28
  161.1 9.6 %collective-permute-start.2 = (bf16[1792,256]{1,0:T(8,128)(2,1)S(1)}, bf16[1792,256]{1,0:T(8,128)(2,1)}, u32[]{:S(2)}, u32[]{:S(2)}) collective-permute-start(bf16[1792,256]{1,0:T(8,128)(2,1)S(1)} %all_gather.11.k0_ref.v0_ref), channel_id=1, source_target_pairs={{0,1},{1,0},{2,3},{3,2},{4,5},{5,4},{6,7},{7,6},{8,9},{9,8},{10,11... | collective-permute-start | bytes 2752520 | tf_op jit(solution)/shard_map/ppermute | solution.py:457
  187.1 20.7 %all-to-all-start.3 = ((bf16[4,912,128]{2,1,0:T(8,128)(2,1)}), bf16[4,912,128]{2,1,0:T(8,128)(2,1)S(1)}, u32[]{:S(2)}, u32[]{:S(2)}) async-start(bf16[4,912,128]{2,1,0:T(8,128)(2,1)} %attend.1), calls=%async_computation.3 | async-start | bytes 1867776 | tf_op jit(solution)/shard_map/all_to_all | solution.py:460
  190.8 5.0 %copy-start.9 = (f32[31,192]{1,0:T(8,128)S(1)}, f32[31,192]{1,0:T(8,128)}, u32[]{:S(2)}) copy-start(f32[31,192]{1,0:T(8,128)} %param.26) | copy-start | bytes 71428
  190.8 5.0 %copy-start.11 = (f32[192]{0:T(256)S(1)}, f32[192]{0:T(256)}, u32[]{:S(2)}) copy-start(f32[192]{0:T(256)} %param.27) | copy-start | bytes 2308
  193.9 8.9 %collective-permute-start.5 = (bf16[8,15,192]{2,1,0:T(8,128)(2,1)}, bf16[8,15,192]{2,1,0:T(8,128)(2,1)S(1)}, u32[]{:S(2)}, u32[]{:S(2)}) collective-permute-start(bf16[8,15,192]{2,1,0:T(8,128)(2,1)} %get-tuple-element.16), channel_id=1, source_target_pairs={{0,1},{1,2},{2,3},{3,4},{4,5},{5,6},{6,7},{7,0},{8,9},{9,10},{10,1... | collective-permute-start | bytes 138248 | tf_op jit(solution)/shard_map/ppermute | solution.py:469
  195.8 8.5 %collective-permute-start.6 = (bf16[8,15,192]{2,1,0:T(8,128)(2,1)}, bf16[8,15,192]{2,1,0:T(8,128)(2,1)S(1)}, u32[]{:S(2)}, u32[]{:S(2)}) collective-permute-start(bf16[8,15,192]{2,1,0:T(8,128)(2,1)} %get-tuple-element.17), channel_id=1, source_target_pairs={{1,0},{2,1},{3,2},{4,3},{5,4},{6,5},{7,6},{0,7},{9,8},{10,9},{11,1... | collective-permute-start | bytes 138248 | tf_op jit(solution)/shard_map/ppermute | solution.py:470
  195.9 6.3 %collective-permute-start.3 = (f32[40,192]{1,0:T(8,128)S(1)}, f32[40,192]{1,0:T(8,128)S(1)}, u32[]{:S(2)}, u32[]{:S(2)}) collective-permute-start(f32[40,192]{1,0:T(8,128)S(1)} %maximum_maximum_fusion), channel_id=1, source_target_pairs={{0,0},{1,32},{2,8},{3,40},{4,16},{5,48},{6,24},{7,56},{8,1},{9,33}... | collective-permute-start | bytes 92168 | tf_op jit(solution)/shard_map/ppermute | solution.py:433
  200.8 2.0 collective-permute-start.7
  202.8 1.5 copy-start.10
  202.8 1.5 copy-start.7
  204.3 0.6 copy-start.8
  207.9 7.7 %copy-start.2 = (bf16[4,912,128]{2,1,0:T(8,128)(2,1)}, bf16[4,912,128]{2,1,0:T(8,128)(2,1)S(1)}, u32[]{:S(2)}) copy-start(bf16[4,912,128]{2,1,0:T(8,128)(2,1)S(1)} %all-to-all-done.3.parts_ref) | copy-start | bytes 2801668
  207.9 13.3 %all-to-all-start.4 = ((f32[8,8,128]{2,1,0:T(8,128)}), f32[8,8,128]{2,1,0:T(8,128)S(1)}, u32[]{:S(2)}, u32[]{:S(2)}) async-start(f32[8,8,128]{2,1,0:T(8,128)} %get-tuple-element.20), calls=%async_computation.4 | async-start | bytes 65536 | tf_op jit(solution)/shard_map/all_to_all | solution.py:476
  221.2 0.6 copy-start.5

commit v7 on v6

--- a/solution.py
+++ b/solution.py
@@ -308,8 +308,11 @@
     lines = []
     for y in range(n):
         acc = jnp.zeros((seg, glu_ref.shape[2]), F32)
-        for j in range(CONV_W):
-            acc = acc + w_ref[j : j + 1, :] * pad_ref[y, j : j + seg]
+        for r in range(8):
+            taps = range(r, CONV_W, 8)
+            shifted = pad_ref[y, r : taps[-1] + seg]
+            for j in taps:
+                acc = acc + w_ref[j : j + 1, :] * shifted[j - r : j - r + seg]
         sum_ref[y] = acc
         column = jnp.sum(acc * acc, axis=1, keepdims=True)
         lines.append(jnp.sum(jnp.where(wide_eye(seg), column, 0.0), axis=0, keepdims=True))
@@ -374,11 +377,12 @@
 
 def sum_kernel(x_ref, out_ref):
     seg = out_ref.shape[0]
+    total = x_ref[0].astype(F32)
+    for g in range(1, x_ref.shape[0]):
+        total = total + x_ref[g].astype(F32)
     for b in range(out_ref.shape[1] // WIDTH):
-        total = x_ref[0, seg * b : seg * b + seg, :].astype(F32)
-        for g in range(1, x_ref.shape[0]):
-            total = total + x_ref[g, seg * b : seg * b + seg, :].astype(F32)
-        out_ref[:, WIDTH * b : WIDTH * b + WIDTH] = total.astype(BF)
+        block = total[seg * b : seg * b + seg]
+        out_ref[:, WIDTH * b : WIDTH * b + WIDTH] = block.astype(BF)
 
 
 def sum_of(parts, seg):

time: 259 us -> 259 us (level)
  no operation moved by 1% of the time
where the time goes in v7:
time: 259 us; the launch traced here: 255 us
  blocking collectives  107 us (41%)
  starting transfers between devices  61.2 us (24%)
  waiting for transfers between devices  38.5 us (15%)
  Pallas kernels  38.4 us (15%)
  local copies, waits for them, and re-layouts  9.38 us (4%)
    all_to_all x1, blocking collectives, local(): rest = lax.all_to_all(rest, 'x', 0, 0, tiled=True)  31.3 us
    all_to_all x1, blocking collectives, local(): reduced = lax.all_to_all(term, 'y', 0, 0, tiled=True)  27.4 us
    all_gather x1, blocking collectives, local(): by_z = lax.all_gather(shard, 'z', axis=0)  27.1 us
    all_to_all x1, waiting for transfers between devices, local(): mine = lax.all_to_all(blocks, PLANE, 0, 0, tiled=True)  21.5 us
    all_gather x1, blocking collectives, local(): kv = lax.all_gather(kv, 'z', axis=0, tiled=True)  21.3 us
    pallas_call x1, Pallas kernels, attend(): pl.pallas_call(functools.partial(attend_kernel, tok=tok, rows=rows, keys=...  16.5 us
    all_to_all x1, starting transfers between devices, local(): mine = lax.all_to_all(blocks, PLANE, 0, 0, tiled=True)  14.9 us
    ppermute x1, starting transfers between devices, local(): shard = lax.ppermute(jnp.concatenate(weights, axis=1), PLANE, swap)  8.83 us
  transfers between devices with their start and end apart: 12, of which 7 were waited for; matrix products, arithmetic and copies ran while one was open for 1% of the time, Pallas kernels for 12%

profile of v7, /device:TPU:1, one launch (start us, length us, event | category | flops | bytes accessed | tf_op | source)
XLA Modules:
  0.0 254.8 jit_solution(5988438841099323365)
XLA Ops:
  0.9 8.8 %collective-permute-start = (bf16[32,1344]{1,0:T(8,128)(2,1)S(1)}, bf16[32,1344]{1,0:T(8,128)(2,1)S(1)}, u32[]{:S(2)}, u32[]{:S(2)}) collective-permute-start(bf16[32,1344]{1,0:T(8,128)(2,1)S(1)} %concatenate.9), channel_id=1, source_target_pairs={{0,0},{1,32},{2,8},{3,40},{4,16},{5,48},{6,24},{7,56},{8,1},{9,33}... | collective-permute-start | bytes 258056 | tf_op jit(solution)/shard_map/ppermute | solution.py:427
  9.7 1.5 collective-permute-done
  11.3 27.1 %all-gather = bf16[256,1344]{1,0:T(8,128)(2,1)S(1)} all-gather(bf16[32,1344]{1,0:T(8,128)(2,1)S(1)} %collective-permute-done), channel_id=2, replica_groups=mesh['z'=8,'y'=8,'x'=4,'c'=2] {'z'}, dimensions={0}, use_global_device_ids=true | all-gather | bytes 774144 | tf_op jit(solution)/shard_map/all_gather | solution.py:444
  38.4 1.1 broadcast_in_dim.35
  39.4 5.6 %all-to-all-start.1 = ((bf16[4,256,512]{2,1,0:T(8,128)(2,1)}), bf16[4,256,512]{2,1,0:T(8,128)(2,1)S(1)}, u32[]{:S(2)}, u32[]{:S(2)}) async-start(bf16[4,256,512]{2,1,0:T(8,128)(2,1)} %broadcast_in_dim.35), calls=%async_computation.1 | async-start | bytes 2097152 | tf_op jit(solution)/shard_map/all_to_all | solution.py:38
  45.1 2.0 pack.1
  47.0 7.8 %all-to-all-done.1.own_ref = bf16[4,256,512]{2,1,0:T(8,128)(2,1)S(1)} async-done(((bf16[4,256,512]{2,1,0:T(8,128)(2,1)}), bf16[4,256,512]{2,1,0:T(8,128)(2,1)S(1)}, u32[]{:S(2)}, u32[]{:S(2)}) %all-to-all-start.1) | async-done | bytes 1048608 | tf_op jit(solution)/shard_map/all_to_all | solution.py:38
  54.8 14.9 %all-to-all-start = ((bf16[64,56,128]{2,1,0:T(8,128)(2,1)}), bf16[64,56,128]{2,1,0:T(8,128)(2,1)S(1)}, u32[]{:S(2)}, u32[]{:S(2)}) async-start(bf16[64,56,128]{2,1,0:T(8,128)(2,1)} %pack.1), calls=%async_computation | async-start | bytes 1835008 | tf_op jit(solution)/shard_map/all_to_all | solution.py:441
  69.7 2.4 collective-permute-start.1
  73.8 21.5 %all-to-all-done.x_ref = bf16[64,56,128]{2,1,0:T(8,128)(2,1)S(1)} async-done(((bf16[64,56,128]{2,1,0:T(8,128)(2,1)}), bf16[64,56,128]{2,1,0:T(8,128)(2,1)S(1)}, u32[]{:S(2)}, u32[]{:S(2)}) %all-to-all-start) | async-done | bytes 917536 | tf_op jit(solution)/shard_map/all_to_all | solution.py:441
  95.3 0.9 copy-done.3
  96.2 2.7 %norm.1.x_ref = bf16[224,2048]{1,0:T(8,128)(2,1)} custom-call(bf16[64,56,128]{2,1,0:T(8,128)(2,1)} %copy-done.3, f32[1,2048]{1,0:T(1,128)} %bitcast.8), custom_call_target="tpu_custom_call" | custom-call | tf_op jit(solution)/shard_map/norm/pallas_call | solution.py:87
  98.9 1.6 broadcast_in_dim.37._
  100.5 3.5 %qkv.1 = (bf16[4,256,1152]{2,1,0:T(8,128)(2,1)}, bf16[224,256]{1,0:T(8,128)(2,1)}) custom-call(s32[1]{0:T(128)} %bitcast.core_ref, bf16[224,2048]{1,0:T(8,128)(2,1)} %norm.1.x_ref, bf16[4,256,512]{2,1,0:T(8,128)(2,1)} %copy-done.1, bf16[4,256,512]{2,1,0:T(8,128)(2,1)} %collective-permute-done.1.other_ref, ...), custom_call_target="tpu_custom_call", output_to_operand_aliasing={{0}: (6, {})} | custom-call | tf_op jit(solution)/shard_map/qkv/pallas_call | solution.py:240
  104.1 31.3 %all_to_all.30.qs_ref.own_ref = bf16[4,256,1152]{2,1,0:T(8,128)(2,1)S(1)} all-to-all(bf16[4,256,1152]{2,1,0:T(8,128)(2,1)} %get-tuple-element.13), channel_id=1, replica_groups=mesh['z'=8,'y'=8,'x'=4,'c'=2] {'x'}, dimensions={0} | all-to-all | bytes 4718592 | tf_op jit(solution)/shard_map/all_to_all | solution.py:459
  135.3 4.5 %collective-permute-start.4 = (bf16[4,256,1152]{2,1,0:T(8,128)(2,1)S(1)}, bf16[4,256,1152]{2,1,0:T(8,128)(2,1)}, u32[]{:S(2)}, u32[]{:S(2)}) collective-permute-start(bf16[4,256,1152]{2,1,0:T(8,128)(2,1)S(1)} %all_to_all.30.qs_ref.own_ref), channel_id=1, source_target_pairs={{0,1},{1,0},{2,3},{3,2},{4,5},{5,4},{6,7},{7,6},{8,9},{9,8},{10,11... | collective-permute-start | bytes 7077896 | tf_op jit(solution)/shard_map/ppermute | solution.py:462
  139.8 21.3 %all_gather.11.k0_ref.v0_ref = bf16[1792,256]{1,0:T(8,128)(2,1)S(1)} all-gather(bf16[224,256]{1,0:T(8,128)(2,1)S(1)} %copy-done.6), channel_id=1, replica_groups=mesh['z'=8,'y'=8,'x'=4,'c'=2] {'z'}, dimensions={0}, use_global_device_ids=true | all-gather | bytes 1032192 | tf_op jit(solution)/shard_map/all_gather | solution.py:460
  161.1 7.6 %collective-permute-start.2 = (bf16[1792,256]{1,0:T(8,128)(2,1)S(1)}, bf16[1792,256]{1,0:T(8,128)(2,1)}, u32[]{:S(2)}, u32[]{:S(2)}) collective-permute-start(bf16[1792,256]{1,0:T(8,128)(2,1)S(1)} %all_gather.11.k0_ref.v0_ref), channel_id=1, source_target_pairs={{0,1},{1,0},{2,3},{3,2},{4,5},{5,4},{6,7},{7,6},{8,9},{9,8},{10,11... | collective-permute-start | bytes 2752520 | tf_op jit(solution)/shard_map/ppermute | solution.py:461
  168.6 2.0 collective-permute-done.2.k1_ref.v1_ref
  170.7 16.5 %attend.1 = bf16[4,912,128]{2,1,0:T(8,128)(2,1)} custom-call(bf16[4,256,1152]{2,1,0:T(8,128)(2,1)} %copy-done, bf16[1792,256]{1,0:T(8,128)(2,1)} %copy-done.4, bf16[1792,256]{1,0:T(8,128)(2,1)} %copy-done.4, bf16[1792,256]{1,0:T(8,128)(2,1)} %collective-permute-done.2.k1_ref.v1_ref, bf16[1792,256]{1,0:T(8,128)(2,1)} %collective-permute-done.2.k1_ref.v1_ref), custom_call_target="tpu_custom_call" | custom-call | flops 9865003008 | bytes 3670016 | tf_op jit(solution)/shard_map/attend/pallas_call | solution.py:149
  187.1 3.5 %all-to-all-start.3 = ((bf16[4,912,128]{2,1,0:T(8,128)(2,1)}), bf16[4,912,128]{2,1,0:T(8,128)(2,1)S(1)}, u32[]{:S(2)}, u32[]{:S(2)}) async-start(bf16[4,912,128]{2,1,0:T(8,128)(2,1)} %attend.1), calls=%async_computation.3 | async-start | bytes 1867776 | tf_op jit(solution)/shard_map/all_to_all | solution.py:464
  190.8 3.1 %glu.1 = (bf16[8,28,192]{2,1,0:T(8,128)(2,1)}, bf16[8,15,192]{2,1,0:T(8,128)(2,1)}, bf16[8,15,192]{2,1,0:T(8,128)(2,1)}, bf16[1,15,192]{2,1,0:T(8,128)(2,1)}) custom-call(s32[1]{0:T(128)} %bitcast.core_ref, s32[1]{0:T(128)} %bitcast.6.t_ref, bf16[224,2048]{1,0:T(8,128)(2,1)} %norm.1.x_ref, bf16[4,256,1152]{2,1,0:T(8,128)(2,1)} %copy-done, ...), custom_call_target="tpu_custom_call" | custom-call | tf_op jit(solution)/shard_map/glu/pallas_call | solution.py:273
  193.9 1.9 collective-permute-start.5
  195.9 4.9 %collective-permute-start.3 = (f32[40,192]{1,0:T(8,128)S(1)}, f32[40,192]{1,0:T(8,128)S(1)}, u32[]{:S(2)}, u32[]{:S(2)}) collective-permute-start(f32[40,192]{1,0:T(8,128)S(1)} %maximum_maximum_fusion), channel_id=1, source_target_pairs={{0,0},{1,32},{2,8},{3,40},{4,16},{5,48},{6,24},{7,56},{8,1},{9,33}... | collective-permute-start | bytes 92168 | tf_op jit(solution)/shard_map/ppermute | solution.py:437
  202.8 1.5 collective-permute-done.6.right_ref
  204.9 3.0 %conv.1 = (f32[8,28,192]{2,1,0:T(8,128)}, f32[8,8,128]{2,1,0:T(8,128)}) custom-call(s32[1]{0:T(128)} %bitcast.6.t_ref, bf16[8,28,192]{2,1,0:T(8,128)(2,1)} %get-tuple-element.15.glu_ref, bf16[8,15,192]{2,1,0:T(8,128)(2,1)} %copy-done.7, bf16[8,15,192]{2,1,0:T(8,128)(2,1)} %copy-done.8, bf16[1,15,192]{2,1,0:T(8,128)(2,1)} %copy-done.10, f32[31,192]{1,0:T(8,128)} %slice.28.w_ref), custom_call_target="tpu_custom_call" | custom-call | tf_op jit(solution)/shard_map/conv/pallas_call | solution.py:326
  207.9 6.4 %all-to-all-start.4 = ((f32[8,8,128]{2,1,0:T(8,128)}), f32[8,8,128]{2,1,0:T(8,128)S(1)}, u32[]{:S(2)}, u32[]{:S(2)}) async-start(f32[8,8,128]{2,1,0:T(8,128)} %get-tuple-element.20), calls=%async_computation.4 | async-start | bytes 65536 | tf_op jit(solution)/shard_map/all_to_all | solution.py:480
  215.6 2.1 combine.1.att_ref
  217.7 3.5 %all-to-all-done.4.sq_ref = f32[8,8,128]{2,1,0:T(8,128)S(1)} async-done(((f32[8,8,128]{2,1,0:T(8,128)}), f32[8,8,128]{2,1,0:T(8,128)S(1)}, u32[]{:S(2)}, u32[]{:S(2)}) %all-to-all-start.4) | async-done | bytes 32800 | tf_op jit(solution)/shard_map/all_to_all | solution.py:480
  221.8 3.6 %out.1 = bf16[8,448,128]{2,1,0:T(8,128)(2,1)} custom-call(s32[1]{0:T(128)} %bitcast.core_ref, bf16[224,256]{1,0:T(8,128)(2,1)} %combine.1.att_ref, f32[8,28,192]{2,1,0:T(8,128)} %get-tuple-element.19.conv_ref, f32[8,8,128]{2,1,0:T(8,128)} %copy-done.5, f32[1,192]{1,0:T(1,128)} %slice.29.gain_ref, bf16[4,256,1152]{2,1,0:T(8,128)(2,1)} %copy-done, ...), custom_call_target="tpu_custom_call" | custom-call | tf_op jit(solution)/shard_map/out/pallas_call | solution.py:367
  225.4 27.4 %all_to_all.31.x_ref = bf16[8,448,128]{2,1,0:T(8,128)(2,1)} all-to-all(bf16[8,448,128]{2,1,0:T(8,128)(2,1)} %out.1), channel_id=1, replica_groups=mesh['z'=8,'y'=8,'x'=4,'c'=2] {'y'}, dimensions={0} | all-to-all | bytes 1835008 | tf_op jit(solution)/shard_map/all_to_all | solution.py:484
  252.8 2.0 sum.1
  (57 shorter events, 7.2 us)
Async XLA Ops:
  0.9 10.4 %collective-permute-start = (bf16[32,1344]{1,0:T(8,128)(2,1)S(1)}, bf16[32,1344]{1,0:T(8,128)(2,1)S(1)}, u32[]{:S(2)}, u32[]{:S(2)}) collective-permute-start(bf16[32,1344]{1,0:T(8,128)(2,1)S(1)} %concatenate.9), channel_id=1, source_target_pairs={{0,0},{1,32},{2,8},{3,40},{4,16},{5,48},{6,24},{7,56},{8,1},{9,33}... | collective-permute-start | bytes 258056 | tf_op jit(solution)/shard_map/ppermute | solution.py:427
  39.4 32.6 %copy-start.13 = (f32[64]{0:T(128)S(1)}, f32[64]{0:T(128)}, u32[]{:S(2)}) copy-start(f32[64]{0:T(128)} %param.22) | copy-start | bytes 772
  39.4 33.2 %copy-start.14 = (f32[64]{0:T(128)S(1)}, f32[64]{0:T(128)}, u32[]{:S(2)}) copy-start(f32[64]{0:T(128)} %param.23) | copy-start | bytes 772
  39.4 15.4 %all-to-all-start.1 = ((bf16[4,256,512]{2,1,0:T(8,128)(2,1)}), bf16[4,256,512]{2,1,0:T(8,128)(2,1)S(1)}, u32[]{:S(2)}, u32[]{:S(2)}) async-start(bf16[4,256,512]{2,1,0:T(8,128)(2,1)} %broadcast_in_dim.35), calls=%async_computation.1 | async-start | bytes 2097152 | tf_op jit(solution)/shard_map/all_to_all | solution.py:38
  54.8 44.1 %copy-start.1 = (bf16[4,256,512]{2,1,0:T(8,128)(2,1)}, bf16[4,256,512]{2,1,0:T(8,128)(2,1)S(1)}, u32[]{:S(2)}) copy-start(bf16[4,256,512]{2,1,0:T(8,128)(2,1)S(1)} %all-to-all-done.1.own_ref) | copy-start | bytes 3145732
  54.8 40.5 %all-to-all-start = ((bf16[64,56,128]{2,1,0:T(8,128)(2,1)}), bf16[64,56,128]{2,1,0:T(8,128)(2,1)S(1)}, u32[]{:S(2)}, u32[]{:S(2)}) async-start(bf16[64,56,128]{2,1,0:T(8,128)(2,1)} %pack.1), calls=%async_computation | async-start | bytes 1835008 | tf_op jit(solution)/shard_map/all_to_all | solution.py:441
  69.7 29.3 %collective-permute-start.1 = (bf16[4,256,512]{2,1,0:T(8,128)(2,1)S(1)}, bf16[4,256,512]{2,1,0:T(8,128)(2,1)}, u32[]{:S(2)}, u32[]{:S(2)}) collective-permute-start(bf16[4,256,512]{2,1,0:T(8,128)(2,1)S(1)} %all-to-all-done.1.own_ref), channel_id=1, source_target_pairs={{0,1},{1,0},{2,3},{3,2},{4,5},{5,4},{6,7},{7,6},{8,9},{9,8},{10,11... | collective-permute-start | bytes 3145736 | tf_op jit(solution)/shard_map/ppermute | solution.py:449
  95.3 0.9 copy-start.3
  104.0 35.7 %copy-start.6 = (bf16[224,256]{1,0:T(8,128)(2,1)S(1)}, bf16[224,256]{1,0:T(8,128)(2,1)}, u32[]{:S(2)}) copy-start(bf16[224,256]{1,0:T(8,128)(2,1)} %get-tuple-element.14) | copy-start | bytes 344068
  135.3 35.3 %copy-start = (bf16[4,256,1152]{2,1,0:T(8,128)(2,1)}, bf16[4,256,1152]{2,1,0:T(8,128)(2,1)S(1)}, u32[]{:S(2)}) copy-start(bf16[4,256,1152]{2,1,0:T(8,128)(2,1)S(1)} %all_to_all.30.qs_ref.own_ref) | copy-start | bytes 7077892
  135.3 55.5 %collective-permute-start.4 = (bf16[4,256,1152]{2,1,0:T(8,128)(2,1)S(1)}, bf16[4,256,1152]{2,1,0:T(8,128)(2,1)}, u32[]{:S(2)}, u32[]{:S(2)}) collective-permute-start(bf16[4,256,1152]{2,1,0:T(8,128)(2,1)S(1)} %all_to_all.30.qs_ref.own_ref), channel_id=1, source_target_pairs={{0,1},{1,0},{2,3},{3,2},{4,5},{5,4},{6,7},{7,6},{8,9},{9,8},{10,11... | collective-permute-start | bytes 7077896 | tf_op jit(solution)/shard_map/ppermute | solution.py:462
  161.1 9.6 %copy-start.4 = (bf16[1792,256]{1,0:T(8,128)(2,1)}, bf16[1792,256]{1,0:T(8,128)(2,1)S(1)}, u32[]{:S(2)}) copy-start(bf16[1792,256]{1,0:T(8,128)(2,1)S(1)} %all_gather.11.k0_ref.v0_ref) | copy-start | bytes 2752516
  161.1 29.6 %copy-start.12 = (f32[2]{0:T(128)S(1)}, f32[2]{0:T(128)}, u32[]{:S(2)}) copy-start(f32[2]{0:T(128)} %param.24) | copy-start | bytes 28
  161.1 9.6 %collective-permute-start.2 = (bf16[1792,256]{1,0:T(8,128)(2,1)S(1)}, bf16[1792,256]{1,0:T(8,128)(2,1)}, u32[]{:S(2)}, u32[]{:S(2)}) collective-permute-start(bf16[1792,256]{1,0:T(8,128)(2,1)S(1)} %all_gather.11.k0_ref.v0_ref), channel_id=1, source_target_pairs={{0,1},{1,0},{2,3},{3,2},{4,5},{5,4},{6,7},{7,6},{8,9},{9,8},{10,11... | collective-permute-start | bytes 2752520 | tf_op jit(solution)/shard_map/ppermute | solution.py:461
  187.1 20.8 %all-to-all-start.3 = ((bf16[4,912,128]{2,1,0:T(8,128)(2,1)}), bf16[4,912,128]{2,1,0:T(8,128)(2,1)S(1)}, u32[]{:S(2)}, u32[]{:S(2)}) async-start(bf16[4,912,128]{2,1,0:T(8,128)(2,1)} %attend.1), calls=%async_computation.3 | async-start | bytes 1867776 | tf_op jit(solution)/shard_map/all_to_all | solution.py:464
  190.8 5.0 %copy-start.9 = (f32[31,192]{1,0:T(8,128)S(1)}, f32[31,192]{1,0:T(8,128)}, u32[]{:S(2)}) copy-start(f32[31,192]{1,0:T(8,128)} %param.26) | copy-start | bytes 71428
  190.8 5.0 %copy-start.11 = (f32[192]{0:T(256)S(1)}, f32[192]{0:T(256)}, u32[]{:S(2)}) copy-start(f32[192]{0:T(256)} %param.27) | copy-start | bytes 2308
  193.9 8.9 %collective-permute-start.5 = (bf16[8,15,192]{2,1,0:T(8,128)(2,1)}, bf16[8,15,192]{2,1,0:T(8,128)(2,1)S(1)}, u32[]{:S(2)}, u32[]{:S(2)}) collective-permute-start(bf16[8,15,192]{2,1,0:T(8,128)(2,1)} %get-tuple-element.16), channel_id=1, source_target_pairs={{0,1},{1,2},{2,3},{3,4},{4,5},{5,6},{6,7},{7,0},{8,9},{9,10},{10,1... | collective-permute-start | bytes 138248 | tf_op jit(solution)/shard_map/ppermute | solution.py:473
  195.8 8.5 %collective-permute-start.6 = (bf16[8,15,192]{2,1,0:T(8,128)(2,1)}, bf16[8,15,192]{2,1,0:T(8,128)(2,1)S(1)}, u32[]{:S(2)}, u32[]{:S(2)}) collective-permute-start(bf16[8,15,192]{2,1,0:T(8,128)(2,1)} %get-tuple-element.17), channel_id=1, source_target_pairs={{1,0},{2,1},{3,2},{4,3},{5,4},{6,5},{7,6},{0,7},{9,8},{10,9},{11,1... | collective-permute-start | bytes 138248 | tf_op jit(solution)/shard_map/ppermute | solution.py:474
  195.9 6.3 %collective-permute-start.3 = (f32[40,192]{1,0:T(8,128)S(1)}, f32[40,192]{1,0:T(8,128)S(1)}, u32[]{:S(2)}, u32[]{:S(2)}) collective-permute-start(f32[40,192]{1,0:T(8,128)S(1)} %maximum_maximum_fusion), channel_id=1, source_target_pairs={{0,0},{1,32},{2,8},{3,40},{4,16},{5,48},{6,24},{7,56},{8,1},{9,33}... | collective-permute-start | bytes 92168 | tf_op jit(solution)/shard_map/ppermute | solution.py:437
  200.8 2.0 collective-permute-start.7
  202.8 1.5 copy-start.10
  202.8 1.5 copy-start.7
  204.3 0.6 copy-start.8
  207.9 7.7 %copy-start.2 = (bf16[4,912,128]{2,1,0:T(8,128)(2,1)}, bf16[4,912,128]{2,1,0:T(8,128)(2,1)S(1)}, u32[]{:S(2)}) copy-start(bf16[4,912,128]{2,1,0:T(8,128)(2,1)S(1)} %all-to-all-done.3.parts_ref) | copy-start | bytes 2801668
  207.9 13.3 %all-to-all-start.4 = ((f32[8,8,128]{2,1,0:T(8,128)}), f32[8,8,128]{2,1,0:T(8,128)S(1)}, u32[]{:S(2)}, u32[]{:S(2)}) async-start(f32[8,8,128]{2,1,0:T(8,128)} %get-tuple-element.20), calls=%async_computation.4 | async-start | bytes 65536 | tf_op jit(solution)/shard_map/all_to_all | solution.py:480
  221.2 0.6 copy-start.5
